TPU v7x, 256 devices: a whole 4x4x8 slice. The times are simulated.
256 devices in a mesh: dp: 4 (over x), kv: 32 (over z, y), tp: 2 (over core).
Axes of the slice: x: 4, y: 4, z: 8, core: 2. Of those that a mesh axis runs over, the one named last changes fastest.
Arguments:
- tokens: bfloat16 [4, 16, 2048], P('dp', None, 'kv'), may hold values from -18 to 18, as said below
- norm_gain: float32 [2048], P('kv'), may hold values from 0.1 to 1.9
- w_query: bfloat16 [2048, 3072], P('kv', 'tp'), may hold values from -0.125 to 0.125
- w_key: bfloat16 [2048, 3072], P('kv', 'tp'), may hold values from -0.125 to 0.125
- w_value: bfloat16 [2048, 3072], P('kv', 'tp'), may hold values from -0.125 to 0.125
- w_gate: bfloat16 [2048, 3072], P('kv', 'tp'), may hold values from -0.125 to 0.125
- w_out: bfloat16 [3072, 2048], P('tp', 'kv'), may hold values from -0.109375 to 0.109375
- head_bias: float32 [24], P('tp'), may hold values from -14 to -2
- cache_keys: bfloat16 [4, 16384, 24, 128], P('dp', 'kv', 'tp'), may hold values from -18 to 18, as said below
- cache_values: bfloat16 [4, 16384, 24, 128], P('dp', 'kv', 'tp'), may hold values from -6 to 6
- prefix_len: int32 [4], P('dp'), may hold values from 12288 to 16364
- accepted: int32 [4], P('dp'), may hold values from 1 to 4
- parent: int32 [4, 16], P('dp'), may hold values from -1 to 14, as said below
Outputs:
- mixed: bfloat16 [4, 16, 2048], P('dp', None, 'kv')
- keys_next: bfloat16 [4, 16384, 24, 128], P('dp', 'kv', 'tp')
- values_next: bfloat16 [4, 16384, 24, 128], P('dp', 'kv', 'tp')
Inputs may be any that keep to these rules, and one draw needn't show every extreme that they name: `tokens`: entries of order one. `cache_keys`: entries of order one. parent of proposal 0 is -1; for p of 1 or more, parent[p] lies in max(p - 3, 0) to p - 1.
All inputs are finite; a program needn't handle non-finite values.
Results may differ from a plain program's by a relative error of at most 0.012.
Values may be sent and summed in bfloat16 or wider, within the bound.
No kernel may reach another device: no remote copies, remote signals or barrier semaphores. Data moves between devices by JAX's collectives and lax.ppermute only.
A program may use at most 64 MiB of HBM per device.

v0:
```python
import jax
import jax.numpy as jnp
from jax import lax
from jax.sharding import PartitionSpec as P

D = 2048
HEAD = 128


EPS = 1e-06


def sent_to_all(value, axis):
    count = lax.axis_size(axis)
    return lax.all_to_all(
        jnp.broadcast_to(value[None], (count, *value.shape)), axis, 0, 0, tiled=True
    )


def over_copies(value, axis):
    return sent_to_all(value, axis).sum(axis=0)


def in_blocks(value, dim, count):
    lengths = value.shape
    pieces = value.reshape(*lengths[:dim], count, lengths[dim] // count, *lengths[dim + 1 :])
    return jnp.moveaxis(pieces, dim, 0)


def summed_on_arrival(value, axis, dim):
    pieces = in_blocks(value, dim, lax.axis_size(axis))
    arrived = lax.all_to_all(pieces, axis, split_axis=0, concat_axis=0, tiled=True)
    return arrived.sum(axis=0)


def laid_out(pieces, dim):
    lengths = list(pieces.shape[1:])
    lengths[dim] *= pieces.shape[0]
    return jnp.moveaxis(pieces, 0, dim).reshape(lengths)


def gather_directly(value, axis, dim):
    pieces = sent_to_all(value, axis)
    return laid_out(pieces, dim)


def taken_together(value, axis):
    everything = sent_to_all(value, axis)
    return jnp.sum(everything.astype(jnp.float32), axis=0)


def gathered_total(value, axis):
    return lax.all_gather(value, axis).astype(jnp.float32).sum(0)


def ancestry(parent):
    count = parent.shape[-1]
    places = jnp.arange(count, dtype=jnp.int32)
    reach = (parent[:, :, None] == places[None, None, :]).astype(jnp.float32)
    for repeat in range(count.bit_length()):
        reach = jnp.minimum(
            reach + jnp.einsum("spj,sjk->spk", reach, reach, precision=lax.Precision.HIGHEST), 1.0
        )
    return reach > 0.5


def after_table(count):
    places = jnp.arange(count, dtype=jnp.int32)
    return (places[:, None] > places[None, :]).astype(jnp.float32)


def sum_after(values):
    table = after_table(values.shape[-1])
    return jnp.einsum("shpk,kc->shpc", values, table, precision=lax.Precision.HIGHEST)


def local(
    tokens,
    norm_gain,
    w_query,
    w_key,
    w_value,
    w_gate,
    w_out,
    head_bias,
    cache_keys,
    cache_values,
    prefix_len,
    accepted,
    parent,
):
    seqs, props, columns = tokens.shape
    width = w_query.shape[1]
    heads = width // HEAD
    flat = tokens.astype(jnp.float32).reshape(seqs * props, columns)
    square_part = jnp.sum(flat * flat, axis=1)
    scaled = (flat * norm_gain).astype(jnp.bfloat16)
    partial_value = jnp.concatenate(
        [
            jnp.dot(scaled, weight, preferred_element_type=jnp.float32)
            for weight in (w_query, w_key, w_value, w_gate)
        ],
        axis=1,
    )
    squares = over_copies(square_part, "kv")
    share = summed_on_arrival(partial_value, "kv", 1)
    rscale = lax.rsqrt(squares / D + EPS)
    projected = gather_directly((share * rscale[:, None]).astype(jnp.bfloat16), "kv", 1)
    shaped = projected.reshape(seqs, props, 4, heads, HEAD)
    query = shaped[:, :, 0]
    key_new = shaped[:, :, 1]
    value_new = shaped[:, :, 2]
    gate = projected[:, 3 * width :].astype(jnp.float32)
    factor = HEAD ** (-0.5)
    bias_col = head_bias[None, :, None, None]
    ctx_dev = cache_keys.shape[1]
    places = lax.axis_index("kv") * ctx_dev + jnp.arange(ctx_dev, dtype=jnp.int32)
    valid = prefix_len + accepted
    live = (places[None, :] < valid[:, None])[:, None, None, :]
    scores = (
        jnp.einsum("sphd,schd->shpc", query, cache_keys, preferred_element_type=jnp.float32)
        * factor
        + bias_col
    )
    keep_log = jnp.where(live, jax.nn.log_sigmoid(-scores), 0.0)
    shard_rest = jnp.sum(keep_log, axis=3)
    family = ancestry(parent)[:, None]
    tree_scores = (
        jnp.einsum("sphd,sjhd->shpj", query, key_new, preferred_element_type=jnp.float32) * factor
        + bias_col
    )
    tree_keep = jnp.where(family, jax.nn.log_sigmoid(-tree_scores), 0.0)
    tail = jnp.sum(tree_keep, axis=3)
    every = gather_directly(shard_rest[None], "kv", 0)
    after = jnp.arange(every.shape[0], dtype=jnp.int32) > lax.axis_index("kv")
    beyond = jnp.sum(jnp.where(after[:, None, None, None], every, 0.0), axis=0)
    later_cache = sum_after(keep_log) + (beyond + tail)[..., None]
    cache_weight = jnp.where(live, jnp.exp(jax.nn.log_sigmoid(scores) + later_cache), 0.0).astype(
        jnp.bfloat16
    )
    later_tree = sum_after(tree_keep)
    tree_weight = jnp.where(
        family, jnp.exp(jax.nn.log_sigmoid(tree_scores) + later_tree), 0.0
    ).astype(jnp.bfloat16)
    local_sum = jnp.einsum(
        "shpc,schd->sphd", cache_weight, cache_values, preferred_element_type=jnp.float32
    )
    attended = taken_together(local_sum.astype(jnp.bfloat16), "kv").astype(jnp.float32)
    attended = attended + jnp.einsum(
        "shpj,sjhd->sphd", tree_weight, value_new, preferred_element_type=jnp.float32
    )
    mixin = (attended.reshape(seqs * props, width) * jax.nn.silu(gate)).astype(jnp.bfloat16)
    part_out = jnp.dot(mixin, w_out, preferred_element_type=jnp.float32).astype(jnp.bfloat16)
    part_out = lax.optimization_barrier(part_out).astype(jnp.float32)
    mixed = (
        gathered_total(part_out.astype(jnp.bfloat16), "tp")
        .astype(jnp.float32)
        .astype(jnp.bfloat16)
        .reshape(seqs, props, w_out.shape[1])
    )
    relative = places[None, :] - valid[:, None]
    picker = (relative[:, :, None] == jnp.arange(props, dtype=jnp.int32)[None, None, :]).astype(
        jnp.bfloat16
    )
    inside = ((relative >= 0) & (relative < props))[:, :, None, None]
    placed_keys = jnp.einsum(
        "scp,sphd->schd", picker, key_new, preferred_element_type=jnp.float32
    ).astype(jnp.bfloat16)
    placed_values = jnp.einsum(
        "scp,sphd->schd", picker, value_new, preferred_element_type=jnp.float32
    ).astype(jnp.bfloat16)
    keys_next = jnp.where(inside, placed_keys, cache_keys)
    values_next = jnp.where(inside, placed_values, cache_values)
    return (mixed, keys_next, values_next)


def solution(mesh):
    return jax.shard_map(
        local,
        mesh=mesh,
        in_specs=(
            P("dp", None, "kv"),
            P("kv"),
            P("kv", "tp"),
            P("kv", "tp"),
            P("kv", "tp"),
            P("kv", "tp"),
            P("tp", "kv"),
            P("tp"),
            P("dp", "kv", "tp", None),
            P("dp", "kv", "tp", None),
            P("dp"),
            P("dp"),
            P("dp", None),
        ),
        out_specs=(P("dp", None, "kv"), P("dp", "kv", "tp", None), P("dp", "kv", "tp", None)),
        check_vma=False,
    )
```

profile of v0, /device:TPU:1, one launch (start us, length us, event | category | flops | bytes accessed | tf_op | source)
XLA Modules:
  0.0 135.6 jit_solution(6108012998178321168)
XLA Ops:
  2.1 12.0 %all-to-all-start.1 = ((f32[32,1,16]{2,1,0:T(1,128)}), f32[32,1,16]{2,1,0:T(1,128)S(1)}, u32[]{:S(2)}, u32[]{:S(2)}) async-start(f32[32,1,16]{2,1,0:T(1,128)} %broadcast_in_dim.59), calls=%async_computation.1 | async-start | bytes 32768 | tf_op jit(solution)/shard_map/all_to_all | solution.py:15
  15.0 1.1 fusion.72
  16.1 1.1 fusion.74
  17.2 1.1 fusion.76
  18.8 1.1 copy.88
  19.9 2.8 %all-to-all-done.1 = f32[32,1,16]{2,1,0:T(1,128)S(1)} async-done(((f32[32,1,16]{2,1,0:T(1,128)}), f32[32,1,16]{2,1,0:T(1,128)S(1)}, u32[]{:S(2)}, u32[]{:S(2)}) %all-to-all-start.1) | async-done | bytes 2080 | tf_op jit(solution)/shard_map/all_to_all | solution.py:15
  22.7 6.4 %all-to-all-start = ((f32[32,16,192]{2,1,0:T(8,128)}), f32[32,16,192]{2,1,0:T(8,128)S(1)}, u32[]{:S(2)}, u32[]{:S(2)}) async-start(f32[32,16,192]{2,1,0:T(8,128)} %bitcast.114), calls=%async_computation | async-start | bytes 1048576 | tf_op jit(solution)/shard_map/all_to_all | solution.py:32
  29.6 14.9 %all-to-all-done = f32[32,16,192]{2,1,0:T(8,128)S(1)} async-done(((f32[32,16,192]{2,1,0:T(8,128)}), f32[32,16,192]{2,1,0:T(8,128)S(1)}, u32[]{:S(2)}, u32[]{:S(2)}) %all-to-all-start) | async-done | bytes 393248 | tf_op jit(solution)/shard_map/all_to_all | solution.py:32
  45.4 6.1 %all-to-all-start.2 = ((bf16[32,16,192]{2,1,0:T(8,128)(2,1)}), bf16[32,16,192]{2,1,0:T(8,128)(2,1)S(1)}, u32[]{:S(2)}, u32[]{:S(2)}) async-start(bf16[32,16,192]{2,1,0:T(8,128)(2,1)} %broadcast_in_dim.60), calls=%async_computation.2 | async-start | bytes 524288 | tf_op jit(solution)/shard_map/all_to_all | solution.py:15
  53.1 8.8 %all-to-all-done.2 = bf16[32,16,192]{2,1,0:T(8,128)(2,1)S(1)} async-done(((bf16[32,16,192]{2,1,0:T(8,128)(2,1)}), bf16[32,16,192]{2,1,0:T(8,128)(2,1)S(1)}, u32[]{:S(2)}, u32[]{:S(2)}) %all-to-all-start.2) | async-done | bytes 196640 | tf_op jit(solution)/shard_map/all_to_all | solution.py:15
  64.8 1.1 reduce.12
  66.7 4.6 %all-to-all-start.3 = ((f32[32,1,192]{2,1,0:T(1,128)}), f32[32,1,192]{2,1,0:T(1,128)S(1)}, u32[]{:S(2)}, u32[]{:S(2)}) async-start(f32[32,1,192]{2,1,0:T(1,128)} %reshape.424), calls=%async_computation.3 | async-start | bytes 65536 | tf_op jit(solution)/shard_map/all_to_all | solution.py:15
  71.4 8.6 %all-to-all-done.3 = f32[32,1,192]{2,1,0:T(1,128)S(1)} async-done(((f32[32,1,192]{2,1,0:T(1,128)}), f32[32,1,192]{2,1,0:T(1,128)S(1)}, u32[]{:S(2)}, u32[]{:S(2)}) %all-to-all-start.3) | async-done | bytes 24608 | tf_op jit(solution)/shard_map/all_to_all | solution.py:15
  81.4 2.1 %fusion.13 = bf16[12,16,512]{2,1,0:T(8,128)(2,1)S(1)} fusion(f32[12,16,512]{2,1,0:T(8,128)} %copy-done.4, f32[12,16]{1,0:T(8,128)S(1)} %add.138, pred[512]{0:T(512)(128)(4,1)S(1)} %fusion.69, u16[16,512]{1,0:T(8,128)(2,1)S(1)} %get-tuple-element.8), kind=kOutput, calls=%fused_computation.16 | convolution fusion | flops 606502912 | bytes 607488 | tf_op jit(solution)/shard_map/shpk,kc->shpc/dot_general | solution.py:74
  83.9 1.5 %broadcast_in_dim.104 = bf16[32,1,16,12,128]{4,2,3,1,0:T(8,128)(2,1)} broadcast(bf16[16,12,128]{2,0,1:T(8,128)(2,1)S(1)} %fusion.22), dimensions={2,3,4} | broadcast | bytes 1622016 | tf_op jit(solution)/shard_map/broadcast_in_dim | solution.py:16
  85.4 4.7 %all-to-all-start.4 = ((bf16[32,1,16,12,128]{4,2,3,1,0:T(8,128)(2,1)}), bf16[32,1,16,12,128]{4,2,3,1,0:T(8,128)(2,1)}, u32[]{:S(2)}, u32[]{:S(2)}) async-start(bf16[32,1,16,12,128]{4,2,3,1,0:T(8,128)(2,1)} %broadcast_in_dim.104), calls=%async_computation.4 | async-start | bytes 3145728 | tf_op jit(solution)/shard_map/all_to_all | solution.py:15
  90.1 1.9 %reshape.416 = bf16[16,6144]{1,0:T(8,128)(2,1)} reshape(bf16[16,32,192]{2,1,0:T(8,128)(2,1)} %copy-done.3) | data formatting | bytes 393216 | tf_op jit(solution)/shard_map/reshape | solution.py:39
  92.0 1.2 fusion.18
  93.3 1.8 %bitcast_select_fusion.1 = bf16[1,512,12,128]{3,1,2,0:T(8,128)(2,1)} fusion(bf16[1,512,12,128]{3,1,2,0:T(8,128)(2,1)S(1)} %copy-done.1, pred[512]{0:T(512)(128)(4,1)S(1)} %compare_and_fusion, bf16[1,16,1,12,128]{4,3,2,1,0:T(8,128)(2,1)S(1)} %get-tuple-element.4, s32[512]{0:T(512)S(1)} %fusion.68), kind=kOutput, calls=%fused_computation.4 | convolution fusion | flops 26746880 | bytes 3197440 | tf_op jit(solution)/shard_map/scp,sphd->schd/dot_general | solution.py:166
  95.1 1.8 %bitcast_select_fusion = bf16[1,512,12,128]{3,1,2,0:T(8,128)(2,1)} fusion(bf16[1,512,12,128]{3,1,2,0:T(8,128)(2,1)S(1)} %copy-done.2, pred[512]{0:T(512)(128)(4,1)S(1)} %compare_and_fusion, bf16[1,16,1,12,128]{4,3,2,1,0:T(8,128)(2,1)S(1)} %get-tuple-element.3, s32[512]{0:T(512)S(1)} %fusion.68), kind=kOutput, calls=%fused_computation.3 | convolution fusion | flops 26746880 | bytes 3197440 | tf_op jit(solution)/shard_map/scp,sphd->schd/dot_general | solution.py:169
  96.8 27.9 %all-to-all-done.4 = bf16[32,1,16,12,128]{4,2,3,1,0:T(8,128)(2,1)} async-done(((bf16[32,1,16,12,128]{4,2,3,1,0:T(8,128)(2,1)}), bf16[32,1,16,12,128]{4,2,3,1,0:T(8,128)(2,1)}, u32[]{:S(2)}, u32[]{:S(2)}) %all-to-all-start.4) | async-done | bytes 1572896 | tf_op jit(solution)/shard_map/all_to_all | solution.py:15
  124.7 1.6 %convert_reduce_fusion = f32[16,12,128]{2,0,1:T(8,128)S(1)} fusion(bf16[32,1,16,12,128]{4,2,3,1,0:T(8,128)(2,1)} %all-to-all-done.4), kind=kLoop, calls=%fused_computation | loop fusion | flops 1548288 | bytes 1671168 | tf_op jit(solution)/shard_map/reduce_sum | solution.py:49
  126.6 1.0 convolution_convert_fusion.2
  127.6 7.4 %all-gather = bf16[32,64]{1,0:T(8,128)(2,1)S(1)} all-gather(bf16[16,64]{1,0:T(8,128)(2,1)S(1)} %convolution_convert_fusion.2), channel_id=2, replica_groups=mesh['dp'=4,'kv'=32,'tp'=2] {'tp'}, dimensions={0}, use_global_device_ids=true | all-gather | bytes 6144 | tf_op jit(solution)/shard_map/all_gather | solution.py:53
  (56 shorter events, 10.4 us)
Async XLA Ops:
  0.6 13.5 %copy-start = (bf16[64,1536]{1,0:T(8,128)(2,1)S(1)}, bf16[64,1536]{1,0:T(8,128)(2,1)}, u32[]{:S(2)}) copy-start(bf16[64,1536]{1,0:T(8,128)(2,1)} %param.18) | copy-start | bytes 589828
  0.6 17.7 %copy-start.8 = (s32[1,16]{1,0:T(1,128)S(1)}, s32[1,16]{1,0:T(1,128)}, u32[]{:S(2)}) copy-start(s32[1,16]{1,0:T(1,128)} %param.25) | copy-start | bytes 196
  2.1 20.6 %all-to-all-start.1 = ((f32[32,1,16]{2,1,0:T(1,128)}), f32[32,1,16]{2,1,0:T(1,128)S(1)}, u32[]{:S(2)}, u32[]{:S(2)}) async-start(f32[32,1,16]{2,1,0:T(1,128)} %broadcast_in_dim.59), calls=%async_computation.1 | async-start | bytes 32768 | tf_op jit(solution)/shard_map/all_to_all | solution.py:15
  22.7 21.8 %all-to-all-start = ((f32[32,16,192]{2,1,0:T(8,128)}), f32[32,16,192]{2,1,0:T(8,128)S(1)}, u32[]{:S(2)}, u32[]{:S(2)}) async-start(f32[32,16,192]{2,1,0:T(8,128)} %bitcast.114), calls=%async_computation | async-start | bytes 1048576 | tf_op jit(solution)/shard_map/all_to_all | solution.py:32
  29.1 33.2 %copy-start.6 = (f32[12]{0:T(128)S(1)}, f32[12]{0:T(128)}, u32[]{:S(2)}) copy-start(f32[12]{0:T(128)} %param.20) | copy-start | bytes 148
  29.4 33.1 %copy-start.1 = (bf16[1,512,12,128]{3,1,2,0:T(8,128)(2,1)S(1)}, bf16[1,512,12,128]{3,1,2,0:T(8,128)(2,1)}, u32[]{:S(2)}) copy-start(bf16[1,512,12,128]{3,1,2,0:T(8,128)(2,1)} %param.21) | copy-start | bytes 4718596
  45.4 16.5 %all-to-all-start.2 = ((bf16[32,16,192]{2,1,0:T(8,128)(2,1)}), bf16[32,16,192]{2,1,0:T(8,128)(2,1)S(1)}, u32[]{:S(2)}, u32[]{:S(2)}) async-start(bf16[32,16,192]{2,1,0:T(8,128)(2,1)} %broadcast_in_dim.60), calls=%async_computation.2 | async-start | bytes 524288 | tf_op jit(solution)/shard_map/all_to_all | solution.py:15
  62.0 1.1 copy-start.3
  62.5 8.8 %copy-start.5 = (f32[12,16,16]{1,2,0:T(8,128)}, f32[12,16,16]{1,2,0:T(8,128)S(1)}, u32[]{:S(2)}) copy-start(f32[12,16,16]{1,2,0:T(8,128)S(1)} %get-tuple-element.7) | copy-start | bytes 36868
  63.1 0.7 copy-start.4
  66.7 13.3 %all-to-all-start.3 = ((f32[32,1,192]{2,1,0:T(1,128)}), f32[32,1,192]{2,1,0:T(1,128)S(1)}, u32[]{:S(2)}, u32[]{:S(2)}) async-start(f32[32,1,192]{2,1,0:T(1,128)} %reshape.424), calls=%async_computation.3 | async-start | bytes 65536 | tf_op jit(solution)/shard_map/all_to_all | solution.py:15
  81.4 2.2 %copy-start.2 = (bf16[1,512,12,128]{3,1,2,0:T(8,128)(2,1)S(1)}, bf16[1,512,12,128]{3,1,2,0:T(8,128)(2,1)}, u32[]{:S(2)}) copy-start(bf16[1,512,12,128]{3,1,2,0:T(8,128)(2,1)} %param.22) | copy-start | bytes 4718596
  85.4 39.3 %all-to-all-start.4 = ((bf16[32,1,16,12,128]{4,2,3,1,0:T(8,128)(2,1)}), bf16[32,1,16,12,128]{4,2,3,1,0:T(8,128)(2,1)}, u32[]{:S(2)}, u32[]{:S(2)}) async-start(bf16[32,1,16,12,128]{4,2,3,1,0:T(8,128)(2,1)} %broadcast_in_dim.104), calls=%async_computation.4 | async-start | bytes 3145728 | tf_op jit(solution)/shard_map/all_to_all | solution.py:15
  96.8 29.8 %copy-start.7 = (bf16[1536,64]{0,1:T(8,128)(2,1)S(1)}, bf16[1536,64]{0,1:T(8,128)(2,1)}, u32[]{:S(2)}) copy-start(bf16[1536,64]{0,1:T(8,128)(2,1)} %param.19) | copy-start | bytes 589828
where the time goes:
time: 136 us
  waiting for transfers between devices  63 us (46%)
  starting transfers between devices  33.9 us (25%)
  matrix products  14 us (10%)
  local copies, waits for them, and re-layouts  9.12 us (7%)
  blocking collectives  7.38 us (5%)
  other arithmetic  5.85 us (4%)
  between operations  2.27 us (2%)
    all_to_all x4, waiting for transfers between devices, sent_to_all(): lax.all_to_all(jnp.broadcast_to(value[None], (count, *value.shape)), axis...  48.1 us
    all_to_all x4, starting transfers between devices, sent_to_all(): lax.all_to_all(jnp.broadcast_to(value[None], (count, *value.shape)), axis...  27.5 us
    all_to_all x1, waiting for transfers between devices, summed_on_arrival(): lax.all_to_all(pieces, axis, split_axis=0, concat_axis=0, tiled=True)  14.9 us
    all_gather x1, blocking collectives, gathered_total(): return lax.all_gather(value, axis).astype(jnp.float32).sum(0)  7.38 us
    all_to_all x1, starting transfers between devices, summed_on_arrival(): lax.all_to_all(pieces, axis, split_axis=0, concat_axis=0, tiled=True)  6.43 us
    dot_general x4, matrix products, local(): jnp.dot(scaled, weight, preferred_element_type=jnp.float32)  4.15 us
    dot_general x2, matrix products, sum_after(): jnp.einsum('shpk,kc->shpc', values, table, precision=lax.Precision.HIGHEST)  3.38 us
    broadcast_in_dim x3, local copies, waits for them, and re-layouts, sent_to_all(): jnp.broadcast_to(value[None], (count, *value.shape))  2.86 us
  transfers between devices with their start and end apart: 5, of which 5 were waited for; matrix products, arithmetic and copies ran while one was open for 10% of the time, Pallas kernels for 0%

commit v1 on v0

v1 whole, which is shorter than its diff:
```python
import jax
import jax.numpy as jnp
from jax import lax
from jax.sharding import PartitionSpec as P

D = 2048
HEAD = 128
EPS = 1e-06
INNER = 8


def groups_of(count):
    outer = count // INNER
    inner_groups = [[a * INNER + i for i in range(INNER)] for a in range(outer)]
    outer_groups = [[a * INNER + i for a in range(outer)] for i in range(INNER)]
    return inner_groups, outer_groups


def exchange(pieces, groups):
    return lax.all_to_all(pieces, "kv", 0, 0, axis_index_groups=groups, tiled=True)


def to_all(value, groups):
    return exchange(jnp.broadcast_to(value[None], (len(groups[0]), *value.shape)), groups)


def in_three(value):
    high = lax.reduce_precision(value, 8, 7)
    rest = value - high
    middle = lax.reduce_precision(rest, 8, 7)
    return jnp.concatenate([high, middle, rest - middle], axis=-1).astype(jnp.bfloat16)


def from_three(value, count):
    value = value[..., : 3 * count].astype(jnp.float32)
    return value[..., :count] + value[..., count : 2 * count] + value[..., 2 * count :]


def block(value, rows):
    return jnp.pad(value, ((0, rows - value.shape[0]), (0, HEAD - value.shape[1])))


def ancestry(parent):
    count = parent.shape[-1]
    places = jnp.arange(count, dtype=jnp.int32)
    reach = (parent[:, None] == places[None, :]).astype(jnp.float32)
    for repeat in range(count.bit_length()):
        reach = jnp.minimum(reach + jnp.dot(reach, reach), 1.0)
    return reach > 0.5


def sum_after(values):
    count = values.shape[-1]
    places = jnp.arange(count, dtype=jnp.int32)
    table = (places[:, None] > places[None, :]).astype(jnp.bfloat16)
    flat = values.reshape(-1, count)
    total = 0.0
    for piece in range(3):
        part = lax.reduce_precision(flat, 8, 7)
        flat = flat - part
        total = total + jnp.dot(
            part.astype(jnp.bfloat16), table, preferred_element_type=jnp.float32
        )
    return total.reshape(values.shape)


def log_sigmoids(scores):
    soft = jnp.log1p(jnp.exp(-jnp.abs(scores)))
    return jnp.minimum(scores, 0.0) - soft, jnp.minimum(-scores, 0.0) - soft


def merged(values, rests, extra):
    total = 0.0
    beyond = extra
    for index in reversed(range(values.shape[0])):
        total = total + jnp.exp(beyond)[..., None] * values[index].astype(jnp.float32)
        beyond = beyond + rests[index]
    return total, beyond


def local(
    tokens,
    norm_gain,
    w_query,
    w_key,
    w_value,
    w_gate,
    w_out,
    head_bias,
    cache_keys,
    cache_values,
    prefix_len,
    accepted,
    parent,
):
    inner_groups, outer_groups = groups_of(lax.axis_size("kv"))
    spot = lax.axis_index("kv")
    _, props, columns = tokens.shape
    heads = w_query.shape[1] // HEAD
    rows = heads * props
    share = 3 * rows // INNER
    flat = tokens[0].astype(jnp.float32)
    square_part = jnp.sum(flat * flat, axis=1)
    scaled = (flat * norm_gain).astype(jnp.bfloat16)
    parts = [
        jnp.einsum(
            "pk,khd->hpd",
            scaled,
            weight.reshape(columns, heads, HEAD),
            preferred_element_type=jnp.float32,
        ).astype(jnp.bfloat16).reshape(rows, HEAD)
        for weight in (w_query, w_key, w_value, w_gate)
    ]
    wide = lambda value: jnp.broadcast_to(value[None], (INNER, *value.shape))
    pieces = jnp.concatenate(
        [
            wide(parts[0]),
            jnp.concatenate(parts[1:], axis=0).reshape(INNER, share, HEAD),
            wide(block(in_three(square_part[None]), 8)),
        ],
        axis=1,
    )
    total = exchange(pieces, inner_groups).astype(jnp.float32).sum(axis=0)
    squares = from_three(total[rows + share], props)
    pieces = jnp.concatenate(
        [total[: rows + share].astype(jnp.bfloat16), block(in_three(squares[None]), 8)], axis=0
    )
    total = to_all(pieces, outer_groups).astype(jnp.float32).sum(axis=0)
    squares = from_three(total[rows + share], props)
    rscale = lax.rsqrt(squares / D + EPS)
    query = (
        (total[:rows].reshape(heads, props, HEAD) * rscale[None, :, None]).astype(jnp.bfloat16)
    )
    turned = jnp.where((spot * share) % props == 0, rscale, jnp.roll(rscale, props // 2))
    turned = jnp.tile(turned, -(-share // props))[:share]
    own_share = (total[rows : rows + share] * turned[:, None]).astype(jnp.bfloat16)

    factor = HEAD ** (-0.5)
    bias_col = head_bias[:, None, None]
    ctx_dev = cache_keys.shape[1]
    valid = (prefix_len + accepted)[0]
    places = spot * ctx_dev + jnp.arange(ctx_dev, dtype=jnp.int32)
    live = (places < valid)[None, None, :]
    scores = (
        jnp.einsum("hpd,chd->hpc", query, cache_keys[0], preferred_element_type=jnp.float32)
        * factor
        + bias_col
    )
    take_log, keep_log = log_sigmoids(scores)
    keep_log = jnp.where(live, keep_log, 0.0)
    rest = jnp.sum(keep_log, axis=2)
    weight = jnp.where(live, jnp.exp(take_log + sum_after(keep_log)), 0.0).astype(jnp.bfloat16)
    local_sum = jnp.einsum(
        "hpc,chd->hpd", weight, cache_values[0], preferred_element_type=jnp.float32
    )
    pieces = jnp.concatenate(
        [
            local_sum.astype(jnp.bfloat16).reshape(rows, HEAD),
            own_share,
            block(in_three(rest), 16),
        ],
        axis=0,
    )
    arrived = to_all(pieces, inner_groups)
    value_sum, rest = merged(
        arrived[:, :rows].reshape(INNER, heads, props, HEAD),
        from_three(arrived[:, rows + share : rows + share + heads], props),
        jnp.zeros((heads, props), jnp.float32),
    )
    shares = arrived[:, rows : rows + share].reshape(3, heads, props, HEAD)
    pieces = jnp.concatenate(
        [value_sum.astype(jnp.bfloat16).reshape(rows, HEAD), block(in_three(rest), 16)], axis=0
    )
    arrived = to_all(pieces, outer_groups)
    key_new, value_new, gate = shares[0], shares[1], shares[2]

    family = ancestry(parent[0])[None]
    tree_scores = (
        jnp.einsum("hpd,hjd->hpj", query, key_new, preferred_element_type=jnp.float32) * factor
        + bias_col
    )
    tree_take, tree_keep = log_sigmoids(tree_scores)
    tree_keep = jnp.where(family, tree_keep, 0.0)
    tail = jnp.sum(tree_keep, axis=2)
    tree_weight = jnp.where(family, jnp.exp(tree_take + sum_after(tree_keep)), 0.0).astype(
        jnp.bfloat16
    )
    tree_part = jnp.einsum(
        "hpj,hjd->hpd", tree_weight, value_new, preferred_element_type=jnp.float32
    )
    opened = jax.nn.silu(gate.astype(jnp.float32))

    attended, _ = merged(
        arrived[:, :rows].reshape(len(outer_groups[0]), heads, props, HEAD),
        from_three(arrived[:, rows : rows + heads], props),
        tail,
    )
    mixin = ((attended + tree_part) * opened).astype(jnp.bfloat16)
    part_out = jnp.einsum(
        "hpd,hdo->po",
        mixin,
        w_out.reshape(heads, HEAD, w_out.shape[1]),
        preferred_element_type=jnp.float32,
    ).astype(jnp.bfloat16)
    both = lax.all_gather(part_out, "tp").astype(jnp.float32)
    mixed = both.sum(0).astype(jnp.bfloat16)[None]

    offset = valid - spot * ctx_dev
    start = jnp.clip(offset, 0, ctx_dev - props)
    source = jnp.arange(props, dtype=jnp.int32) + start - offset
    picker = (source[:, None] == jnp.arange(props, dtype=jnp.int32)[None, :]).astype(jnp.bfloat16)
    inside = ((source >= 0) & (source < props))[None, :, None, None]

    def written(cache, fresh):
        placed = jnp.einsum(
            "rp,hpd->rhd", picker, fresh, preferred_element_type=jnp.float32
        ).astype(jnp.bfloat16)[None]
        there = lax.dynamic_slice(cache, (0, start, 0, 0), (1, props, heads, HEAD))
        return lax.dynamic_update_slice(cache, jnp.where(inside, placed, there), (0, start, 0, 0))

    return (mixed, written(cache_keys, key_new), written(cache_values, value_new))


def solution(mesh):
    return jax.shard_map(
        local,
        mesh=mesh,
        in_specs=(
            P("dp", None, "kv"),
            P("kv"),
            P("kv", "tp"),
            P("kv", "tp"),
            P("kv", "tp"),
            P("kv", "tp"),
            P("tp", "kv"),
            P("tp"),
            P("dp", "kv", "tp", None),
            P("dp", "kv", "tp", None),
            P("dp"),
            P("dp"),
            P("dp", None),
        ),
        out_specs=(P("dp", None, "kv"), P("dp", "kv", "tp", None), P("dp", "kv", "tp", None)),
        check_vma=False,
    )
```

time: 136 us -> 90.5 us (0.67)
  waiting for transfers between devices: 63 us -> 11.7 us
  starting transfers between devices: 33.9 us -> 14.9 us
  blocking collectives: 7.38 us -> 22.5 us
  local copies, waits for them, and re-layouts: 9.12 us -> 14.9 us
  other arithmetic: 5.85 us -> 8.35 us
    all_to_all x5 -> x3, waiting for transfers between devices: 63 us -> 11.7 us  [exchange(): lax.all_to_all(pieces, 'kv', 0, 0, axis_index_groups=groups, tiled=True)]
    all_to_all x5 -> x3, starting transfers between devices: 33.9 us -> 14.9 us  [exchange(): lax.all_to_all(pieces, 'kv', 0, 0, axis_index_groups=groups, tiled=True)]
    all_to_all x0 -> x1, blocking collectives: none -> 15.6 us  [exchange(): lax.all_to_all(pieces, 'kv', 0, 0, axis_index_groups=groups, tiled=True)]
    convert_element_type x1 -> x5, other arithmetic: 0.07 us -> 3.15 us  [the longest x1 1.22 us: local(): value_sum.astype(jnp.bfloat16).reshape(rows, HEAD)]
    dynamic_update_slice x0 -> x2, local copies, waits for them, and re-layouts: none -> 1.86 us  [written(): lax.dynamic_update_slice(cache, jnp.where(inside, placed, there), (0, sta...]
    slice x1 -> x5, local copies, waits for them, and re-layouts: 0.02 us -> 1.7 us  [the longest x1 0.93 us: local(): shares = arrived[:, rows:rows + share].reshape(3, heads, props, HEAD)]
    unnamed x22 -> x32, local copies, waits for them, and re-layouts: 2.51 us -> 3.9 us
    exp x0 -> x4, other arithmetic: none -> 1.39 us  [merged(): jnp.exp(beyond)[..., None] * values[index].astype(jnp.float32)]
  transfers between devices with their start and end apart: 5 -> 3, of which waited for: 5 -> 2; matrix products, arithmetic and copies ran while one was open for 10% -> 20% of each run, Pallas kernels for 0% -> 0%
where the time goes in v1:
time: 90.5 us; the launch traced here: 89.2 us
  blocking collectives  22.5 us (25%)
  local copies, waits for them, and re-layouts  14.9 us (16%)
  starting transfers between devices  14.9 us (16%)
  matrix products  14.5 us (16%)
  waiting for transfers between devices  11.7 us (13%)
  other arithmetic  8.35 us (9%)
  between operations  2.32 us (3%)
    all_to_all x1, blocking collectives, exchange(): lax.all_to_all(pieces, 'kv', 0, 0, axis_index_groups=groups, tiled=True)  15.6 us
    all_to_all x3, starting transfers between devices, exchange(): lax.all_to_all(pieces, 'kv', 0, 0, axis_index_groups=groups, tiled=True)  14.9 us
    all_to_all x3, waiting for transfers between devices, exchange(): lax.all_to_all(pieces, 'kv', 0, 0, axis_index_groups=groups, tiled=True)  11.7 us
    all_gather x1, blocking collectives, local(): both = lax.all_gather(part_out, 'tp').astype(jnp.float32)  6.86 us
    dot_general x6, matrix products, sum_after(): jnp.dot(part.astype(jnp.bfloat16), table, preferred_element_type=jnp.floa...  4.08 us
    unnamed x32, local copies, waits for them, and re-layouts  3.9 us
    dot_general x2, matrix products, written(): jnp.einsum('rp,hpd->rhd', picker, fresh, preferred_element_type=jnp.float32)  3.31 us
    dot_general x1, matrix products, local(): jnp.einsum('hpd,hjd->hpj', query, key_new, preferred_element_type=jnp.flo...  2.4 us
  transfers between devices with their start and end apart: 3, of which 2 were waited for; matrix products, arithmetic and copies ran while one was open for 20% of the time, Pallas kernels for 0%

profile of v1, /device:TPU:1, one launch (start us, length us, event | category | flops | bytes accessed | tf_op | source)
XLA Modules:
  0.0 89.2 jit_solution(14339949764162512932)
XLA Ops:
  0.7 1.5 %copy.80 = bf16[1,512,12,128]{3,1,2,0:T(8,128)(2,1)S(1)} copy(bf16[1,512,12,128]{3,1,2,0:T(8,128)(2,1)} %param.21) | data formatting | bytes 3145728
  4.2 15.6 %all_to_all.20 = bf16[8,272,128]{2,1,0:T(8,128)(2,1)S(1)} all-to-all(bf16[8,272,128]{2,1,0:T(8,128)(2,1)S(1)} %pad_maximum_fusion), channel_id=1, replica_groups={{0,2,4,6,8,10,12,14},{16,18,20,22,24,26,28,30},{32,34,36,38,40,42,44,46..., dimensions={0} | all-to-all | bytes 1114112 | tf_op jit(solution)/shard_map/all_to_all | solution.py:20
  20.9 7.3 %all-to-all-start.1 = ((bf16[4,272,128]{2,1,0:T(8,128)(2,1)}), bf16[4,272,128]{2,1,0:T(8,128)(2,1)}, u32[]{:S(2)}, u32[]{:S(2)}) async-start(bf16[4,272,128]{2,1,0:T(8,128)(2,1)} %broadcast_in_dim.58), calls=%async_computation.1 | async-start | bytes 557056 | tf_op jit(solution)/shard_map/all_to_all | solution.py:20
  29.7 6.6 %all-to-all-done.1 = bf16[4,272,128]{2,1,0:T(8,128)(2,1)} async-done(((bf16[4,272,128]{2,1,0:T(8,128)(2,1)}), bf16[4,272,128]{2,1,0:T(8,128)(2,1)}, u32[]{:S(2)}, u32[]{:S(2)}) %all-to-all-start.1) | async-done | bytes 278560 | tf_op jit(solution)/shard_map/all_to_all | solution.py:20
  36.3 1.0 %convert_reduce_fusion.1 = f32[272,128]{1,0:T(8,128)S(1)} fusion(bf16[4,272,128]{2,1,0:T(8,128)(2,1)} %all-to-all-done.1), kind=kLoop, calls=%fused_computation.48 | loop fusion | flops 243712 | bytes 417792 | tf_op jit(solution)/shard_map/reduce_sum | solution.py:128
  38.0 1.4 %fusion.155 = (f32[12,16]{1,0:T(8,128)S(1)}, f32[12,16,512]{2,1,0:T(8,128)}, f32[12,16,512]{2,1,0:T(8,128)}) fusion(pred[512]{0:T(512)(128)(4,1)S(1)} %add_compare_fusion, f32[12]{0:T(128)S(1)} %copy-done.13, bf16[1,512,12,128]{3,1,2,0:T(8,128)(2,1)S(1)} %copy.80, f32[12,16,128]{2,1,0:T(8,128)S(1)} %bitcast.222, f32[16]{0:T(128)S(1)} %fusion.169), kind=kOutput, calls=%fused_computation.250 | convolution fusion | flops 26099520 | bytes 2458992 | tf_op jit(solution)/shard_map/hpd,chd->hpc/dot_general | solution.py:145
  39.8 1.1 %fusion.31 = (bf16[192,512]{1,0:T(8,128)(2,1)S(1)}, bf16[192,512]{1,0:T(8,128)(2,1)S(1)}, bf16[192,512]{1,0:T(8,128)(2,1)S(1)}) fusion(f32[12,16,512]{2,1,0:T(8,128)} %get-tuple-element.12), kind=kLoop, calls=%fused_computation.50 | loop fusion | flops 786432 | bytes 983040 | tf_op jit(solution)/shard_map/convert_element_type | solution.py:62
  43.2 4.2 %all-to-all-start.2 = ((bf16[8,280,128]{2,1,0:T(8,128)(2,1)}), bf16[8,280,128]{2,1,0:T(8,128)(2,1)}, u32[]{:S(2)}, u32[]{:S(2)}) async-start(bf16[8,280,128]{2,1,0:T(8,128)(2,1)} %broadcast_in_dim.60), calls=%async_computation.2 | async-start | bytes 1146880 | tf_op jit(solution)/shard_map/all_to_all | solution.py:20
  49.7 5.1 %all-to-all-done.2 = bf16[8,280,128]{2,1,0:T(8,128)(2,1)} async-done(((bf16[8,280,128]{2,1,0:T(8,128)(2,1)}), bf16[8,280,128]{2,1,0:T(8,128)(2,1)}, u32[]{:S(2)}, u32[]{:S(2)}) %all-to-all-start.2) | async-done | bytes 573472 | tf_op jit(solution)/shard_map/all_to_all | solution.py:20
  56.4 1.2 %fusion.54 = bf16[192,128]{1,0:T(8,128)(2,1)S(1)} fusion(bf16[8,280,128]{2,1,0:T(8,128)(2,1)} %all-to-all-done.2, f32[192]{0:T(256)S(1)} %reshape.503, f32[192]{0:T(256)S(1)} %reshape.500, f32[192]{0:T(256)S(1)} %reshape.485, f32[192]{0:T(256)S(1)} %exp.116, f32[192]{0:T(256)S(1)} %exp.114, f32[192]{0:T(256)S(1)} %exp.112, f32[192]{0:T(256)S(1)} %exp.110), kind=kLoop, calls=%fused_computation.82 | loop fusion | flops 565248 | bytes 447744 | tf_op jit(solution)/shard_map/convert_element_type | solution.py:172
  58.3 3.4 %all-to-all-start.3 = ((bf16[4,208,128]{2,1,0:T(8,128)(2,1)}), bf16[4,208,128]{2,1,0:T(8,128)(2,1)S(1)}, u32[]{:S(2)}, u32[]{:S(2)}) async-start(bf16[4,208,128]{2,1,0:T(8,128)(2,1)} %broadcast_in_dim.61), calls=%async_computation.3 | async-start | bytes 425984 | tf_op jit(solution)/shard_map/all_to_all | solution.py:20
  61.7 0.9 %slice.252 = bf16[8,72,128]{2,1,0:T(8,128)(2,1)S(1)} slice(bf16[8,280,128]{2,1,0:T(8,128)(2,1)} %all-to-all-done.2), slice={[0:8], [192:264], [0:128]} | slice | bytes 294912 | tf_op jit(solution)/shard_map/slice | solution.py:170
  63.3 2.4 %fusion.151 = (f32[12,16]{1,0:T(8,128)}, f32[12,16,16]{1,2,0:T(8,128)S(1)}, f32[12,16,16]{1,2,0:T(8,128)}) fusion(pred[16,16]{0,1:T(8,128)(4,1)} %copy.30, f32[12]{0:T(128)} %param.20, bf16[3,12,16,128]{3,2,1,0:T(8,128)(2,1)S(1)} %bitcast.229, f32[12,16,128]{2,1,0:T(8,128)} %bitcast.223, f32[16]{0:T(128)} %copy-done.12), kind=kOutput, calls=%fused_computation.247 | convolution fusion | flops 863040 | bytes 173168 | tf_op jit(solution)/shard_map/hpd,hjd->hpj/dot_general | solution.py:179
  66.4 1.6 %reshape.476 = f32[192,16]{0,1:T(8,128)} reshape(f32[12,16,16]{1,0,2:T(8,128)} %copy.35) | data formatting | bytes 24576 | tf_op jit(solution)/shard_map/reshape | solution.py:56
  68.9 0.9 %convolution_add_fusion.4 = f32[192,16]{0,1:T(8,128)S(1)} fusion(f32[192,16]{0,1:T(8,128)S(1)} %fusion.83, f32[192,16]{0,1:T(8,128)} %reshape.476), kind=kOutput, calls=%fused_computation.25 | convolution fusion | flops 113920 | bytes 36864 | tf_op jit(solution)/shard_map/dot_general | solution.py:61
  69.8 1.6 %fusion.28 = bf16[1,16,12,128]{3,1,2,0:T(8,128)(2,1)} fusion(bf16[1,512,12,128]{3,1,2,0:T(8,128)(2,1)S(1)} %copy.80, s32[]{:T(128)S(6)} %min.40, pred[16]{0:T(512)(128)(4,1)} %compare_and_fusion, bf16[3,12,16,128]{3,2,1,0:T(8,128)(2,1)} %bitcast.230, s32[16]{0:T(128)} %add_subtract_fusion), kind=kOutput, calls=%fused_computation.40 | convolution fusion | flops 835840 | bytes 148484 | tf_op jit(solution)/shard_map/rp,hpd->rhd/dot_general | solution.py:215
  71.4 1.5 %convolution_add_fusion.3 = f32[192,16]{0,1:T(8,128)} fusion(f32[192,16]{0,1:T(8,128)S(1)} %convolution_add_fusion.4, f32[192,16]{0,1:T(8,128)} %reshape.476), kind=kOutput, calls=%fused_computation.24 | convolution fusion | flops 120064 | bytes 36864 | tf_op jit(solution)/shard_map/dot_general | solution.py:61
  72.9 1.5 %reshape.477 = f32[12,16,16]{1,0,2:T(8,128)} reshape(f32[192,16]{0,1:T(8,128)} %convolution_add_fusion.3) | data formatting | bytes 24576 | tf_op jit(solution)/shard_map/reshape | solution.py:64
  74.4 0.9 %dynamic_update_slice.6 = bf16[1,512,12,128]{3,1,2,0:T(8,128)(2,1)S(1)} dynamic-update-slice(bf16[1,512,12,128]{3,1,2,0:T(8,128)(2,1)S(1)} %copy.80, bf16[1,16,12,128]{3,1,2,0:T(8,128)(2,1)} %fusion.28, s32[]{:T(128)} %constant.46.clone.1, s32[]{:T(128)S(6)} %min.40, s32[]{:T(128)} %constant.46.clone.1, s32[]{:T(128)} %constant.46.clone.1) | dynamic-update-slice | bytes 98308 | tf_op jit(solution)/shard_map/dynamic_update_slice | solution.py:219
  75.3 1.7 %fusion.27 = bf16[1,16,12,128]{3,1,2,0:T(8,128)(2,1)} fusion(bf16[1,512,12,128]{3,1,2,0:T(8,128)(2,1)S(1)} %copy.81, s32[]{:T(128)S(6)} %min.40, pred[16]{0:T(512)(128)(4,1)} %compare_and_fusion, bf16[3,12,16,128]{3,2,1,0:T(8,128)(2,1)} %bitcast.231, s32[16]{0:T(128)} %add_subtract_fusion), kind=kOutput, calls=%fused_computation.39 | convolution fusion | flops 835840 | bytes 148484 | tf_op jit(solution)/shard_map/rp,hpd->rhd/dot_general | solution.py:215
  77.0 0.9 %dynamic_update_slice.7 = bf16[1,512,12,128]{3,1,2,0:T(8,128)(2,1)S(1)} dynamic-update-slice(bf16[1,512,12,128]{3,1,2,0:T(8,128)(2,1)S(1)} %copy.81, bf16[1,16,12,128]{3,1,2,0:T(8,128)(2,1)} %fusion.27, s32[]{:T(128)} %constant.46.clone.1, s32[]{:T(128)S(6)} %min.40, s32[]{:T(128)} %constant.46.clone.1, s32[]{:T(128)} %constant.46.clone.1) | dynamic-update-slice | bytes 98308 | tf_op jit(solution)/shard_map/dynamic_update_slice | solution.py:219
  78.1 1.4 %fusion.123 = (f32[12,16]{1,0:T(8,128)}, f32[12,16]{1,0:T(8,128)}, f32[12,16]{1,0:T(8,128)}, f32[12,16]{1,0:T(8,128)}) fusion(f32[12,16]{1,0:T(8,128)} %get-tuple-element.3, f32[4,12,16]{2,1,0:T(8,128)S(1)} %slice_add_fusion.2), kind=kLoop, calls=%fused_computation.207 | loop fusion | flops 576 | bytes 6144 | tf_op jit(solution)/shard_map/exp | solution.py:76
  80.1 1.6 %fusion.25 = bf16[16,64]{1,0:T(8,128)(2,1)S(1)} fusion(bf16[12,16,128]{2,1,0:T(8,128)(2,1)} %bitcast.234, bf16[12,16,128]{2,1,0:T(8,128)(2,1)} %bitcast.235, bf16[12,16,128]{2,1,0:T(8,128)(2,1)} %bitcast.236, bf16[12,16,128]{2,1,0:T(8,128)(2,1)} %bitcast.233, f32[12,16,16]{1,0,2:T(8,128)} %reshape.477, f32[12,16,16]{1,2,0:T(8,128)} %get-tuple-element.44, ...), kind=kOutput, calls=%fused_computation.37 | convolution fusion | flops 4421632 | bytes 757760 | tf_op jit(solution)/shard_map/hpd,hdo->po/dot_general | solution.py:199
  81.7 6.9 %all-gather = bf16[32,64]{1,0:T(8,128)(2,1)S(1)} all-gather(bf16[16,64]{1,0:T(8,128)(2,1)S(1)} %fusion.25), channel_id=2, replica_groups=mesh['dp'=4,'kv'=32,'tp'=2] {'tp'}, dimensions={0}, use_global_device_ids=true | all-gather | bytes 6144 | tf_op jit(solution)/shard_map/all_gather | solution.py:205
  (98 shorter events, 14.6 us)
Async XLA Ops:
  0.6 2.8 %copy-start = (bf16[64,1536]{1,0:T(8,128)(2,1)S(1)}, bf16[64,1536]{1,0:T(8,128)(2,1)}, u32[]{:S(2)}) copy-start(bf16[64,1536]{1,0:T(8,128)(2,1)} %param.18) | copy-start | bytes 589828
  0.6 1.9 %copy-start.3 = (bf16[1,512,12,128]{3,1,2,0:T(8,128)(2,1)S(1)}, bf16[1,512,12,128]{3,1,2,0:T(8,128)(2,1)}, u32[]{:S(2)}) copy-start(bf16[1,512,12,128]{3,1,2,0:T(8,128)(2,1)} %param.22) | copy-start | bytes 4718596
  2.6 0.7 copy-start.10
  2.6 0.8 copy-start.11
  2.6 1.0 %copy-start.6 = (bf16[64,1536]{1,0:T(8,128)(2,1)S(1)}, bf16[64,1536]{1,0:T(8,128)(2,1)}, u32[]{:S(2)}) copy-start(bf16[64,1536]{1,0:T(8,128)(2,1)} %param.17) | copy-start | bytes 589828
  2.6 1.1 %copy-start.7 = (bf16[64,1536]{1,0:T(8,128)(2,1)S(1)}, bf16[64,1536]{1,0:T(8,128)(2,1)}, u32[]{:S(2)}) copy-start(bf16[64,1536]{1,0:T(8,128)(2,1)} %param.16) | copy-start | bytes 589828
  2.6 1.3 %copy-start.8 = (bf16[64,1536]{1,0:T(8,128)(2,1)S(1)}, bf16[64,1536]{1,0:T(8,128)(2,1)}, u32[]{:S(2)}) copy-start(bf16[64,1536]{1,0:T(8,128)(2,1)} %param.15) | copy-start | bytes 589828
  4.2 25.3 %copy-start.14 = (s32[1,16]{1,0:T(1,128)S(1)}, s32[1,16]{1,0:T(1,128)}, u32[]{:S(2)}) copy-start(s32[1,16]{1,0:T(1,128)} %param.25) | copy-start | bytes 196
  19.9 18.1 %copy-start.13 = (f32[12]{0:T(128)S(1)}, f32[12]{0:T(128)}, u32[]{:S(2)}) copy-start(f32[12]{0:T(128)} %param.20) | copy-start | bytes 148
  20.9 15.4 %all-to-all-start.1 = ((bf16[4,272,128]{2,1,0:T(8,128)(2,1)}), bf16[4,272,128]{2,1,0:T(8,128)(2,1)}, u32[]{:S(2)}, u32[]{:S(2)}) async-start(bf16[4,272,128]{2,1,0:T(8,128)(2,1)} %broadcast_in_dim.58), calls=%async_computation.1 | async-start | bytes 557056 | tf_op jit(solution)/shard_map/all_to_all | solution.py:20
  37.4 0.6 copy-start.5
  37.4 2.2 %copy-start.12 = (f32[16]{0:T(128)}, f32[16]{0:T(128)S(1)}, u32[]{:S(2)}) copy-start(f32[16]{0:T(128)S(1)} %fusion.169) | copy-start | bytes 196
  40.9 1.0 %copy-start.4 = (f32[12,16,512]{2,1,0:T(8,128)S(1)}, f32[12,16,512]{2,1,0:T(8,128)}, u32[]{:S(2)}) copy-start(f32[12,16,512]{2,1,0:T(8,128)} %get-tuple-element.43) | copy-start | bytes 1179652
  43.2 11.6 %all-to-all-start.2 = ((bf16[8,280,128]{2,1,0:T(8,128)(2,1)}), bf16[8,280,128]{2,1,0:T(8,128)(2,1)}, u32[]{:S(2)}, u32[]{:S(2)}) async-start(bf16[8,280,128]{2,1,0:T(8,128)(2,1)} %broadcast_in_dim.60), calls=%async_computation.2 | async-start | bytes 1146880 | tf_op jit(solution)/shard_map/all_to_all | solution.py:20
  58.3 19.7 %all-to-all-start.3 = ((bf16[4,208,128]{2,1,0:T(8,128)(2,1)}), bf16[4,208,128]{2,1,0:T(8,128)(2,1)S(1)}, u32[]{:S(2)}, u32[]{:S(2)}) async-start(bf16[4,208,128]{2,1,0:T(8,128)(2,1)} %broadcast_in_dim.61), calls=%async_computation.3 | async-start | bytes 425984 | tf_op jit(solution)/shard_map/all_to_all | solution.py:20
  62.6 0.7 copy-start.9
  75.3 13.9 %copy-start.1 = (bf16[1,512,12,128]{3,1,2,0:T(8,128)(2,1)}, bf16[1,512,12,128]{3,1,2,0:T(8,128)(2,1)S(1)}, u32[]{:S(2)}) copy-start(bf16[1,512,12,128]{3,1,2,0:T(8,128)(2,1)S(1)} %dynamic_update_slice.6) | copy-start | bytes 4718596
  77.9 11.2 %copy-start.2 = (bf16[1,512,12,128]{3,1,2,0:T(8,128)(2,1)}, bf16[1,512,12,128]{3,1,2,0:T(8,128)(2,1)S(1)}, u32[]{:S(2)}) copy-start(bf16[1,512,12,128]{3,1,2,0:T(8,128)(2,1)S(1)} %dynamic_update_slice.7) | copy-start | bytes 4718596

commit v2 on v0

v2 whole, which is shorter than its diff:
```python
import jax
import jax.numpy as jnp
from jax import lax
from jax.experimental import pallas as pl
from jax.experimental.pallas import tpu as pltpu
from jax.sharding import PartitionSpec as P

D = 2048
HEAD = 128
EPS = 1e-06
INNER = 8
PROPS = 16
WINDOW = 32
F32 = jnp.float32
BF16 = jnp.bfloat16
VMEM = pl.BlockSpec(memory_space=pltpu.VMEM)
SMEM = pl.BlockSpec(memory_space=pltpu.SMEM)
ANY = pl.BlockSpec(memory_space=pl.ANY)


def groups_of(count):
    outer = count // INNER
    inner_groups = [[a * INNER + i for i in range(INNER)] for a in range(outer)]
    outer_groups = [[a * INNER + i for a in range(outer)] for i in range(INNER)]
    return inner_groups, outer_groups


def exchange(pieces, groups):
    return lax.all_to_all(pieces, "kv", 0, 0, axis_index_groups=groups, tiled=True)


def iota(shape, dim):
    return lax.broadcasted_iota(jnp.int32, shape, dim)


def in_three(value):
    high = value.astype(BF16).astype(F32)
    rest = value - high
    middle = rest.astype(BF16).astype(F32)
    return high, middle, rest - middle


def dot(left, right):
    return jnp.dot(left, right, preferred_element_type=F32)


def dot_t(left, right):
    return lax.dot_general(left, right, (((1,), (1,)), ((), ())), preferred_element_type=F32)


def log_sigmoids(scores):
    soft = jnp.log1p(jnp.exp(-jnp.abs(scores)))
    return jnp.minimum(scores, 0.0) - soft, jnp.minimum(-scores, 0.0) - soft


def square_block(squares):
    lane = iota((PROPS, HEAD), 1)
    block = jnp.zeros((PROPS, HEAD), F32)
    for index, piece in enumerate(in_three(squares)):
        block = jnp.where(lane == index, piece, block)
    return block.astype(BF16)


def rest_block(rests):
    lane = iota((PROPS, HEAD), 1)
    block = jnp.zeros((PROPS, HEAD), F32)
    for index, rest in enumerate(rests):
        block = jnp.where(lane == index, rest, block)
    high, middle, low = in_three(block)
    block = high + pltpu.roll(middle, PROPS, 1) + pltpu.roll(low, 2 * PROPS, 1)
    return block.astype(BF16)


def rest_sums(block):
    block = block.astype(F32)
    return block + pltpu.roll(block, HEAD - PROPS, 1) + pltpu.roll(block, HEAD - 2 * PROPS, 1)


def after_table(width):
    row = iota((width, 2 * HEAD), 0)
    column = iota((width, 2 * HEAD), 1)
    return jnp.where((row > column) | (column >= HEAD), 1.0, 0.0).astype(BF16)


def after_and_all(values, table):
    high = values.astype(BF16)
    rest = values - high.astype(F32)
    middle = rest.astype(BF16)
    low = (rest - middle.astype(F32)).astype(BF16)
    sums = dot(high, table) + dot(middle, table) + dot(low, table)
    return sums[:, :HEAD], sums[:, HEAD:]


def project_kernel(tokens, gain, w_query, w_key, w_value, w_gate, out):
    heads = w_query.shape[1] // HEAD
    rows = heads * PROPS
    share = out.shape[1] - rows - PROPS
    flat = tokens[...].astype(F32)
    block = square_block(jnp.sum(flat * flat, axis=1, keepdims=True))
    scaled = (flat * gain[...]).astype(BF16)
    query = dot(scaled, w_query[...]).astype(BF16)
    for dest in range(INNER):
        for head in range(heads):
            out[dest, head * PROPS : (head + 1) * PROPS, :] = query[
                :, head * HEAD : (head + 1) * HEAD
            ]
        out[dest, rows + share :, :] = block
    slots = share // PROPS
    for which, weight in enumerate((w_key, w_value, w_gate)):
        part = dot(scaled, weight[...]).astype(BF16)
        for head in range(heads):
            dest, slot = divmod(which * heads + head, slots)
            out[dest, rows + slot * PROPS : rows + (slot + 1) * PROPS, :] = part[
                :, head * HEAD : (head + 1) * HEAD
            ]
    for spare in range(3 * heads, INNER * slots):
        dest, slot = divmod(spare, slots)
        out[dest, rows + slot * PROPS : rows + (slot + 1) * PROPS, :] = jnp.zeros(
            (PROPS, HEAD), BF16
        )


def add_up(arrived):
    total = arrived[0].astype(F32)
    for index in range(1, arrived.shape[0]):
        total = total + arrived[index].astype(F32)
    return total


def forward_kernel(arrived, out):
    count = arrived.shape[1] - PROPS
    total = add_up(arrived)
    sums = total[:count].astype(BF16)
    block = square_block(jnp.sum(total[count:], axis=1, keepdims=True))
    for dest in range(out.shape[0]):
        out[dest, :count, :] = sums
        out[dest, count:, :] = block


def attend_kernel(
    scalars,
    arrived,
    bias,
    keys,
    values,
    out,
    query_out,
    keys_next,
    values_next,
    keys_window,
    values_window,
    sems,
):
    heads, ctx_dev, _ = keys.shape
    rows = heads * PROPS
    copies = [
        pltpu.make_async_copy(keys, keys_next, sems.at[0]),
        pltpu.make_async_copy(values, values_next, sems.at[1]),
    ]
    for copy in copies:
        copy.start()
    offset = scalars[0]
    first = pl.multiple_of(scalars[1], PROPS)
    total = add_up(arrived)
    squares = jnp.sum(total[arrived.shape[1] - PROPS :], axis=1, keepdims=True)
    rscale = lax.rsqrt(squares / D + EPS)
    share = arrived.shape[1] - PROPS - rows
    for slot in range(share // PROPS):
        there = slice(rows + slot * PROPS, rows + (slot + 1) * PROPS)
        piece = (total[there] * rscale).astype(BF16)
        for dest in range(INNER):
            out[dest, there, :] = piece
    factor = HEAD ** (-0.5)
    live = iota((PROPS, ctx_dev), 1) < offset
    takes, keeps = [], []
    for head in range(heads):
        there = slice(head * PROPS, (head + 1) * PROPS)
        query = (total[there] * rscale).astype(BF16)
        query_out[there, :] = query
        scores = dot_t(query, keys[head]) * factor + bias[head : head + 1, :]
        take, keep = log_sigmoids(scores)
        takes.append(take)
        keeps.append(jnp.where(live, keep, 0.0))
    keep = jnp.concatenate(keeps, axis=0)
    table = after_table(HEAD)
    beyond = jnp.zeros((rows, HEAD), F32)
    laters = []
    for chunk in reversed(range(ctx_dev // HEAD)):
        inside, whole = after_and_all(keep[:, chunk * HEAD : (chunk + 1) * HEAD], table)
        laters.append(inside + beyond)
        beyond = beyond + whole
    later = jnp.concatenate(laters[::-1], axis=1)
    rests = []
    for head in range(heads):
        there = slice(head * PROPS, (head + 1) * PROPS)
        weight = jnp.where(live, jnp.exp(takes[head] + later[there]), 0.0).astype(BF16)
        summed = dot(weight, values[head]).astype(BF16)
        for dest in range(INNER):
            out[dest, there, :] = summed
        rests.append(beyond[there])
    block = rest_block(rests)
    for dest in range(INNER):
        out[dest, rows + share :, :] = block
    keys_window[...] = keys[:, pl.ds(first, WINDOW), :]
    values_window[...] = values[:, pl.ds(first, WINDOW), :]
    for copy in copies:
        copy.wait()


def merge_kernel(arrived, out, fresh):
    count = arrived.shape[0]
    rows = out.shape[1] - PROPS
    heads = rows // PROPS
    share = arrived.shape[1] - PROPS - rows
    for source in range(count):
        fresh[source * share : (source + 1) * share, :] = arrived[source, rows : rows + share, :]
    beyond = jnp.zeros((PROPS, HEAD), F32)
    factors = []
    for source in reversed(range(count)):
        factors.append(jnp.exp(beyond))
        beyond = beyond + rest_sums(arrived[source, rows + share :, :])
    factors = factors[::-1]
    for head in range(heads):
        there = slice(head * PROPS, (head + 1) * PROPS)
        total = jnp.zeros((PROPS, HEAD), F32)
        for source in range(count):
            total = total + factors[source][:, head : head + 1] * arrived[
                source, there, :
            ].astype(F32)
        total = total.astype(BF16)
        for dest in range(out.shape[0]):
            out[dest, there, :] = total
    block = rest_block([beyond[:, head : head + 1] for head in range(heads)])
    for dest in range(out.shape[0]):
        out[dest, rows:, :] = block


def finish_kernel(
    scalars,
    parent,
    arrived,
    fresh,
    query,
    bias,
    w_out,
    keys_window,
    values_window,
    keys_old,
    values_old,
    out,
    keys_next,
    values_next,
    mixin,
    patches,
    masks,
    sems,
):
    del keys_old, values_old
    count = arrived.shape[0]
    rows = arrived.shape[1] - PROPS
    heads = rows // PROPS
    offset = scalars[0]
    first = pl.multiple_of(scalars[1], PROPS)
    source = first + iota((WINDOW, PROPS), 0) - offset
    picker = jnp.where(source == iota((WINDOW, PROPS), 1), 1.0, 0.0).astype(BF16)
    source = first + iota((WINDOW, HEAD), 0) - offset
    inside = (source >= 0) & (source < PROPS)
    copies = []
    for which, (window, target) in enumerate(
        ((keys_window, keys_next), (values_window, values_next))
    ):
        patched = patches.at[which]
        for head in range(heads):
            start = (which * heads + head) * PROPS
            placed = dot(picker, fresh[start : start + PROPS, :])
            patches[which, head] = jnp.where(inside, placed, window[head].astype(F32)).astype(BF16)
        copies.append(
            pltpu.make_async_copy(patched, target.at[:, pl.ds(first, WINDOW), :], sems.at[which])
        )
        copies[-1].start()
    row = iota((PROPS, PROPS), 0)
    reach = jnp.zeros((PROPS, PROPS), jnp.int32)
    masks[0] = 0
    for index in range(1, PROPS):
        above = parent[index]
        mask = masks[above] | (1 << above)
        masks[index] = mask
        reach = jnp.where(row == index, mask, reach)
    family = ((reach >> iota((PROPS, PROPS), 1)) & 1) == 1
    factor = HEAD ** (-0.5)
    takes, keeps = [], []
    for head in range(heads):
        there = slice(head * PROPS, (head + 1) * PROPS)
        scores = dot_t(query[there, :], fresh[there, :]) * factor + bias[head : head + 1, :PROPS]
        take, keep = log_sigmoids(scores)
        takes.append(take)
        keeps.append(jnp.where(family, keep, 0.0))
    later, tail = after_and_all(jnp.concatenate(keeps, axis=0), after_table(PROPS))
    beyond = jnp.zeros((PROPS, HEAD), F32)
    beyonds = []
    for index in reversed(range(count)):
        beyonds.append(beyond)
        beyond = beyond + rest_sums(arrived[index, rows:, :])
    beyonds = beyonds[::-1]
    for head in range(heads):
        there = slice(head * PROPS, (head + 1) * PROPS)
        weight = jnp.where(family, jnp.exp(takes[head] + later[there, :PROPS]), 0.0).astype(BF16)
        start = (heads + head) * PROPS
        total = dot(weight, fresh[start : start + PROPS, :])
        for index in range(count):
            total = total + jnp.exp(beyonds[index][:, head : head + 1] + tail[there]) * arrived[
                index, there, :
            ].astype(F32)
        start = (2 * heads + head) * PROPS
        gate = fresh[start : start + PROPS, :].astype(F32)
        mixin[:, head * HEAD : (head + 1) * HEAD] = (total * (gate * jax.nn.sigmoid(gate))).astype(
            BF16
        )
    out[...] = dot_t(mixin[...], w_out[...]).astype(BF16)
    for copy in copies:
        copy.wait()


def shaped(dims, dtype=BF16):
    return jax.ShapeDtypeStruct(dims, dtype)


def local(
    tokens,
    norm_gain,
    w_query,
    w_key,
    w_value,
    w_gate,
    w_out,
    head_bias,
    cache_keys,
    cache_values,
    prefix_len,
    accepted,
    parent,
):
    inner_groups, outer_groups = groups_of(lax.axis_size("kv"))
    outer = len(outer_groups[0])
    spot = lax.axis_index("kv")
    heads = w_query.shape[1] // HEAD
    ctx_dev = cache_keys.shape[1]
    rows = heads * PROPS
    share = -(-3 * heads // INNER) * PROPS
    sent = rows + share + PROPS
    offset = (prefix_len + accepted)[0] - spot * ctx_dev
    first = jnp.clip(offset // PROPS * PROPS, 0, ctx_dev - WINDOW)
    scalars = jnp.stack([offset, first])
    bias = jnp.broadcast_to(head_bias[:, None], (heads, ctx_dev))
    keys = jnp.transpose(cache_keys[0], (1, 0, 2))
    values = jnp.transpose(cache_values[0], (1, 0, 2))

    pieces = pl.pallas_call(
        project_kernel,
        out_shape=shaped((INNER, sent, HEAD)),
        in_specs=[VMEM] * 6,
        out_specs=VMEM,
        name="project",
    )(tokens[0], norm_gain[None], w_query, w_key, w_value, w_gate)
    pieces = pl.pallas_call(
        forward_kernel,
        out_shape=shaped((outer, sent, HEAD)),
        in_specs=[VMEM],
        out_specs=VMEM,
        name="forward",
    )(exchange(pieces, inner_groups))
    window = shaped((heads, WINDOW, HEAD))
    pieces, query, keys_next, values_next, keys_window, values_window = pl.pallas_call(
        attend_kernel,
        out_shape=(
            shaped((INNER, sent, HEAD)),
            shaped((rows, HEAD)),
            shaped(keys.shape),
            shaped(values.shape),
            window,
            window,
        ),
        in_specs=[SMEM, VMEM, VMEM, VMEM, VMEM],
        out_specs=(VMEM, VMEM, ANY, ANY, VMEM, VMEM),
        scratch_shapes=[pltpu.SemaphoreType.DMA((2,))],
        name="attend",
    )(scalars, exchange(pieces, outer_groups), bias, keys, values)
    pieces, fresh = pl.pallas_call(
        merge_kernel,
        out_shape=(shaped((outer, rows + PROPS, HEAD)), shaped((INNER * share, HEAD))),
        in_specs=[VMEM],
        out_specs=(VMEM, VMEM),
        name="merge",
    )(exchange(pieces, inner_groups))
    part_out, keys_next, values_next = pl.pallas_call(
        finish_kernel,
        out_shape=(
            shaped((PROPS, w_out.shape[1])),
            shaped(keys.shape),
            shaped(values.shape),
        ),
        in_specs=[SMEM, SMEM] + [VMEM] * 7 + [ANY, ANY],
        out_specs=(VMEM, ANY, ANY),
        input_output_aliases={9: 1, 10: 2},
        scratch_shapes=[
            pltpu.VMEM((PROPS, heads * HEAD), BF16),
            pltpu.VMEM((2, heads, WINDOW, HEAD), BF16),
            pltpu.SMEM((PROPS,), jnp.int32),
            pltpu.SemaphoreType.DMA((2,)),
        ],
        name="finish",
    )(
        scalars,
        parent[0],
        exchange(pieces, outer_groups),
        fresh,
        query,
        bias,
        w_out.T,
        keys_window,
        values_window,
        keys_next,
        values_next,
    )
    both = lax.all_gather(part_out, "tp").astype(F32)
    mixed = both.sum(0).astype(BF16)[None]
    return (
        mixed,
        jnp.transpose(keys_next, (1, 0, 2))[None],
        jnp.transpose(values_next, (1, 0, 2))[None],
    )


def solution(mesh):
    return jax.shard_map(
        local,
        mesh=mesh,
        in_specs=(
            P("dp", None, "kv"),
            P("kv"),
            P("kv", "tp"),
            P("kv", "tp"),
            P("kv", "tp"),
            P("kv", "tp"),
            P("tp", "kv"),
            P("tp"),
            P("dp", "kv", "tp", None),
            P("dp", "kv", "tp", None),
            P("dp"),
            P("dp"),
            P("dp", None),
        ),
        out_specs=(P("dp", None, "kv"), P("dp", "kv", "tp", None), P("dp", "kv", "tp", None)),
        check_vma=False,
    )
```

time: 136 us -> 80.5 us (0.59)
  waiting for transfers between devices: 63 us -> 6.3 us
  blocking collectives: 7.38 us -> 48.8 us
  starting transfers between devices: 33.9 us -> 7.28 us
  matrix products: 14 us -> 0 us
  Pallas kernels: 0 us -> 13.7 us
  local copies, waits for them, and re-layouts: 9.12 us -> 0.72 us
  other arithmetic: 5.85 us -> 1.18 us
    all_to_all x5 -> x1, waiting for transfers between devices: 63 us -> 6.3 us  [exchange(): lax.all_to_all(pieces, 'kv', 0, 0, axis_index_groups=groups, tiled=True)]
    all_to_all x0 -> x3, blocking collectives: none -> 40.5 us  [exchange(): lax.all_to_all(pieces, 'kv', 0, 0, axis_index_groups=groups, tiled=True)]
    all_to_all x5 -> x1, starting transfers between devices: 33.9 us -> 7.28 us  [exchange(): lax.all_to_all(pieces, 'kv', 0, 0, axis_index_groups=groups, tiled=True)]
    dot_general x18 -> x0, matrix products: 14 us -> none  [the longest x4 4.15 us: local(): jnp.dot(scaled, weight, preferred_element_type=jnp.float32)]
    pallas_call x0 -> x5, Pallas kernels: none -> 13.7 us  [the longest x1 4.6 us: local(): pl.pallas_call(attend_kernel, out_shape=(shaped((INNER, sent, HEAD)), sha...]
    reduce_sum x8 -> x1, other arithmetic: 3.87 us -> 0.6 us  [local(): mixed = both.sum(0).astype(BF16)[None]]
    reshape x3 -> x0, local copies, waits for them, and re-layouts: 3.26 us -> none  [the longest x1 1.92 us: laid_out(): return jnp.moveaxis(pieces, 0, dim).reshape(lengths)]
    unnamed x22 -> x4, local copies, waits for them, and re-layouts: 2.51 us -> 0.01 us
  transfers between devices with their start and end apart: 5 -> 1, of which waited for: 5 -> 1; matrix products, arithmetic and copies ran while one was open for 10% -> 1% of each run, Pallas kernels for 0% -> 0%
where the time goes in v2:
time: 80.5 us; the launch traced here: 79.9 us
  blocking collectives  48.8 us (61%)
  Pallas kernels  13.7 us (17%)
  starting transfers between devices  7.28 us (9%)
  waiting for transfers between devices  6.3 us (8%)
  between operations  1.98 us (2%)
  other arithmetic  1.18 us (1%)
    all_to_all x3, blocking collectives, exchange(): lax.all_to_all(pieces, 'kv', 0, 0, axis_index_groups=groups, tiled=True)  40.5 us
    all_gather x1, blocking collectives, local(): both = lax.all_gather(part_out, 'tp').astype(F32)  8.26 us
    all_to_all x1, starting transfers between devices, exchange(): lax.all_to_all(pieces, 'kv', 0, 0, axis_index_groups=groups, tiled=True)  7.28 us
    all_to_all x1, waiting for transfers between devices, exchange(): lax.all_to_all(pieces, 'kv', 0, 0, axis_index_groups=groups, tiled=True)  6.3 us
    pallas_call x1, Pallas kernels, local(): pl.pallas_call(attend_kernel, out_shape=(shaped((INNER, sent, HEAD)), sha...  4.6 us
    pallas_call x1, Pallas kernels, local(): pl.pallas_call(finish_kernel, out_shape=(shaped((PROPS, w_out.shape[1])),...  2.68 us
    pallas_call x1, Pallas kernels, local(): pl.pallas_call(project_kernel, out_shape=shaped((INNER, sent, HEAD)), in_...  2.29 us
    pallas_call x1, Pallas kernels, local(): pl.pallas_call(merge_kernel, out_shape=(shaped((outer, rows + PROPS, HEAD...  2.22 us
  transfers between devices with their start and end apart: 1, of which 1 were waited for; matrix products, arithmetic and copies ran while one was open for 1% of the time, Pallas kernels for 0%

profile of v2, /device:TPU:1, one launch (start us, length us, event | category | flops | bytes accessed | tf_op | source)
XLA Modules:
  0.0 79.9 jit_solution(11295509715349705350)
XLA Ops:
  0.6 2.3 %project.1 = bf16[8,288,128]{2,1,0:T(8,128)(2,1)} custom-call(bf16[16,64]{1,0:T(8,128)(2,1)} %bitcast.27, f32[1,64]{1,0:T(1,128)} %bitcast.29, bf16[64,1536]{1,0:T(8,128)(2,1)} %w_query.1, bf16[64,1536]{1,0:T(8,128)(2,1)} %w_key.1, bf16[64,1536]{1,0:T(8,128)(2,1)} %w_value.1, bf16[64,1536]{1,0:T(8,128)(2,1)} %w_gate.1), custom_call_target="tpu_custom_call" | custom-call | tf_op jit(solution)/shard_map/project/pallas_call | solution.py:358
  2.9 0.0 copy-start.1
  2.9 16.2 %all_to_all.20.arrived = bf16[8,288,128]{2,1,0:T(8,128)(2,1)} all-to-all(bf16[8,288,128]{2,1,0:T(8,128)(2,1)} %project.1), channel_id=1, replica_groups={{0,2,4,6,8,10,12,14},{16,18,20,22,24,26,28,30},{32,34,36,38,40,42,44,46..., dimensions={0} | all-to-all | bytes 1179648 | tf_op jit(solution)/shard_map/all_to_all | solution.py:29
  19.1 1.9 %forward.1 = bf16[4,288,128]{2,1,0:T(8,128)(2,1)} custom-call(bf16[8,288,128]{2,1,0:T(8,128)(2,1)} %all_to_all.20.arrived), custom_call_target="tpu_custom_call" | custom-call | tf_op jit(solution)/shard_map/forward/pallas_call | solution.py:365
  21.0 7.3 %all-to-all-start.1 = ((bf16[4,288,128]{2,1,0:T(8,128)(2,1)}), bf16[4,288,128]{2,1,0:T(8,128)(2,1)S(1)}, u32[]{:S(2)}, u32[]{:S(2)}) async-start(bf16[4,288,128]{2,1,0:T(8,128)(2,1)} %forward.1), calls=%async_computation.1 | async-start | bytes 589824 | tf_op jit(solution)/shard_map/all_to_all | solution.py:29
  29.6 0.6 pad_add_fusion.scalars
  30.2 6.3 %all-to-all-done.1.arrived = bf16[4,288,128]{2,1,0:T(8,128)(2,1)S(1)} async-done(((bf16[4,288,128]{2,1,0:T(8,128)(2,1)}), bf16[4,288,128]{2,1,0:T(8,128)(2,1)S(1)}, u32[]{:S(2)}, u32[]{:S(2)}) %all-to-all-start.1) | async-done | bytes 294944 | tf_op jit(solution)/shard_map/all_to_all | solution.py:29
  36.5 0.0 copy-start
  36.5 0.0 copy-done.1
  36.5 0.7 broadcast_in_dim.19.bias
  37.2 0.0 copy-done
  37.2 4.6 %attend.1 = (bf16[8,288,128]{2,1,0:T(8,128)(2,1)}, bf16[192,128]{1,0:T(8,128)(2,1)}, bf16[12,512,128]{2,1,0:T(8,128)(2,1)}, bf16[12,512,128]{2,1,0:T(8,128)(2,1)...) custom-call(s32[2]{0:T(128)} %pad_add_fusion.scalars, bf16[4,288,128]{2,1,0:T(8,128)(2,1)} %copy-done, ...), custom_call_target="tpu_custom_call" | custom-call | tf_op jit(solution)/shard_map/attend/pallas_call | solution.py:373
  41.9 12.2 %all_to_all.21.arrived = bf16[8,288,128]{2,1,0:T(8,128)(2,1)} all-to-all(bf16[8,288,128]{2,1,0:T(8,128)(2,1)} %get-tuple-element.14), channel_id=1, replica_groups={{0,2,4,6,8,10,12,14},{16,18,20,22,24,26,28,30},{32,34,36,38,40,42,44,46..., dimensions={0} | all-to-all | bytes 1179648 | tf_op jit(solution)/shard_map/all_to_all | solution.py:29
  54.1 2.2 %merge.1 = (bf16[4,208,128]{2,1,0:T(8,128)(2,1)}, bf16[640,128]{1,0:T(8,128)(2,1)}) custom-call(bf16[8,288,128]{2,1,0:T(8,128)(2,1)} %all_to_all.21.arrived), custom_call_target="tpu_custom_call" | custom-call | tf_op jit(solution)/shard_map/merge/pallas_call | solution.py:388
  56.3 12.1 %all_to_all.22.arrived = bf16[4,208,128]{2,1,0:T(8,128)(2,1)} all-to-all(bf16[4,208,128]{2,1,0:T(8,128)(2,1)} %get-tuple-element.15), channel_id=1, replica_groups={{0,16,32,48},{2,18,34,50},{4,20,36,52},{6,22,38,54},{8,24,40,56},{10,26..., dimensions={0} | all-to-all | bytes 425984 | tf_op jit(solution)/shard_map/all_to_all | solution.py:29
  68.4 2.7 %finish.1 = (bf16[16,64]{1,0:T(8,128)(2,1)}, bf16[12,512,128]{2,1,0:T(8,128)(2,1)}, bf16[12,512,128]{2,1,0:T(8,128)(2,1)}) custom-call(s32[2]{0:T(128)} %pad_add_fusion.scalars, s32[16]{0:T(128)} %bitcast.30, bf16[4,208,128]{2,1,0:T(8,128)(2,1)} %all_to_all.22.arrived, ...), custom_call_target="tpu_custom_call", output_to_operand_aliasing={{1}: (9, {}), {2}: (10, {})} | custom-call | tf_op jit(solution)/shard_map/finish/pallas_call | solution.py:395
  71.1 8.3 %all-gather = bf16[32,64]{1,0:T(8,128)(2,1)S(1)} all-gather(bf16[16,64]{1,0:T(8,128)(2,1)} %get-tuple-element.22), channel_id=2, replica_groups=mesh['dp'=4,'kv'=32,'tp'=2] {'tp'}, dimensions={0}, use_global_device_ids=true | all-gather | bytes 6144 | tf_op jit(solution)/shard_map/all_gather | solution.py:425
  79.3 0.6 reduce_sum.12
Async XLA Ops:
  2.9 33.6 %copy-start.1 = (f32[12]{0:T(128)S(1)}, f32[12]{0:T(128)}, u32[]{:S(2)}) copy-start(f32[12]{0:T(128)} %param.20) | copy-start | bytes 148
  21.0 15.5 %all-to-all-start.1 = ((bf16[4,288,128]{2,1,0:T(8,128)(2,1)}), bf16[4,288,128]{2,1,0:T(8,128)(2,1)S(1)}, u32[]{:S(2)}, u32[]{:S(2)}) async-start(bf16[4,288,128]{2,1,0:T(8,128)(2,1)} %forward.1), calls=%async_computation.1 | async-start | bytes 589824 | tf_op jit(solution)/shard_map/all_to_all | solution.py:29
  36.5 0.7 copy-start

commit v3 on v2

--- a/solution.py
+++ b/solution.py
@@ -16,6 +16,7 @@
 VMEM = pl.BlockSpec(memory_space=pltpu.VMEM)
 SMEM = pl.BlockSpec(memory_space=pltpu.SMEM)
 ANY = pl.BlockSpec(memory_space=pl.ANY)
+PARAMS = pltpu.CompilerParams(vmem_limit_bytes=16 * 2**20)
 
 
 def groups_of(count):
@@ -91,13 +92,49 @@
     return sums[:, :HEAD], sums[:, HEAD:]
 
 
-def project_kernel(tokens, gain, w_query, w_key, w_value, w_gate, out):
+def project_kernel(
+    prefix_len,
+    accepted,
+    tokens_far,
+    gain_far,
+    query_far,
+    key_far,
+    value_far,
+    gate_far,
+    out,
+    tokens,
+    gain,
+    w_query,
+    w_key,
+    w_value,
+    w_gate,
+    sems,
+):
+    del prefix_len, accepted
+    copies = [
+        pltpu.make_async_copy(source, target, sems.at[index])
+        for index, (source, target) in enumerate(
+            (
+                (tokens_far, tokens),
+                (gain_far, gain),
+                (query_far, w_query),
+                (key_far, w_key),
+                (value_far, w_value),
+                (gate_far, w_gate),
+            )
+        )
+    ]
+    for copy in copies:
+        copy.start()
     heads = w_query.shape[1] // HEAD
     rows = heads * PROPS
     share = out.shape[1] - rows - PROPS
+    copies[0].wait()
     flat = tokens[...].astype(F32)
     block = square_block(jnp.sum(flat * flat, axis=1, keepdims=True))
+    copies[1].wait()
     scaled = (flat * gain[...]).astype(BF16)
+    copies[2].wait()
     query = dot(scaled, w_query[...]).astype(BF16)
     for dest in range(INNER):
         for head in range(heads):
@@ -107,6 +144,7 @@
         out[dest, rows + share :, :] = block
     slots = share // PROPS
     for which, weight in enumerate((w_key, w_value, w_gate)):
+        copies[3 + which].wait()
         part = dot(scaled, weight[...]).astype(BF16)
         for head in range(heads):
             dest, slot = divmod(which * heads + head, slots)
@@ -138,9 +176,10 @@
 
 
 def attend_kernel(
-    scalars,
+    prefix_len,
+    accepted,
+    bias,
     arrived,
-    bias,
     keys,
     values,
     out,
@@ -159,8 +198,7 @@
     ]
     for copy in copies:
         copy.start()
-    offset = scalars[0]
-    first = pl.multiple_of(scalars[1], PROPS)
+    offset, first = window_of(prefix_len, accepted, ctx_dev)
     total = add_up(arrived)
     squares = jnp.sum(total[arrived.shape[1] - PROPS :], axis=1, keepdims=True)
     rscale = lax.rsqrt(squares / D + EPS)
@@ -177,7 +215,7 @@
         there = slice(head * PROPS, (head + 1) * PROPS)
         query = (total[there] * rscale).astype(BF16)
         query_out[there, :] = query
-        scores = dot_t(query, keys[head]) * factor + bias[head : head + 1, :]
+        scores = dot_t(query, keys[head]) * factor + bias[head]
         take, keep = log_sigmoids(scores)
         takes.append(take)
         keeps.append(jnp.where(live, keep, 0.0))
@@ -236,12 +274,13 @@
 
 
 def finish_kernel(
-    scalars,
+    prefix_len,
+    accepted,
+    bias,
     parent,
     arrived,
     fresh,
     query,
-    bias,
     w_out,
     keys_window,
     values_window,
@@ -259,8 +298,7 @@
     count = arrived.shape[0]
     rows = arrived.shape[1] - PROPS
     heads = rows // PROPS
-    offset = scalars[0]
-    first = pl.multiple_of(scalars[1], PROPS)
+    offset, first = window_of(prefix_len, accepted, keys_next.shape[1])
     source = first + iota((WINDOW, PROPS), 0) - offset
     picker = jnp.where(source == iota((WINDOW, PROPS), 1), 1.0, 0.0).astype(BF16)
     source = first + iota((WINDOW, HEAD), 0) - offset
@@ -291,7 +329,7 @@
     takes, keeps = [], []
     for head in range(heads):
         there = slice(head * PROPS, (head + 1) * PROPS)
-        scores = dot_t(query[there, :], fresh[there, :]) * factor + bias[head : head + 1, :PROPS]
+        scores = dot_t(query[there, :], fresh[there, :]) * factor + bias[head]
         take, keep = log_sigmoids(scores)
         takes.append(take)
         keeps.append(jnp.where(family, keep, 0.0))
@@ -325,6 +363,24 @@
     return jax.ShapeDtypeStruct(dims, dtype)
 
 
+def near(dims, dtype=BF16):
+    return pltpu.VMEM(dims, dtype)
+
+
+def held(value):
+    return pltpu.with_memory_space_constraint(value, pltpu.VMEM)
+
+
+def far(value):
+    return pltpu.with_memory_space_constraint(value, pltpu.HBM)
+
+
+def window_of(prefix_len, accepted, ctx_dev):
+    offset = prefix_len[0] + accepted[0] - lax.axis_index("kv") * ctx_dev
+    start = jnp.minimum(jnp.maximum(offset, 0), ctx_dev - WINDOW)
+    return offset, pl.multiple_of((start >> 4) << 4, PROPS)
+
+
 def local(
     tokens,
     norm_gain,
@@ -342,66 +398,85 @@
 ):
     inner_groups, outer_groups = groups_of(lax.axis_size("kv"))
     outer = len(outer_groups[0])
-    spot = lax.axis_index("kv")
-    heads = w_query.shape[1] // HEAD
-    ctx_dev = cache_keys.shape[1]
+    columns, width = w_query.shape
+    heads = width // HEAD
     rows = heads * PROPS
     share = -(-3 * heads // INNER) * PROPS
     sent = rows + share + PROPS
-    offset = (prefix_len + accepted)[0] - spot * ctx_dev
-    first = jnp.clip(offset // PROPS * PROPS, 0, ctx_dev - WINDOW)
-    scalars = jnp.stack([offset, first])
-    bias = jnp.broadcast_to(head_bias[:, None], (heads, ctx_dev))
     keys = jnp.transpose(cache_keys[0], (1, 0, 2))
     values = jnp.transpose(cache_values[0], (1, 0, 2))
 
     pieces = pl.pallas_call(
         project_kernel,
-        out_shape=shaped((INNER, sent, HEAD)),
-        in_specs=[VMEM] * 6,
+        out_shape=near((INNER, sent, HEAD)),
+        in_specs=[SMEM] * 2 + [ANY] * 6,
         out_specs=VMEM,
+        scratch_shapes=[
+            pltpu.VMEM(tokens.shape[1:], BF16),
+            pltpu.VMEM((1, columns), F32),
+            *[pltpu.VMEM(w_query.shape, BF16)] * 4,
+            pltpu.SemaphoreType.DMA((6,)),
+        ],
         name="project",
-    )(tokens[0], norm_gain[None], w_query, w_key, w_value, w_gate)
+        compiler_params=PARAMS,
+    )(
+        prefix_len,
+        accepted,
+        *(
+            far(value)
+            for value in (tokens[0], norm_gain[None], w_query, w_key, w_value, w_gate)
+        ),
+    )
     pieces = pl.pallas_call(
         forward_kernel,
-        out_shape=shaped((outer, sent, HEAD)),
+        out_shape=near((outer, sent, HEAD)),
         in_specs=[VMEM],
         out_specs=VMEM,
         name="forward",
-    )(exchange(pieces, inner_groups))
-    window = shaped((heads, WINDOW, HEAD))
+        compiler_params=PARAMS,
+    )(held(exchange(pieces, inner_groups)))
+    window = near((heads, WINDOW, HEAD))
     pieces, query, keys_next, values_next, keys_window, values_window = pl.pallas_call(
         attend_kernel,
         out_shape=(
-            shaped((INNER, sent, HEAD)),
-            shaped((rows, HEAD)),
+            near((INNER, sent, HEAD)),
+            near((rows, HEAD)),
             shaped(keys.shape),
             shaped(values.shape),
             window,
             window,
         ),
-        in_specs=[SMEM, VMEM, VMEM, VMEM, VMEM],
+        in_specs=[SMEM] * 3 + [VMEM] * 3,
         out_specs=(VMEM, VMEM, ANY, ANY, VMEM, VMEM),
         scratch_shapes=[pltpu.SemaphoreType.DMA((2,))],
         name="attend",
-    )(scalars, exchange(pieces, outer_groups), bias, keys, values)
+        compiler_params=PARAMS,
+    )(
+        prefix_len,
+        accepted,
+        head_bias,
+        held(exchange(pieces, outer_groups)),
+        held(keys),
+        held(values),
+    )
     pieces, fresh = pl.pallas_call(
         merge_kernel,
-        out_shape=(shaped((outer, rows + PROPS, HEAD)), shaped((INNER * share, HEAD))),
+        out_shape=(near((outer, rows + PROPS, HEAD)), near((INNER * share, HEAD))),
         in_specs=[VMEM],
         out_specs=(VMEM, VMEM),
         name="merge",
-    )(exchange(pieces, inner_groups))
+        compiler_params=PARAMS,
+    )(held(exchange(pieces, inner_groups)))
     part_out, keys_next, values_next = pl.pallas_call(
         finish_kernel,
         out_shape=(
-            shaped((PROPS, w_out.shape[1])),
+            near((PROPS, w_out.shape[1])),
             shaped(keys.shape),
             shaped(values.shape),
         ),
-        in_specs=[SMEM, SMEM] + [VMEM] * 7 + [ANY, ANY],
+        in_specs=[SMEM] * 4 + [VMEM] * 6 + [ANY, ANY],
         out_specs=(VMEM, ANY, ANY),
-        input_output_aliases={9: 1, 10: 2},
+        input_output_aliases={10: 1, 11: 2},
         scratch_shapes=[
             pltpu.VMEM((PROPS, heads * HEAD), BF16),
             pltpu.VMEM((2, heads, WINDOW, HEAD), BF16),
@@ -409,16 +484,18 @@
             pltpu.SemaphoreType.DMA((2,)),
         ],
         name="finish",
+        compiler_params=PARAMS,
     )(
-        scalars,
+        prefix_len,
+        accepted,
+        head_bias,
         parent[0],
-        exchange(pieces, outer_groups),
-        fresh,
-        query,
-        bias,
-        w_out.T,
-        keys_window,
-        values_window,
+        held(exchange(pieces, outer_groups)),
+        held(fresh),
+        held(query),
+        held(w_out.T),
+        held(keys_window),
+        held(values_window),
         keys_next,
         values_next,
     )

time: 80.5 us -> 70.6 us (0.88)
  blocking collectives: 48.8 us -> 61.7 us
  Pallas kernels: 13.7 us -> 6 us
  starting transfers between devices: 7.28 us -> 0 us
  waiting for transfers between devices: 6.3 us -> 0 us
    all_to_all x3 -> x4, blocking collectives: 40.5 us -> 54.8 us  [exchange(): lax.all_to_all(pieces, 'kv', 0, 0, axis_index_groups=groups, tiled=True)]
    pallas_call x5, Pallas kernels: 13.7 us -> 6 us  [the longest x1 2.24 us: local(): pl.pallas_call(attend_kernel, out_shape=(near((INNER, sent, HEAD)), near(...]
    all_to_all x1 -> x0, starting transfers between devices: 7.28 us -> none  [exchange(): lax.all_to_all(pieces, 'kv', 0, 0, axis_index_groups=groups, tiled=True)]
    all_to_all x1 -> x0, waiting for transfers between devices: 6.3 us -> none  [exchange(): lax.all_to_all(pieces, 'kv', 0, 0, axis_index_groups=groups, tiled=True)]
    all_gather x1, blocking collectives: 8.26 us -> 6.89 us  [local(): both = lax.all_gather(part_out, 'tp').astype(F32)]
  transfers between devices with their start and end apart: 1 -> 0, of which waited for: 1 -> 0; matrix products, arithmetic and copies ran while one was open for 1% -> 0% of each run, Pallas kernels for 0% -> 0%
where the time goes in v3:
time: 70.6 us; the launch traced here: 70.3 us
  blocking collectives  61.7 us (87%)
  Pallas kernels  6 us (8%)
  between operations  2 us (3%)
    all_to_all x4, blocking collectives, exchange(): lax.all_to_all(pieces, 'kv', 0, 0, axis_index_groups=groups, tiled=True)  54.8 us
    all_gather x1, blocking collectives, local(): both = lax.all_gather(part_out, 'tp').astype(F32)  6.89 us
    pallas_call x1, Pallas kernels, local(): pl.pallas_call(attend_kernel, out_shape=(near((INNER, sent, HEAD)), near(...  2.24 us
    pallas_call x1, Pallas kernels, local(): pl.pallas_call(project_kernel, out_shape=near((INNER, sent, HEAD)), in_sp...  1.74 us
    pallas_call x1, Pallas kernels, local(): pl.pallas_call(finish_kernel, out_shape=(near((PROPS, w_out.shape[1])), s...  1.46 us

profile of v3, /device:TPU:1, one launch (start us, length us, event | category | flops | bytes accessed | tf_op | source)
XLA Modules:
  0.0 70.3 jit_solution(7546062095874690198)
XLA Ops:
  1.9 0.0 copy-start.1
  1.9 1.7 %project.1 = bf16[8,288,128]{2,1,0:T(8,128)(2,1)S(1)} custom-call(s32[1]{0:T(128)S(6)} %copy.20.prefix_len, s32[1]{0:T(128)S(6)} %copy.21.accepted, bf16[16,64]{1,0:T(8,128)(2,1)} %bitcast.25, f32[1,64]{1,0:T(1,128)} %bitcast.27, bf16[64,1536]{1,0:T(8,128)(2,1)} %query_far.1, bf16[64,1536]{1,0:T(8,128)(2,1)} %key_far.1, bf16[64,1536]{1,0:T(8,128)(2,1)} %value_far.1, ...), custom_call_target="tpu_custom_call" | custom-call | tf_op jit(solution)/shard_map/project/pallas_call | solution.py:409
  3.7 0.0 copy-start
  3.7 0.0 copy-start.3
  3.7 15.9 %all_to_all.20.arrived = bf16[8,288,128]{2,1,0:T(8,128)(2,1)S(1)} all-to-all(bf16[8,288,128]{2,1,0:T(8,128)(2,1)S(1)} %project.1), channel_id=1, replica_groups={{0,2,4,6,8,10,12,14},{16,18,20,22,24,26,28,30},{32,34,36,38,40,42,44,46..., dimensions={0} | all-to-all | bytes 1179648 | tf_op jit(solution)/shard_map/all_to_all | solution.py:30
  19.6 0.1 forward.1
  19.7 15.6 %all_to_all.21.arrived = bf16[4,288,128]{2,1,0:T(8,128)(2,1)S(1)} all-to-all(bf16[4,288,128]{2,1,0:T(8,128)(2,1)S(1)} %forward.1), channel_id=1, replica_groups={{0,16,32,48},{2,18,34,50},{4,20,36,52},{6,22,38,54},{8,24,40,56},{10,26..., dimensions={0} | all-to-all | bytes 589824 | tf_op jit(solution)/shard_map/all_to_all | solution.py:30
  35.3 0.0 copy-done.1
  35.3 0.0 copy-done
  35.3 0.0 copy-done.3
  35.3 2.2 %attend.1 = (bf16[8,288,128]{2,1,0:T(8,128)(2,1)S(1)}, bf16[192,128]{1,0:T(8,128)(2,1)S(1)}, bf16[12,512,128]{2,1,0:T(8,128)(2,1)}, bf16[12,512,128]{2,1,0:T(8,1...) custom-call(s32[1]{0:T(128)S(6)} %copy.20.prefix_len, s32[1]{0:T(128)S(6)} %copy.21.accepted, ...), custom_call_target="tpu_custom_call" | custom-call | tf_op jit(solution)/shard_map/attend/pallas_call | solution.py:439
  37.6 0.0 copy-start.2
  37.6 0.0 copy-start.4
  37.6 11.4 %all_to_all.22.arrived = bf16[8,288,128]{2,1,0:T(8,128)(2,1)S(1)} all-to-all(bf16[8,288,128]{2,1,0:T(8,128)(2,1)S(1)} %get-tuple-element.14), channel_id=1, replica_groups={{0,2,4,6,8,10,12,14},{16,18,20,22,24,26,28,30},{32,34,36,38,40,42,44,46..., dimensions={0} | all-to-all | bytes 1179648 | tf_op jit(solution)/shard_map/all_to_all | solution.py:30
  49.0 0.5 merge.1
  49.4 11.9 %all_to_all.23.arrived = bf16[4,208,128]{2,1,0:T(8,128)(2,1)S(1)} all-to-all(bf16[4,208,128]{2,1,0:T(8,128)(2,1)S(1)} %get-tuple-element.15), channel_id=1, replica_groups={{0,16,32,48},{2,18,34,50},{4,20,36,52},{6,22,38,54},{8,24,40,56},{10,26..., dimensions={0} | all-to-all | bytes 425984 | tf_op jit(solution)/shard_map/all_to_all | solution.py:30
  61.3 0.0 copy-done.2
  61.4 0.0 copy-done.4
  61.4 1.5 %finish.1 = (bf16[16,64]{1,0:T(8,128)(2,1)S(1)}, bf16[12,512,128]{2,1,0:T(8,128)(2,1)}, bf16[12,512,128]{2,1,0:T(8,128)(2,1)}) custom-call(s32[1]{0:T(128)S(6)} %copy.20.prefix_len, s32[1]{0:T(128)S(6)} %copy.21.accepted, f32[12]{0:T(128)S(1)} %copy-done.3, s32[16]{0:T(128)S(1)} %bitcast.21, ...), custom_call_target="tpu_custom_call", output_to_operand_aliasing={{1}: (10, {}), {2}: (11, {})} | custom-call | tf_op jit(solution)/shard_map/finish/pallas_call | solution.py:470
  62.8 6.9 %all-gather = bf16[32,64]{1,0:T(8,128)(2,1)S(1)} all-gather(bf16[16,64]{1,0:T(8,128)(2,1)S(1)} %get-tuple-element.22), channel_id=2, replica_groups=mesh['dp'=4,'kv'=32,'tp'=2] {'tp'}, dimensions={0}, use_global_device_ids=true | all-gather | bytes 6144 | tf_op jit(solution)/shard_map/all_gather | solution.py:502
  69.7 0.6 reduce_sum.12
Async XLA Ops:
  1.9 33.4 %copy-start.1 = (bf16[1,512,12,128]{3,1,2,0:T(8,128)(2,1)S(1)}, bf16[1,512,12,128]{3,1,2,0:T(8,128)(2,1)}, u32[]{:S(2)}) copy-start(bf16[1,512,12,128]{3,1,2,0:T(8,128)(2,1)} %param.22) | copy-start | bytes 4718596
  3.7 31.7 %copy-start = (bf16[1,512,12,128]{3,1,2,0:T(8,128)(2,1)S(1)}, bf16[1,512,12,128]{3,1,2,0:T(8,128)(2,1)}, u32[]{:S(2)}) copy-start(bf16[1,512,12,128]{3,1,2,0:T(8,128)(2,1)} %param.21) | copy-start | bytes 4718596
  3.7 31.6 %copy-start.3 = (f32[12]{0:T(128)S(1)}, f32[12]{0:T(128)}, u32[]{:S(2)}) copy-start(f32[12]{0:T(128)} %bias.3) | copy-start | bytes 148
  37.6 23.8 %copy-start.2 = (bf16[1536,64]{0,1:T(8,128)(2,1)S(1)}, bf16[1536,64]{0,1:T(8,128)(2,1)}, u32[]{:S(2)}) copy-start(bf16[1536,64]{0,1:T(8,128)(2,1)} %param.19) | copy-start | bytes 589828
  37.6 23.8 %copy-start.4 = (s32[1,16]{1,0:T(1,128)S(1)}, s32[1,16]{1,0:T(1,128)}, u32[]{:S(2)}) copy-start(s32[1,16]{1,0:T(1,128)} %param.25) | copy-start | bytes 196

commit v4 on v3

--- a/solution.py
+++ b/solution.py
@@ -11,6 +11,7 @@
 INNER = 8
 PROPS = 16
 WINDOW = 32
+STEPS = (2, 1, 3)
 F32 = jnp.float32
 BF16 = jnp.bfloat16
 VMEM = pl.BlockSpec(memory_space=pltpu.VMEM)
@@ -19,15 +20,19 @@
 PARAMS = pltpu.CompilerParams(vmem_limit_bytes=16 * 2**20)
 
 
-def groups_of(count):
-    outer = count // INNER
-    inner_groups = [[a * INNER + i for i in range(INNER)] for a in range(outer)]
-    outer_groups = [[a * INNER + i for a in range(outer)] for i in range(INNER)]
-    return inner_groups, outer_groups
-
-
-def exchange(pieces, groups):
-    return lax.all_to_all(pieces, "kv", 0, 0, axis_index_groups=groups, tiled=True)
+def exchange(pieces):
+    outer = lax.axis_size("kv") // INNER
+    groups = [[a * INNER + i for i in range(INNER)] for a in range(outer)]
+    return held(lax.all_to_all(pieces, "kv", 0, 0, axis_index_groups=groups, tiled=True))
+
+
+def shifted(value):
+    count = lax.axis_size("kv")
+    parts = [value]
+    for step in STEPS:
+        pairs = [(spot, (spot + step * INNER) % count) for spot in range(count)]
+        parts.append(lax.ppermute(value, "kv", pairs))
+    return [held(part) for part in parts]
 
 
 def iota(shape, dim):
@@ -158,28 +163,28 @@
         )
 
 
-def add_up(arrived):
-    total = arrived[0].astype(F32)
-    for index in range(1, arrived.shape[0]):
-        total = total + arrived[index].astype(F32)
+def add_up(parts):
+    total = parts[0].astype(F32)
+    for part in parts[1:]:
+        total = total + part.astype(F32)
     return total
 
 
 def forward_kernel(arrived, out):
     count = arrived.shape[1] - PROPS
-    total = add_up(arrived)
-    sums = total[:count].astype(BF16)
-    block = square_block(jnp.sum(total[count:], axis=1, keepdims=True))
-    for dest in range(out.shape[0]):
-        out[dest, :count, :] = sums
-        out[dest, count:, :] = block
+    total = add_up([arrived[source] for source in range(INNER)])
+    out[:count, :] = total[:count].astype(BF16)
+    out[count:, :] = square_block(jnp.sum(total[count:], axis=1, keepdims=True))
 
 
 def attend_kernel(
     prefix_len,
     accepted,
     bias,
-    arrived,
+    own,
+    first_part,
+    second_part,
+    third_part,
     keys,
     values,
     out,
@@ -199,10 +204,10 @@
     for copy in copies:
         copy.start()
     offset, first = window_of(prefix_len, accepted, ctx_dev)
-    total = add_up(arrived)
-    squares = jnp.sum(total[arrived.shape[1] - PROPS :], axis=1, keepdims=True)
+    total = add_up([own[...], first_part[...], second_part[...], third_part[...]])
+    squares = jnp.sum(total[own.shape[0] - PROPS :], axis=1, keepdims=True)
     rscale = lax.rsqrt(squares / D + EPS)
-    share = arrived.shape[1] - PROPS - rows
+    share = own.shape[0] - PROPS - rows
     for slot in range(share // PROPS):
         there = slice(rows + slot * PROPS, rows + (slot + 1) * PROPS)
         piece = (total[there] * rscale).astype(BF16)
@@ -247,7 +252,7 @@
 
 def merge_kernel(arrived, out, fresh):
     count = arrived.shape[0]
-    rows = out.shape[1] - PROPS
+    rows = out.shape[0] - PROPS
     heads = rows // PROPS
     share = arrived.shape[1] - PROPS - rows
     for source in range(count):
@@ -265,40 +270,33 @@
             total = total + factors[source][:, head : head + 1] * arrived[
                 source, there, :
             ].astype(F32)
-        total = total.astype(BF16)
-        for dest in range(out.shape[0]):
-            out[dest, there, :] = total
-    block = rest_block([beyond[:, head : head + 1] for head in range(heads)])
-    for dest in range(out.shape[0]):
-        out[dest, rows:, :] = block
-
-
-def finish_kernel(
+        out[there, :] = total.astype(BF16)
+    out[rows:, :] = rest_block([beyond[:, head : head + 1] for head in range(heads)])
+
+
+def tree_kernel(
     prefix_len,
     accepted,
     bias,
     parent,
-    arrived,
     fresh,
     query,
-    w_out,
     keys_window,
     values_window,
     keys_old,
     values_old,
-    out,
+    tree_out,
+    tail_out,
+    gate_out,
     keys_next,
     values_next,
-    mixin,
     patches,
     masks,
     sems,
 ):
     del keys_old, values_old
-    count = arrived.shape[0]
-    rows = arrived.shape[1] - PROPS
-    heads = rows // PROPS
-    offset, first = window_of(prefix_len, accepted, keys_next.shape[1])
+    heads, ctx_dev, _ = keys_next.shape
+    offset, first = window_of(prefix_len, accepted, ctx_dev)
     source = first + iota((WINDOW, PROPS), 0) - offset
     picker = jnp.where(source == iota((WINDOW, PROPS), 1), 1.0, 0.0).astype(BF16)
     source = first + iota((WINDOW, HEAD), 0) - offset
@@ -307,13 +305,14 @@
     for which, (window, target) in enumerate(
         ((keys_window, keys_next), (values_window, values_next))
     ):
-        patched = patches.at[which]
         for head in range(heads):
             start = (which * heads + head) * PROPS
             placed = dot(picker, fresh[start : start + PROPS, :])
             patches[which, head] = jnp.where(inside, placed, window[head].astype(F32)).astype(BF16)
         copies.append(
-            pltpu.make_async_copy(patched, target.at[:, pl.ds(first, WINDOW), :], sems.at[which])
+            pltpu.make_async_copy(
+                patches.at[which], target.at[:, pl.ds(first, WINDOW), :], sems.at[which]
+            )
         )
         copies[-1].start()
     row = iota((PROPS, PROPS), 0)
@@ -334,29 +333,41 @@
         takes.append(take)
         keeps.append(jnp.where(family, keep, 0.0))
     later, tail = after_and_all(jnp.concatenate(keeps, axis=0), after_table(PROPS))
-    beyond = jnp.zeros((PROPS, HEAD), F32)
-    beyonds = []
-    for index in reversed(range(count)):
-        beyonds.append(beyond)
-        beyond = beyond + rest_sums(arrived[index, rows:, :])
-    beyonds = beyonds[::-1]
+    tail_out[...] = tail
     for head in range(heads):
         there = slice(head * PROPS, (head + 1) * PROPS)
         weight = jnp.where(family, jnp.exp(takes[head] + later[there, :PROPS]), 0.0).astype(BF16)
         start = (heads + head) * PROPS
-        total = dot(weight, fresh[start : start + PROPS, :])
-        for index in range(count):
-            total = total + jnp.exp(beyonds[index][:, head : head + 1] + tail[there]) * arrived[
-                index, there, :
-            ].astype(F32)
-        start = (2 * heads + head) * PROPS
-        gate = fresh[start : start + PROPS, :].astype(F32)
-        mixin[:, head * HEAD : (head + 1) * HEAD] = (total * (gate * jax.nn.sigmoid(gate))).astype(
-            BF16
-        )
-    out[...] = dot_t(mixin[...], w_out[...]).astype(BF16)
+        tree_out[there, :] = dot(weight, fresh[start : start + PROPS, :])
+    gate = fresh[2 * heads * PROPS : 3 * heads * PROPS, :].astype(F32)
+    gate_out[...] = gate * jax.nn.sigmoid(gate)
     for copy in copies:
         copy.wait()
+
+
+def finish_kernel(tree, tail, gate, w_out, own, first_part, second_part, third_part, out, mixin):
+    parts = (own, first_part, second_part, third_part)
+    outer = len(parts)
+    rows = own.shape[0] - PROPS
+    heads = rows // PROPS
+    place = lax.axis_index("kv") // INNER
+    spots = [lax.rem(place + outer - step, outer) for step in (0, *STEPS)]
+    rests = [rest_sums(part[rows:, :]) for part in parts]
+    beyonds = []
+    for spot in spots:
+        beyond = jnp.zeros((PROPS, HEAD), F32)
+        for other, rest in zip(spots, rests):
+            beyond = beyond + jnp.where(other > spot, rest, 0.0)
+        beyonds.append(beyond)
+    for head in range(heads):
+        there = slice(head * PROPS, (head + 1) * PROPS)
+        total = tree[there, :]
+        for part, beyond in zip(parts, beyonds):
+            total = total + jnp.exp(beyond[:, head : head + 1] + tail[there, :]) * part[
+                there, :
+            ].astype(F32)
+        mixin[:, head * HEAD : (head + 1) * HEAD] = (total * gate[there, :]).astype(BF16)
+    out[...] = dot_t(mixin[...], w_out[...]).astype(BF16)
 
 
 def shaped(dims, dtype=BF16):
@@ -396,8 +407,6 @@
     accepted,
     parent,
 ):
-    inner_groups, outer_groups = groups_of(lax.axis_size("kv"))
-    outer = len(outer_groups[0])
     columns, width = w_query.shape
     heads = width // HEAD
     rows = heads * PROPS
@@ -429,12 +438,12 @@
     )
     pieces = pl.pallas_call(
         forward_kernel,
-        out_shape=near((outer, sent, HEAD)),
+        out_shape=near((sent, HEAD)),
         in_specs=[VMEM],
         out_specs=VMEM,
         name="forward",
         compiler_params=PARAMS,
-    )(held(exchange(pieces, inner_groups)))
+    )(exchange(pieces))
     window = near((heads, WINDOW, HEAD))
     pieces, query, keys_next, values_next, keys_window, values_window = pl.pallas_call(
         attend_kernel,
@@ -446,7 +455,7 @@
             window,
             window,
         ),
-        in_specs=[SMEM] * 3 + [VMEM] * 3,
+        in_specs=[SMEM] * 3 + [VMEM] * 6,
         out_specs=(VMEM, VMEM, ANY, ANY, VMEM, VMEM),
         scratch_shapes=[pltpu.SemaphoreType.DMA((2,))],
         name="attend",
@@ -455,52 +464,59 @@
         prefix_len,
         accepted,
         head_bias,
-        held(exchange(pieces, outer_groups)),
+        *shifted(pieces),
         held(keys),
         held(values),
     )
     pieces, fresh = pl.pallas_call(
         merge_kernel,
-        out_shape=(near((outer, rows + PROPS, HEAD)), near((INNER * share, HEAD))),
+        out_shape=(near((rows + PROPS, HEAD)), near((INNER * share, HEAD))),
         in_specs=[VMEM],
         out_specs=(VMEM, VMEM),
         name="merge",
         compiler_params=PARAMS,
-    )(held(exchange(pieces, inner_groups)))
-    part_out, keys_next, values_next = pl.pallas_call(
-        finish_kernel,
+    )(exchange(pieces))
+    parts = shifted(pieces)
+    tree, tail, gate, keys_next, values_next = pl.pallas_call(
+        tree_kernel,
         out_shape=(
-            near((PROPS, w_out.shape[1])),
+            *[near((rows, HEAD), F32)] * 3,
             shaped(keys.shape),
             shaped(values.shape),
         ),
-        in_specs=[SMEM] * 4 + [VMEM] * 6 + [ANY, ANY],
-        out_specs=(VMEM, ANY, ANY),
-        input_output_aliases={10: 1, 11: 2},
+        in_specs=[SMEM] * 4 + [VMEM] * 4 + [ANY, ANY],
+        out_specs=(VMEM, VMEM, VMEM, ANY, ANY),
+        input_output_aliases={8: 3, 9: 4},
         scratch_shapes=[
-            pltpu.VMEM((PROPS, heads * HEAD), BF16),
             pltpu.VMEM((2, heads, WINDOW, HEAD), BF16),
             pltpu.SMEM((PROPS,), jnp.int32),
             pltpu.SemaphoreType.DMA((2,)),
         ],
-        name="finish",
+        name="tree",
         compiler_params=PARAMS,
     )(
         prefix_len,
         accepted,
         head_bias,
         parent[0],
-        held(exchange(pieces, outer_groups)),
         held(fresh),
         held(query),
-        held(w_out.T),
         held(keys_window),
         held(values_window),
         keys_next,
         values_next,
     )
-    both = lax.all_gather(part_out, "tp").astype(F32)
-    mixed = both.sum(0).astype(BF16)[None]
+    part_out = pl.pallas_call(
+        finish_kernel,
+        out_shape=near((PROPS, w_out.shape[1])),
+        in_specs=[VMEM] * 8,
+        out_specs=VMEM,
+        scratch_shapes=[pltpu.VMEM((PROPS, heads * HEAD), BF16)],
+        name="finish",
+        compiler_params=PARAMS,
+    )(held(tree), held(tail), held(gate), held(w_out.T), *parts)
+    other = lax.ppermute(part_out, "tp", [(0, 1), (1, 0)])
+    mixed = (part_out.astype(F32) + other.astype(F32)).astype(BF16)[None]
     return (
         mixed,
         jnp.transpose(keys_next, (1, 0, 2))[None],

time: 70.6 us -> 65.7 us (0.931)
  blocking collectives: 61.7 us -> 27.8 us
  starting transfers between devices: 0 us -> 21.1 us
  waiting for transfers between devices: 0 us -> 7.53 us
    all_to_all x4 -> x2, blocking collectives: 54.8 us -> 27.8 us  [exchange(): lax.all_to_all(pieces, 'kv', 0, 0, axis_index_groups=groups, tiled=True)]
    ppermute x0 -> x7, starting transfers between devices: none -> 21.1 us  [the longest x6 14.2 us: shifted(): parts.append(lax.ppermute(value, 'kv', pairs))]
    ppermute x0 -> x7, waiting for transfers between devices: none -> 7.53 us  [the longest x6 6.71 us: shifted(): parts.append(lax.ppermute(value, 'kv', pairs))]
    all_gather x1 -> x0, blocking collectives: 6.89 us -> none  [local(): both = lax.all_gather(part_out, 'tp').astype(F32)]
    pallas_call x3 -> x4, Pallas kernels: 2.02 us -> 2.4 us  [the longest x1 1.4 us: local(): pl.pallas_call(tree_kernel, out_shape=(*[near((rows, HEAD), F32)] * 3, sh...]
  transfers between devices with their start and end apart: 0 -> 7, of which waited for: 0 -> 5; matrix products, arithmetic and copies ran while one was open for 0% -> 0% of each run, Pallas kernels for 0% -> 2%
where the time goes in v4:
time: 65.7 us; the launch traced here: 65.5 us
  blocking collectives  27.8 us (42%)
  starting transfers between devices  21.1 us (32%)
  waiting for transfers between devices  7.53 us (11%)
  Pallas kernels  6.53 us (10%)
  between operations  2.01 us (3%)
    all_to_all x2, blocking collectives, exchange(): lax.all_to_all(pieces, 'kv', 0, 0, axis_index_groups=groups, tiled=True)  27.8 us
    ppermute x6, starting transfers between devices, shifted(): parts.append(lax.ppermute(value, 'kv', pairs))  14.2 us
    ppermute x1, starting transfers between devices, local(): other = lax.ppermute(part_out, 'tp', [(0, 1), (1, 0)])  6.86 us
    ppermute x6, waiting for transfers between devices, shifted(): parts.append(lax.ppermute(value, 'kv', pairs))  6.71 us
    pallas_call x1, Pallas kernels, local(): pl.pallas_call(attend_kernel, out_shape=(near((INNER, sent, HEAD)), near(...  2.36 us
    pallas_call x1, Pallas kernels, local(): pl.pallas_call(project_kernel, out_shape=near((INNER, sent, HEAD)), in_sp...  1.77 us
    pallas_call x1, Pallas kernels, local(): pl.pallas_call(tree_kernel, out_shape=(*[near((rows, HEAD), F32)] * 3, sh...  1.4 us
  transfers between devices with their start and end apart: 7, of which 5 were waited for; matrix products, arithmetic and copies ran while one was open for 0% of the time, Pallas kernels for 2%

profile of v4, /device:TPU:1, one launch (start us, length us, event | category | flops | bytes accessed | tf_op | source)
XLA Modules:
  0.0 65.5 jit_solution(10144268809254245588)
XLA Ops:
  2.0 1.8 %project.1 = bf16[8,288,128]{2,1,0:T(8,128)(2,1)S(1)} custom-call(s32[1]{0:T(128)S(6)} %copy.20.prefix_len, s32[1]{0:T(128)S(6)} %copy.21.accepted, bf16[16,64]{1,0:T(8,128)(2,1)} %bitcast.24, f32[1,64]{1,0:T(1,128)} %bitcast.25, bf16[64,1536]{1,0:T(8,128)(2,1)} %query_far.1, bf16[64,1536]{1,0:T(8,128)(2,1)} %key_far.1, bf16[64,1536]{1,0:T(8,128)(2,1)} %value_far.1, ...), custom_call_target="tpu_custom_call" | custom-call | tf_op jit(solution)/shard_map/project/pallas_call | solution.py:418
  3.7 15.8 %all_to_all.10.arrived = bf16[8,288,128]{2,1,0:T(8,128)(2,1)S(1)} all-to-all(bf16[8,288,128]{2,1,0:T(8,128)(2,1)S(1)} %project.1), channel_id=1, replica_groups={{0,2,4,6,8,10,12,14},{16,18,20,22,24,26,28,30},{32,34,36,38,40,42,44,46..., dimensions={0} | all-to-all | bytes 1179648 | tf_op jit(solution)/shard_map/all_to_all | solution.py:26
  19.5 0.1 forward.1.own
  19.6 5.2 %collective-permute-start.2 = (bf16[288,128]{1,0:T(8,128)(2,1)S(1)}, bf16[288,128]{1,0:T(8,128)(2,1)S(1)}, u32[]{:S(2)}, u32[]{:S(2)}) collective-permute-start(bf16[288,128]{1,0:T(8,128)(2,1)S(1)} %forward.1.own), channel_id=1, source_target_pairs={{0,48},{2,50},{4,52},{6,54},{8,56},{10,58},{12,60},{14,62},{16,0},... | collective-permute-start | bytes 221192 | tf_op jit(solution)/shard_map/ppermute | solution.py:34
  24.8 0.0 collective-permute-start.1
  24.8 3.3 %collective-permute-start = (bf16[288,128]{1,0:T(8,128)(2,1)S(1)}, bf16[288,128]{1,0:T(8,128)(2,1)S(1)}, u32[]{:S(2)}, u32[]{:S(2)}) collective-permute-start(bf16[288,128]{1,0:T(8,128)(2,1)S(1)} %forward.1.own), channel_id=1, source_target_pairs={{0,32},{2,34},{4,36},{6,38},{8,40},{10,42},{12,44},{14,46},{16,48}... | collective-permute-start | bytes 221192 | tf_op jit(solution)/shard_map/ppermute | solution.py:34
  28.1 0.0 collective-permute-done.2.third_part
  28.1 2.1 %collective-permute-done.1.second_part = bf16[288,128]{1,0:T(8,128)(2,1)S(1)} collective-permute-done((bf16[288,128]{1,0:T(8,128)(2,1)S(1)}, bf16[288,128]{1,0:T(8,128)(2,1)S(1)}, u32[]{:S(2)}, u32[]{:S(2)}) %collective-permute-start.1) | collective-permute-done | bytes 73760 | tf_op jit(solution)/shard_map/ppermute | solution.py:34
  30.2 1.9 %collective-permute-done.first_part = bf16[288,128]{1,0:T(8,128)(2,1)S(1)} collective-permute-done((bf16[288,128]{1,0:T(8,128)(2,1)S(1)}, bf16[288,128]{1,0:T(8,128)(2,1)S(1)}, u32[]{:S(2)}, u32[]{:S(2)}) %collective-permute-start) | collective-permute-done | bytes 73760 | tf_op jit(solution)/shard_map/ppermute | solution.py:34
  32.1 2.4 %attend.1 = (bf16[8,288,128]{2,1,0:T(8,128)(2,1)S(1)}, bf16[192,128]{1,0:T(8,128)(2,1)S(1)}, bf16[12,512,128]{2,1,0:T(8,128)(2,1)}, bf16[12,512,128]{2,1,0:T(8,1...) custom-call(s32[1]{0:T(128)S(6)} %copy.20.prefix_len, s32[1]{0:T(128)S(6)} %copy.21.accepted, ...), custom_call_target="tpu_custom_call" | custom-call | tf_op jit(solution)/shard_map/attend/pallas_call | solution.py:448
  34.5 0.0 copy-start.4
  34.5 12.0 %all_to_all.11.arrived = bf16[8,288,128]{2,1,0:T(8,128)(2,1)S(1)} all-to-all(bf16[8,288,128]{2,1,0:T(8,128)(2,1)S(1)} %get-tuple-element.16), channel_id=1, replica_groups={{0,2,4,6,8,10,12,14},{16,18,20,22,24,26,28,30},{32,34,36,38,40,42,44,46..., dimensions={0} | all-to-all | bytes 1179648 | tf_op jit(solution)/shard_map/all_to_all | solution.py:26
  46.5 0.5 merge.1
  46.9 2.9 %collective-permute-start.5 = (bf16[208,128]{1,0:T(8,128)(2,1)S(1)}, bf16[208,128]{1,0:T(8,128)(2,1)S(1)}, u32[]{:S(2)}, u32[]{:S(2)}) collective-permute-start(bf16[208,128]{1,0:T(8,128)(2,1)S(1)} %get-tuple-element.26.own), channel_id=1, source_target_pairs={{0,48},{2,50},{4,52},{6,54},{8,56},{10,58},{12,60},{14,62},{16,0},... | collective-permute-start | bytes 159752 | tf_op jit(solution)/shard_map/ppermute | solution.py:34
  49.8 0.0 collective-permute-start.4
  49.8 2.8 %collective-permute-start.3 = (bf16[208,128]{1,0:T(8,128)(2,1)S(1)}, bf16[208,128]{1,0:T(8,128)(2,1)S(1)}, u32[]{:S(2)}, u32[]{:S(2)}) collective-permute-start(bf16[208,128]{1,0:T(8,128)(2,1)S(1)} %get-tuple-element.26.own), channel_id=1, source_target_pairs={{0,32},{2,34},{4,36},{6,38},{8,40},{10,42},{12,44},{14,46},{16,48}... | collective-permute-start | bytes 159752 | tf_op jit(solution)/shard_map/ppermute | solution.py:34
  52.7 1.4 %tree.1 = (f32[192,128]{1,0:T(8,128)S(1)}, f32[192,128]{1,0:T(8,128)S(1)}, f32[192,128]{1,0:T(8,128)S(1)}, bf16[12,512,128]{2,1,0:T(8,128)(2,1)}, bf16[12,512,128]{2,1,0:T(8,128)(2,1)}) custom-call(s32[1]{0:T(128)S(6)} %copy.20.prefix_len, s32[1]{0:T(128)S(6)} %copy.21.accepted, f32[12]{0:T(128)S(1)} %copy-done.3, ...), custom_call_target="tpu_custom_call", output_to_operand_aliasing={{3}: (8, {}), {4}: (9, {})} | custom-call | tf_op jit(solution)/shard_map/tree/pallas_call | solution.py:480
  54.1 0.0 collective-permute-done.5.third_part
  54.1 0.8 %collective-permute-done.4.second_part = bf16[208,128]{1,0:T(8,128)(2,1)S(1)} collective-permute-done((bf16[208,128]{1,0:T(8,128)(2,1)S(1)}, bf16[208,128]{1,0:T(8,128)(2,1)S(1)}, u32[]{:S(2)}, u32[]{:S(2)}) %collective-permute-start.4) | collective-permute-done | bytes 53280 | tf_op jit(solution)/shard_map/ppermute | solution.py:34
  54.9 1.8 %collective-permute-done.3.first_part = bf16[208,128]{1,0:T(8,128)(2,1)S(1)} collective-permute-done((bf16[208,128]{1,0:T(8,128)(2,1)S(1)}, bf16[208,128]{1,0:T(8,128)(2,1)S(1)}, u32[]{:S(2)}, u32[]{:S(2)}) %collective-permute-start.3) | collective-permute-done | bytes 53280 | tf_op jit(solution)/shard_map/ppermute | solution.py:34
  56.8 0.4 finish.1
  57.2 6.9 %collective-permute-start.6 = (bf16[16,64]{1,0:T(8,128)(2,1)S(1)}, bf16[16,64]{1,0:T(8,128)(2,1)S(1)}, u32[]{:S(2)}, u32[]{:S(2)}) collective-permute-start(bf16[16,64]{1,0:T(8,128)(2,1)S(1)} %finish.1), channel_id=1, source_target_pairs={{0,1},{1,0},{2,3},{3,2},{4,5},{5,4},{6,7},{7,6},{8,9},{9,8},{10,11... | collective-permute-start | bytes 6152 | tf_op jit(solution)/shard_map/ppermute | solution.py:518
  64.1 0.8 %collective-permute-done.6 = bf16[16,64]{1,0:T(8,128)(2,1)S(1)} collective-permute-done((bf16[16,64]{1,0:T(8,128)(2,1)S(1)}, bf16[16,64]{1,0:T(8,128)(2,1)S(1)}, u32[]{:S(2)}, u32[]{:S(2)}) %collective-permute-start.6) | collective-permute-done | bytes 2080 | tf_op jit(solution)/shard_map/ppermute | solution.py:518
  64.9 0.6 fusion
  (9 shorter events, 0.0 us)
Async XLA Ops:
  1.9 30.2 %copy-start = (bf16[1,512,12,128]{3,1,2,0:T(8,128)(2,1)S(1)}, bf16[1,512,12,128]{3,1,2,0:T(8,128)(2,1)}, u32[]{:S(2)}) copy-start(bf16[1,512,12,128]{3,1,2,0:T(8,128)(2,1)} %param.21) | copy-start | bytes 4718596
  1.9 30.2 %copy-start.1 = (bf16[1,512,12,128]{3,1,2,0:T(8,128)(2,1)S(1)}, bf16[1,512,12,128]{3,1,2,0:T(8,128)(2,1)}, u32[]{:S(2)}) copy-start(bf16[1,512,12,128]{3,1,2,0:T(8,128)(2,1)} %param.22) | copy-start | bytes 4718596
  1.9 30.2 %copy-start.3 = (f32[12]{0:T(128)S(1)}, f32[12]{0:T(128)}, u32[]{:S(2)}) copy-start(f32[12]{0:T(128)} %bias.3) | copy-start | bytes 148
  19.6 8.5 %collective-permute-start.2 = (bf16[288,128]{1,0:T(8,128)(2,1)S(1)}, bf16[288,128]{1,0:T(8,128)(2,1)S(1)}, u32[]{:S(2)}, u32[]{:S(2)}) collective-permute-start(bf16[288,128]{1,0:T(8,128)(2,1)S(1)} %forward.1.own), channel_id=1, source_target_pairs={{0,48},{2,50},{4,52},{6,54},{8,56},{10,58},{12,60},{14,62},{16,0},... | collective-permute-start | bytes 221192 | tf_op jit(solution)/shard_map/ppermute | solution.py:34
  24.8 5.4 %collective-permute-start.1 = (bf16[288,128]{1,0:T(8,128)(2,1)S(1)}, bf16[288,128]{1,0:T(8,128)(2,1)S(1)}, u32[]{:S(2)}, u32[]{:S(2)}) collective-permute-start(bf16[288,128]{1,0:T(8,128)(2,1)S(1)} %forward.1.own), channel_id=1, source_target_pairs={{0,16},{2,18},{4,20},{6,22},{8,24},{10,26},{12,28},{14,30},{16,32}... | collective-permute-start | bytes 221192 | tf_op jit(solution)/shard_map/ppermute | solution.py:34
  24.8 7.3 %collective-permute-start = (bf16[288,128]{1,0:T(8,128)(2,1)S(1)}, bf16[288,128]{1,0:T(8,128)(2,1)S(1)}, u32[]{:S(2)}, u32[]{:S(2)}) collective-permute-start(bf16[288,128]{1,0:T(8,128)(2,1)S(1)} %forward.1.own), channel_id=1, source_target_pairs={{0,32},{2,34},{4,36},{6,38},{8,40},{10,42},{12,44},{14,46},{16,48}... | collective-permute-start | bytes 221192 | tf_op jit(solution)/shard_map/ppermute | solution.py:34
  34.5 18.2 %copy-start.4 = (s32[1,16]{1,0:T(1,128)S(1)}, s32[1,16]{1,0:T(1,128)}, u32[]{:S(2)}) copy-start(s32[1,16]{1,0:T(1,128)} %param.25) | copy-start | bytes 196
  46.9 7.1 %collective-permute-start.5 = (bf16[208,128]{1,0:T(8,128)(2,1)S(1)}, bf16[208,128]{1,0:T(8,128)(2,1)S(1)}, u32[]{:S(2)}, u32[]{:S(2)}) collective-permute-start(bf16[208,128]{1,0:T(8,128)(2,1)S(1)} %get-tuple-element.26.own), channel_id=1, source_target_pairs={{0,48},{2,50},{4,52},{6,54},{8,56},{10,58},{12,60},{14,62},{16,0},... | collective-permute-start | bytes 159752 | tf_op jit(solution)/shard_map/ppermute | solution.py:34
  49.8 5.1 %collective-permute-start.4 = (bf16[208,128]{1,0:T(8,128)(2,1)S(1)}, bf16[208,128]{1,0:T(8,128)(2,1)S(1)}, u32[]{:S(2)}, u32[]{:S(2)}) collective-permute-start(bf16[208,128]{1,0:T(8,128)(2,1)S(1)} %get-tuple-element.26.own), channel_id=1, source_target_pairs={{0,16},{2,18},{4,20},{6,22},{8,24},{10,26},{12,28},{14,30},{16,32}... | collective-permute-start | bytes 159752 | tf_op jit(solution)/shard_map/ppermute | solution.py:34
  49.8 6.9 %collective-permute-start.3 = (bf16[208,128]{1,0:T(8,128)(2,1)S(1)}, bf16[208,128]{1,0:T(8,128)(2,1)S(1)}, u32[]{:S(2)}, u32[]{:S(2)}) collective-permute-start(bf16[208,128]{1,0:T(8,128)(2,1)S(1)} %get-tuple-element.26.own), channel_id=1, source_target_pairs={{0,32},{2,34},{4,36},{6,38},{8,40},{10,42},{12,44},{14,46},{16,48}... | collective-permute-start | bytes 159752 | tf_op jit(solution)/shard_map/ppermute | solution.py:34
  52.7 4.1 %copy-start.2 = (bf16[1536,64]{0,1:T(8,128)(2,1)S(1)}, bf16[1536,64]{0,1:T(8,128)(2,1)}, u32[]{:S(2)}) copy-start(bf16[1536,64]{0,1:T(8,128)(2,1)} %param.19) | copy-start | bytes 589828
  57.2 7.7 %collective-permute-start.6 = (bf16[16,64]{1,0:T(8,128)(2,1)S(1)}, bf16[16,64]{1,0:T(8,128)(2,1)S(1)}, u32[]{:S(2)}, u32[]{:S(2)}) collective-permute-start(bf16[16,64]{1,0:T(8,128)(2,1)S(1)} %finish.1), channel_id=1, source_target_pairs={{0,1},{1,0},{2,3},{3,2},{4,5},{5,4},{6,7},{7,6},{8,9},{9,8},{10,11... | collective-permute-start | bytes 6152 | tf_op jit(solution)/shard_map/ppermute | solution.py:518

commit v5 on v4

--- a/solution.py
+++ b/solution.py
@@ -98,8 +98,8 @@
 
 
 def project_kernel(
-    prefix_len,
-    accepted,
+    bias_far,
+    parent_far,
     tokens_far,
     gain_far,
     query_far,
@@ -107,6 +107,8 @@
     value_far,
     gate_far,
     out,
+    bias,
+    parent,
     tokens,
     gain,
     w_query,
@@ -115,7 +117,6 @@
     w_gate,
     sems,
 ):
-    del prefix_len, accepted
     copies = [
         pltpu.make_async_copy(source, target, sems.at[index])
         for index, (source, target) in enumerate(
@@ -126,6 +127,8 @@
                 (key_far, w_key),
                 (value_far, w_value),
                 (gate_far, w_gate),
+                (bias_far, bias),
+                (parent_far, parent),
             )
         )
     ]
@@ -161,6 +164,8 @@
         out[dest, rows + slot * PROPS : rows + (slot + 1) * PROPS, :] = jnp.zeros(
             (PROPS, HEAD), BF16
         )
+    for copy in copies[6:]:
+        copy.wait()
 
 
 def add_up(parts):
@@ -186,24 +191,22 @@
     second_part,
     third_part,
     keys,
-    values,
+    values_far,
     out,
     query_out,
-    keys_next,
-    values_next,
-    keys_window,
-    values_window,
-    sems,
+    values,
+    limits,
+    sem,
 ):
     heads, ctx_dev, _ = keys.shape
     rows = heads * PROPS
-    copies = [
-        pltpu.make_async_copy(keys, keys_next, sems.at[0]),
-        pltpu.make_async_copy(values, values_next, sems.at[1]),
-    ]
-    for copy in copies:
-        copy.start()
-    offset, first = window_of(prefix_len, accepted, ctx_dev)
+    load = pltpu.make_async_copy(values_far, values, sem)
+    load.start()
+    offset = prefix_len[0] + accepted[0] - lax.axis_index("kv") * ctx_dev
+    first = jnp.minimum(jnp.maximum(offset, 0), ctx_dev - WINDOW)
+    first = pl.multiple_of((first >> 4) << 4, PROPS)
+    limits[0] = offset
+    limits[1] = first
     total = add_up([own[...], first_part[...], second_part[...], third_part[...]])
     squares = jnp.sum(total[own.shape[0] - PROPS :], axis=1, keepdims=True)
     rscale = lax.rsqrt(squares / D + EPS)
@@ -233,6 +236,7 @@
         laters.append(inside + beyond)
         beyond = beyond + whole
     later = jnp.concatenate(laters[::-1], axis=1)
+    load.wait()
     rests = []
     for head in range(heads):
         there = slice(head * PROPS, (head + 1) * PROPS)
@@ -244,10 +248,6 @@
     block = rest_block(rests)
     for dest in range(INNER):
         out[dest, rows + share :, :] = block
-    keys_window[...] = keys[:, pl.ds(first, WINDOW), :]
-    values_window[...] = values[:, pl.ds(first, WINDOW), :]
-    for copy in copies:
-        copy.wait()
 
 
 def merge_kernel(arrived, out, fresh):
@@ -275,16 +275,13 @@
 
 
 def tree_kernel(
-    prefix_len,
-    accepted,
+    limits,
     bias,
     parent,
     fresh,
     query,
-    keys_window,
-    values_window,
-    keys_old,
-    values_old,
+    keys,
+    values,
     tree_out,
     tail_out,
     gate_out,
@@ -294,27 +291,31 @@
     masks,
     sems,
 ):
-    del keys_old, values_old
-    heads, ctx_dev, _ = keys_next.shape
-    offset, first = window_of(prefix_len, accepted, ctx_dev)
+    heads = keys_next.shape[0]
+    bulk = [
+        pltpu.make_async_copy(keys, keys_next, sems.at[0]),
+        pltpu.make_async_copy(values, values_next, sems.at[1]),
+    ]
+    for copy in bulk:
+        copy.start()
+    offset = limits[0]
+    first = pl.multiple_of(limits[1], PROPS)
     source = first + iota((WINDOW, PROPS), 0) - offset
     picker = jnp.where(source == iota((WINDOW, PROPS), 1), 1.0, 0.0).astype(BF16)
     source = first + iota((WINDOW, HEAD), 0) - offset
     inside = (source >= 0) & (source < PROPS)
     copies = []
-    for which, (window, target) in enumerate(
-        ((keys_window, keys_next), (values_window, values_next))
-    ):
+    for which, (cache, target) in enumerate(((keys, keys_next), (values, values_next))):
         for head in range(heads):
             start = (which * heads + head) * PROPS
             placed = dot(picker, fresh[start : start + PROPS, :])
-            patches[which, head] = jnp.where(inside, placed, window[head].astype(F32)).astype(BF16)
+            there = cache[head, pl.ds(first, WINDOW), :].astype(F32)
+            patches[which, head] = jnp.where(inside, placed, there).astype(BF16)
         copies.append(
             pltpu.make_async_copy(
-                patches.at[which], target.at[:, pl.ds(first, WINDOW), :], sems.at[which]
+                patches.at[which], target.at[:, pl.ds(first, WINDOW), :], sems.at[2 + which]
             )
         )
-        copies[-1].start()
     row = iota((PROPS, PROPS), 0)
     reach = jnp.zeros((PROPS, PROPS), jnp.int32)
     masks[0] = 0
@@ -341,6 +342,9 @@
         tree_out[there, :] = dot(weight, fresh[start : start + PROPS, :])
     gate = fresh[2 * heads * PROPS : 3 * heads * PROPS, :].astype(F32)
     gate_out[...] = gate * jax.nn.sigmoid(gate)
+    for before, copy in zip(bulk, copies):
+        before.wait()
+        copy.start()
     for copy in copies:
         copy.wait()
 
@@ -382,14 +386,16 @@
     return pltpu.with_memory_space_constraint(value, pltpu.VMEM)
 
 
+def small(dims, dtype):
+    return pltpu.SMEM(dims, dtype)
+
+
 def far(value):
     return pltpu.with_memory_space_constraint(value, pltpu.HBM)
 
 
-def window_of(prefix_len, accepted, ctx_dev):
-    offset = prefix_len[0] + accepted[0] - lax.axis_index("kv") * ctx_dev
-    start = jnp.minimum(jnp.maximum(offset, 0), ctx_dev - WINDOW)
-    return offset, pl.multiple_of((start >> 4) << 4, PROPS)
+def kept(value):
+    return pltpu.with_memory_space_constraint(value, pltpu.SMEM)
 
 
 def local(
@@ -415,27 +421,39 @@
     keys = jnp.transpose(cache_keys[0], (1, 0, 2))
     values = jnp.transpose(cache_values[0], (1, 0, 2))
 
-    pieces = pl.pallas_call(
+    pieces, bias, parents = pl.pallas_call(
         project_kernel,
-        out_shape=near((INNER, sent, HEAD)),
-        in_specs=[SMEM] * 2 + [ANY] * 6,
-        out_specs=VMEM,
+        out_shape=(
+            near((INNER, sent, HEAD)),
+            small((heads,), F32),
+            small((PROPS,), jnp.int32),
+        ),
+        in_specs=[ANY] * 8,
+        out_specs=(VMEM, SMEM, SMEM),
         scratch_shapes=[
             pltpu.VMEM(tokens.shape[1:], BF16),
             pltpu.VMEM((1, columns), F32),
             *[pltpu.VMEM(w_query.shape, BF16)] * 4,
-            pltpu.SemaphoreType.DMA((6,)),
+            pltpu.SemaphoreType.DMA((8,)),
         ],
         name="project",
         compiler_params=PARAMS,
     )(
-        prefix_len,
-        accepted,
         *(
             far(value)
-            for value in (tokens[0], norm_gain[None], w_query, w_key, w_value, w_gate)
+            for value in (
+                head_bias,
+                parent[0],
+                tokens[0],
+                norm_gain[None],
+                w_query,
+                w_key,
+                w_value,
+                w_gate,
+            )
         ),
     )
+    bias, parents = kept(bias), kept(parents)
     pieces = pl.pallas_call(
         forward_kernel,
         out_shape=near((sent, HEAD)),
@@ -444,29 +462,27 @@
         name="forward",
         compiler_params=PARAMS,
     )(exchange(pieces))
-    window = near((heads, WINDOW, HEAD))
-    pieces, query, keys_next, values_next, keys_window, values_window = pl.pallas_call(
+    keys = held(keys)
+    pieces, query, near_values, limits = pl.pallas_call(
         attend_kernel,
         out_shape=(
             near((INNER, sent, HEAD)),
             near((rows, HEAD)),
-            shaped(keys.shape),
-            shaped(values.shape),
-            window,
-            window,
+            near(values.shape),
+            small((2,), jnp.int32),
         ),
-        in_specs=[SMEM] * 3 + [VMEM] * 6,
-        out_specs=(VMEM, VMEM, ANY, ANY, VMEM, VMEM),
-        scratch_shapes=[pltpu.SemaphoreType.DMA((2,))],
+        in_specs=[SMEM] * 3 + [VMEM] * 5 + [ANY],
+        out_specs=(VMEM, VMEM, VMEM, SMEM),
+        scratch_shapes=[pltpu.SemaphoreType.DMA],
         name="attend",
         compiler_params=PARAMS,
     )(
         prefix_len,
         accepted,
-        head_bias,
+        bias,
         *shifted(pieces),
-        held(keys),
-        held(values),
+        keys,
+        far(values),
     )
     pieces, fresh = pl.pallas_call(
         merge_kernel,
@@ -484,27 +500,23 @@
             shaped(keys.shape),
             shaped(values.shape),
         ),
-        in_specs=[SMEM] * 4 + [VMEM] * 4 + [ANY, ANY],
+        in_specs=[SMEM] * 3 + [VMEM] * 4,
         out_specs=(VMEM, VMEM, VMEM, ANY, ANY),
-        input_output_aliases={8: 3, 9: 4},
         scratch_shapes=[
             pltpu.VMEM((2, heads, WINDOW, HEAD), BF16),
             pltpu.SMEM((PROPS,), jnp.int32),
-            pltpu.SemaphoreType.DMA((2,)),
+            pltpu.SemaphoreType.DMA((4,)),
         ],
         name="tree",
         compiler_params=PARAMS,
     )(
-        prefix_len,
-        accepted,
-        head_bias,
-        parent[0],
+        kept(limits),
+        bias,
+        parents,
         held(fresh),
         held(query),
-        held(keys_window),
-        held(values_window),
-        keys_next,
-        values_next,
+        keys,
+        held(near_values),
     )
     part_out = pl.pallas_call(
         finish_kernel,

time: 65.7 us -> 62.7 us (0.954)
  waiting for transfers between devices: 7.53 us -> 3.58 us
  starting transfers between devices: 21.1 us -> 22 us
  blocking collectives: 27.8 us -> 27.1 us
    ppermute x6, starting transfers between devices: 14.2 us -> 19.5 us  [shifted(): parts.append(lax.ppermute(value, 'kv', pairs))]
    ppermute x1, starting transfers between devices: 6.86 us -> 2.48 us  [local(): other = lax.ppermute(part_out, 'tp', [(0, 1), (1, 0)])]
    ppermute x6, waiting for transfers between devices: 6.71 us -> 2.75 us  [shifted(): parts.append(lax.ppermute(value, 'kv', pairs))]
    pallas_call x1, Pallas kernels: 1.4 us -> 2.51 us  [local(): pl.pallas_call(tree_kernel, out_shape=(*[near((rows, HEAD), F32)] * 3, sh...]
  transfers between devices with their start and end apart: 7 -> 7, of which waited for: 5 -> 4; matrix products, arithmetic and copies ran while one was open for 0% -> 0% of each run, Pallas kernels for 2% -> 4%
where the time goes in v5:
time: 62.7 us; the launch traced here: 62.5 us
  blocking collectives  27.1 us (43%)
  starting transfers between devices  22 us (35%)
  Pallas kernels  7.17 us (11%)
  waiting for transfers between devices  3.58 us (6%)
  between operations  1.99 us (3%)
    all_to_all x2, blocking collectives, exchange(): lax.all_to_all(pieces, 'kv', 0, 0, axis_index_groups=groups, tiled=True)  27.1 us
    ppermute x6, starting transfers between devices, shifted(): parts.append(lax.ppermute(value, 'kv', pairs))  19.5 us
    ppermute x6, waiting for transfers between devices, shifted(): parts.append(lax.ppermute(value, 'kv', pairs))  2.75 us
    pallas_call x1, Pallas kernels, local(): pl.pallas_call(tree_kernel, out_shape=(*[near((rows, HEAD), F32)] * 3, sh...  2.51 us
    ppermute x1, starting transfers between devices, local(): other = lax.ppermute(part_out, 'tp', [(0, 1), (1, 0)])  2.48 us
    pallas_call x1, Pallas kernels, local(): pl.pallas_call(attend_kernel, out_shape=(near((INNER, sent, HEAD)), near(...  1.88 us
    pallas_call x1, Pallas kernels, local(): pl.pallas_call(project_kernel, out_shape=(near((INNER, sent, HEAD)), smal...  1.77 us
  transfers between devices with their start and end apart: 7, of which 4 were waited for; matrix products, arithmetic and copies ran while one was open for 0% of the time, Pallas kernels for 4%

profile of v5, /device:TPU:1, one launch (start us, length us, event | category | flops | bytes accessed | tf_op | source)
XLA Modules:
  0.0 62.5 jit_solution(8159724907110813916)
XLA Ops:
  0.6 1.8 %project.1 = (bf16[8,288,128]{2,1,0:T(8,128)(2,1)S(1)}, f32[12]{0:T(128)S(4)}, s32[16]{0:T(128)S(4)}) custom-call(f32[12]{0:T(128)} %bias_far.1, s32[16]{0:T(128)} %bitcast.23, bf16[16,64]{1,0:T(8,128)(2,1)} %bitcast.22, f32[1,64]{1,0:T(1,128)} %bitcast.24, bf16[64,1536]{1,0:T(8,128)(2,1)} %query_far.1, bf16[64,1536]{1,0:T(8,128)(2,1)} %key_far.1, ...), custom_call_target="tpu_custom_call" | custom-call | tf_op jit(solution)/shard_map/project/pallas_call | solution.py:424
  2.4 15.8 %all_to_all.10.arrived = bf16[8,288,128]{2,1,0:T(8,128)(2,1)S(1)} all-to-all(bf16[8,288,128]{2,1,0:T(8,128)(2,1)S(1)} %get-tuple-element.18), channel_id=1, replica_groups={{0,2,4,6,8,10,12,14},{16,18,20,22,24,26,28,30},{32,34,36,38,40,42,44,46..., dimensions={0} | all-to-all | bytes 1179648 | tf_op jit(solution)/shard_map/all_to_all | solution.py:26
  18.2 0.1 forward.1.own
  18.3 6.1 %collective-permute-start = (bf16[288,128]{1,0:T(8,128)(2,1)S(1)}, bf16[288,128]{1,0:T(8,128)(2,1)S(1)}, u32[]{:S(2)}, u32[]{:S(2)}) collective-permute-start(bf16[288,128]{1,0:T(8,128)(2,1)S(1)} %forward.1.own), channel_id=1, source_target_pairs={{0,32},{2,34},{4,36},{6,38},{8,40},{10,42},{12,44},{14,46},{16,48}... | collective-permute-start | bytes 221192 | tf_op jit(solution)/shard_map/ppermute | solution.py:34
  24.4 1.2 %collective-permute-start.1 = (bf16[288,128]{1,0:T(8,128)(2,1)S(1)}, bf16[288,128]{1,0:T(8,128)(2,1)S(1)}, u32[]{:S(2)}, u32[]{:S(2)}) collective-permute-start(bf16[288,128]{1,0:T(8,128)(2,1)S(1)} %forward.1.own), channel_id=1, source_target_pairs={{0,16},{2,18},{4,20},{6,22},{8,24},{10,26},{12,28},{14,30},{16,32}... | collective-permute-start | bytes 221192 | tf_op jit(solution)/shard_map/ppermute | solution.py:34
  25.6 2.4 %collective-permute-start.2 = (bf16[288,128]{1,0:T(8,128)(2,1)S(1)}, bf16[288,128]{1,0:T(8,128)(2,1)S(1)}, u32[]{:S(2)}, u32[]{:S(2)}) collective-permute-start(bf16[288,128]{1,0:T(8,128)(2,1)S(1)} %forward.1.own), channel_id=1, source_target_pairs={{0,48},{2,50},{4,52},{6,54},{8,56},{10,58},{12,60},{14,62},{16,0},... | collective-permute-start | bytes 221192 | tf_op jit(solution)/shard_map/ppermute | solution.py:34
  29.3 0.0 collective-permute-done.first_part
  29.3 1.4 %collective-permute-done.1.second_part = bf16[288,128]{1,0:T(8,128)(2,1)S(1)} collective-permute-done((bf16[288,128]{1,0:T(8,128)(2,1)S(1)}, bf16[288,128]{1,0:T(8,128)(2,1)S(1)}, u32[]{:S(2)}, u32[]{:S(2)}) %collective-permute-start.1) | collective-permute-done | bytes 73760 | tf_op jit(solution)/shard_map/ppermute | solution.py:34
  30.7 0.9 %collective-permute-done.2.third_part = bf16[288,128]{1,0:T(8,128)(2,1)S(1)} collective-permute-done((bf16[288,128]{1,0:T(8,128)(2,1)S(1)}, bf16[288,128]{1,0:T(8,128)(2,1)S(1)}, u32[]{:S(2)}, u32[]{:S(2)}) %collective-permute-start.2) | collective-permute-done | bytes 73760 | tf_op jit(solution)/shard_map/ppermute | solution.py:34
  31.5 0.0 copy-done
  31.6 1.9 %attend.1 = (bf16[8,288,128]{2,1,0:T(8,128)(2,1)S(1)}, bf16[192,128]{1,0:T(8,128)(2,1)S(1)}, bf16[12,512,128]{2,1,0:T(8,128)(2,1)S(1)}, s32[2]{0:T(128)S(4)}) custom-call(s32[1]{0:T(128)S(6)} %copy.16.prefix_len, s32[1]{0:T(128)S(6)} %copy.17.accepted, f32[12]{0:T(128)S(4)} %get-tuple-element.17.bias, bf16[288,128]{1,0:T(8,128)(2,1)S(1)} %forward.1.own, ...), custom_call_target="tpu_custom_call" | custom-call | tf_op jit(solution)/shard_map/attend/pallas_call | solution.py:466
  33.4 11.3 %all_to_all.11.arrived = bf16[8,288,128]{2,1,0:T(8,128)(2,1)S(1)} all-to-all(bf16[8,288,128]{2,1,0:T(8,128)(2,1)S(1)} %get-tuple-element.21), channel_id=1, replica_groups={{0,2,4,6,8,10,12,14},{16,18,20,22,24,26,28,30},{32,34,36,38,40,42,44,46..., dimensions={0} | all-to-all | bytes 1179648 | tf_op jit(solution)/shard_map/all_to_all | solution.py:26
  44.8 0.5 merge.1
  45.2 6.3 %collective-permute-start.3 = (bf16[208,128]{1,0:T(8,128)(2,1)S(1)}, bf16[208,128]{1,0:T(8,128)(2,1)S(1)}, u32[]{:S(2)}, u32[]{:S(2)}) collective-permute-start(bf16[208,128]{1,0:T(8,128)(2,1)S(1)} %get-tuple-element.28.own), channel_id=1, source_target_pairs={{0,32},{2,34},{4,36},{6,38},{8,40},{10,42},{12,44},{14,46},{16,48}... | collective-permute-start | bytes 159752 | tf_op jit(solution)/shard_map/ppermute | solution.py:34
  51.5 0.0 collective-permute-start.4
  51.5 3.6 %collective-permute-start.5 = (bf16[208,128]{1,0:T(8,128)(2,1)S(1)}, bf16[208,128]{1,0:T(8,128)(2,1)S(1)}, u32[]{:S(2)}, u32[]{:S(2)}) collective-permute-start(bf16[208,128]{1,0:T(8,128)(2,1)S(1)} %get-tuple-element.28.own), channel_id=1, source_target_pairs={{0,48},{2,50},{4,52},{6,54},{8,56},{10,58},{12,60},{14,62},{16,0},... | collective-permute-start | bytes 159752 | tf_op jit(solution)/shard_map/ppermute | solution.py:34
  55.1 2.5 %tree.1 = (f32[192,128]{1,0:T(8,128)S(1)}, f32[192,128]{1,0:T(8,128)S(1)}, f32[192,128]{1,0:T(8,128)S(1)}, bf16[12,512,128]{2,1,0:T(8,128)(2,1)}, bf16[12,512,128]{2,1,0:T(8,128)(2,1)}) custom-call(s32[2]{0:T(128)S(4)} %get-tuple-element.19.limits, f32[12]{0:T(128)S(4)} %get-tuple-element.17.bias, s32[16]{0:T(128)S(4)} %get-tuple-element.20.parent, ...), custom_call_target="tpu_custom_call" | custom-call | tf_op jit(solution)/shard_map/tree/pallas_call | solution.py:496
  57.6 0.0 collective-permute-done.3.first_part
  57.6 0.5 collective-permute-done.4.second_part
  58.1 0.0 collective-permute-done.5.third_part
  58.1 0.4 finish.1
  58.6 2.5 %collective-permute-start.6 = (bf16[16,64]{1,0:T(8,128)(2,1)S(1)}, bf16[16,64]{1,0:T(8,128)(2,1)S(1)}, u32[]{:S(2)}, u32[]{:S(2)}) collective-permute-start(bf16[16,64]{1,0:T(8,128)(2,1)S(1)} %finish.1), channel_id=1, source_target_pairs={{0,1},{1,0},{2,3},{3,2},{4,5},{5,4},{6,7},{7,6},{8,9},{9,8},{10,11... | collective-permute-start | bytes 6152 | tf_op jit(solution)/shard_map/ppermute | solution.py:530
  61.1 0.8 %collective-permute-done.6 = bf16[16,64]{1,0:T(8,128)(2,1)S(1)} collective-permute-done((bf16[16,64]{1,0:T(8,128)(2,1)S(1)}, bf16[16,64]{1,0:T(8,128)(2,1)S(1)}, u32[]{:S(2)}, u32[]{:S(2)}) %collective-permute-start.6) | collective-permute-done | bytes 2080 | tf_op jit(solution)/shard_map/ppermute | solution.py:530
  61.9 0.6 fusion
  (3 shorter events, 0.0 us)
Async XLA Ops:
  0.6 30.9 %copy-start = (bf16[1,512,12,128]{3,1,2,0:T(8,128)(2,1)S(1)}, bf16[1,512,12,128]{3,1,2,0:T(8,128)(2,1)}, u32[]{:S(2)}) copy-start(bf16[1,512,12,128]{3,1,2,0:T(8,128)(2,1)} %param.21) | copy-start | bytes 4718596
  18.3 11.0 %collective-permute-start = (bf16[288,128]{1,0:T(8,128)(2,1)S(1)}, bf16[288,128]{1,0:T(8,128)(2,1)S(1)}, u32[]{:S(2)}, u32[]{:S(2)}) collective-permute-start(bf16[288,128]{1,0:T(8,128)(2,1)S(1)} %forward.1.own), channel_id=1, source_target_pairs={{0,32},{2,34},{4,36},{6,38},{8,40},{10,42},{12,44},{14,46},{16,48}... | collective-permute-start | bytes 221192 | tf_op jit(solution)/shard_map/ppermute | solution.py:34
  24.4 6.2 %collective-permute-start.1 = (bf16[288,128]{1,0:T(8,128)(2,1)S(1)}, bf16[288,128]{1,0:T(8,128)(2,1)S(1)}, u32[]{:S(2)}, u32[]{:S(2)}) collective-permute-start(bf16[288,128]{1,0:T(8,128)(2,1)S(1)} %forward.1.own), channel_id=1, source_target_pairs={{0,16},{2,18},{4,20},{6,22},{8,24},{10,26},{12,28},{14,30},{16,32}... | collective-permute-start | bytes 221192 | tf_op jit(solution)/shard_map/ppermute | solution.py:34
  25.6 5.9 %collective-permute-start.2 = (bf16[288,128]{1,0:T(8,128)(2,1)S(1)}, bf16[288,128]{1,0:T(8,128)(2,1)S(1)}, u32[]{:S(2)}, u32[]{:S(2)}) collective-permute-start(bf16[288,128]{1,0:T(8,128)(2,1)S(1)} %forward.1.own), channel_id=1, source_target_pairs={{0,48},{2,50},{4,52},{6,54},{8,56},{10,58},{12,60},{14,62},{16,0},... | collective-permute-start | bytes 221192 | tf_op jit(solution)/shard_map/ppermute | solution.py:34
  45.2 12.4 %collective-permute-start.3 = (bf16[208,128]{1,0:T(8,128)(2,1)S(1)}, bf16[208,128]{1,0:T(8,128)(2,1)S(1)}, u32[]{:S(2)}, u32[]{:S(2)}) collective-permute-start(bf16[208,128]{1,0:T(8,128)(2,1)S(1)} %get-tuple-element.28.own), channel_id=1, source_target_pairs={{0,32},{2,34},{4,36},{6,38},{8,40},{10,42},{12,44},{14,46},{16,48}... | collective-permute-start | bytes 159752 | tf_op jit(solution)/shard_map/ppermute | solution.py:34
  51.5 6.6 %collective-permute-start.4 = (bf16[208,128]{1,0:T(8,128)(2,1)S(1)}, bf16[208,128]{1,0:T(8,128)(2,1)S(1)}, u32[]{:S(2)}, u32[]{:S(2)}) collective-permute-start(bf16[208,128]{1,0:T(8,128)(2,1)S(1)} %get-tuple-element.28.own), channel_id=1, source_target_pairs={{0,16},{2,18},{4,20},{6,22},{8,24},{10,26},{12,28},{14,30},{16,32}... | collective-permute-start | bytes 159752 | tf_op jit(solution)/shard_map/ppermute | solution.py:34
  51.5 6.6 %collective-permute-start.5 = (bf16[208,128]{1,0:T(8,128)(2,1)S(1)}, bf16[208,128]{1,0:T(8,128)(2,1)S(1)}, u32[]{:S(2)}, u32[]{:S(2)}) collective-permute-start(bf16[208,128]{1,0:T(8,128)(2,1)S(1)} %get-tuple-element.28.own), channel_id=1, source_target_pairs={{0,48},{2,50},{4,52},{6,54},{8,56},{10,58},{12,60},{14,62},{16,0},... | collective-permute-start | bytes 159752 | tf_op jit(solution)/shard_map/ppermute | solution.py:34
  55.1 3.0 %copy-start.1 = (bf16[1536,64]{0,1:T(8,128)(2,1)S(1)}, bf16[1536,64]{0,1:T(8,128)(2,1)}, u32[]{:S(2)}) copy-start(bf16[1536,64]{0,1:T(8,128)(2,1)} %param.19) | copy-start | bytes 589828
  58.6 3.3 %collective-permute-start.6 = (bf16[16,64]{1,0:T(8,128)(2,1)S(1)}, bf16[16,64]{1,0:T(8,128)(2,1)S(1)}, u32[]{:S(2)}, u32[]{:S(2)}) collective-permute-start(bf16[16,64]{1,0:T(8,128)(2,1)S(1)} %finish.1), channel_id=1, source_target_pairs={{0,1},{1,0},{2,3},{3,2},{4,5},{5,4},{6,7},{7,6},{8,9},{9,8},{10,11... | collective-permute-start | bytes 6152 | tf_op jit(solution)/shard_map/ppermute | solution.py:530

commit v6 on v5

--- a/solution.py
+++ b/solution.py
@@ -182,6 +182,18 @@
     out[count:, :] = square_block(jnp.sum(total[count:], axis=1, keepdims=True))
 
 
+def fetch_kernel(sums, keys_far, values_far, keys, values, sems):
+    del sums
+    copies = [
+        pltpu.make_async_copy(keys_far, keys, sems.at[0]),
+        pltpu.make_async_copy(values_far, values, sems.at[1]),
+    ]
+    for copy in copies:
+        copy.start()
+    for copy in copies:
+        copy.wait()
+
+
 def attend_kernel(
     prefix_len,
     accepted,
@@ -191,17 +203,13 @@
     second_part,
     third_part,
     keys,
-    values_far,
+    values,
     out,
     query_out,
-    values,
     limits,
-    sem,
 ):
     heads, ctx_dev, _ = keys.shape
     rows = heads * PROPS
-    load = pltpu.make_async_copy(values_far, values, sem)
-    load.start()
     offset = prefix_len[0] + accepted[0] - lax.axis_index("kv") * ctx_dev
     first = jnp.minimum(jnp.maximum(offset, 0), ctx_dev - WINDOW)
     first = pl.multiple_of((first >> 4) << 4, PROPS)
@@ -236,7 +244,6 @@
         laters.append(inside + beyond)
         beyond = beyond + whole
     later = jnp.concatenate(laters[::-1], axis=1)
-    load.wait()
     rests = []
     for head in range(heads):
         there = slice(head * PROPS, (head + 1) * PROPS)
@@ -462,18 +469,25 @@
         name="forward",
         compiler_params=PARAMS,
     )(exchange(pieces))
-    keys = held(keys)
-    pieces, query, near_values, limits = pl.pallas_call(
+    keys, values = pl.pallas_call(
+        fetch_kernel,
+        out_shape=(near(keys.shape), near(values.shape)),
+        in_specs=[ANY] * 3,
+        out_specs=(VMEM, VMEM),
+        scratch_shapes=[pltpu.SemaphoreType.DMA((2,))],
+        name="fetch",
+        compiler_params=PARAMS,
+    )(held(pieces), far(keys), far(values))
+    keys, values = held(keys), held(values)
+    pieces, query, limits = pl.pallas_call(
         attend_kernel,
         out_shape=(
             near((INNER, sent, HEAD)),
             near((rows, HEAD)),
-            near(values.shape),
             small((2,), jnp.int32),
         ),
-        in_specs=[SMEM] * 3 + [VMEM] * 5 + [ANY],
-        out_specs=(VMEM, VMEM, VMEM, SMEM),
-        scratch_shapes=[pltpu.SemaphoreType.DMA],
+        in_specs=[SMEM] * 3 + [VMEM] * 6,
+        out_specs=(VMEM, VMEM, SMEM),
         name="attend",
         compiler_params=PARAMS,
     )(
@@ -482,7 +496,7 @@
         bias,
         *shifted(pieces),
         keys,
-        far(values),
+        values,
     )
     pieces, fresh = pl.pallas_call(
         merge_kernel,
@@ -516,7 +530,7 @@
         held(fresh),
         held(query),
         keys,
-        held(near_values),
+        values,
     )
     part_out = pl.pallas_call(
         finish_kernel,

time: 62.7 us -> 62 us (0.989)
  waiting for transfers between devices: 3.58 us -> 1.66 us
  Pallas kernels: 7.17 us -> 8.35 us
    ppermute x6, waiting for transfers between devices: 2.75 us -> 0.84 us  [shifted(): parts.append(lax.ppermute(value, 'kv', pairs))]
    pallas_call x0 -> x1, Pallas kernels: none -> 1.9 us  [local(): pl.pallas_call(fetch_kernel, out_shape=(near(keys.shape), near(values.sha...]
  transfers between devices with their start and end apart: 7 -> 7, of which waited for: 4 -> 3; matrix products, arithmetic and copies ran while one was open for 0% -> 0% of each run, Pallas kernels for 4% -> 7%
where the time goes in v6:
time: 62 us; the launch traced here: 61.7 us
  blocking collectives  27.1 us (44%)
  starting transfers between devices  22 us (35%)
  Pallas kernels  8.35 us (13%)
  between operations  2 us (3%)
  waiting for transfers between devices  1.66 us (3%)
    all_to_all x2, blocking collectives, exchange(): lax.all_to_all(pieces, 'kv', 0, 0, axis_index_groups=groups, tiled=True)  27.1 us
    ppermute x6, starting transfers between devices, shifted(): parts.append(lax.ppermute(value, 'kv', pairs))  19.6 us
    pallas_call x1, Pallas kernels, local(): pl.pallas_call(tree_kernel, out_shape=(*[near((rows, HEAD), F32)] * 3, sh...  2.51 us
    ppermute x1, starting transfers between devices, local(): other = lax.ppermute(part_out, 'tp', [(0, 1), (1, 0)])  2.49 us
    pallas_call x1, Pallas kernels, local(): pl.pallas_call(fetch_kernel, out_shape=(near(keys.shape), near(values.sha...  1.9 us
    pallas_call x1, Pallas kernels, local(): pl.pallas_call(project_kernel, out_shape=(near((INNER, sent, HEAD)), smal...  1.66 us
    pallas_call x1, Pallas kernels, local(): pl.pallas_call(attend_kernel, out_shape=(near((INNER, sent, HEAD)), near(...  1.28 us
  transfers between devices with their start and end apart: 7, of which 3 were waited for; matrix products, arithmetic and copies ran while one was open for 0% of the time, Pallas kernels for 7%

profile of v6, /device:TPU:1, one launch (start us, length us, event | category | flops | bytes accessed | tf_op | source)
XLA Modules:
  0.0 61.7 jit_solution(2818337846151677498)
XLA Ops:
  0.6 1.7 %project.1 = (bf16[8,288,128]{2,1,0:T(8,128)(2,1)S(1)}, f32[12]{0:T(128)S(4)}, s32[16]{0:T(128)S(4)}) custom-call(f32[12]{0:T(128)} %bias_far.1, s32[16]{0:T(128)} %bitcast.22, bf16[16,64]{1,0:T(8,128)(2,1)} %bitcast.21, f32[1,64]{1,0:T(1,128)} %bitcast.23, bf16[64,1536]{1,0:T(8,128)(2,1)} %query_far.1, bf16[64,1536]{1,0:T(8,128)(2,1)} %key_far.1, ...), custom_call_target="tpu_custom_call" | custom-call | tf_op jit(solution)/shard_map/project/pallas_call | solution.py:431
  2.3 15.8 %all_to_all.10.arrived = bf16[8,288,128]{2,1,0:T(8,128)(2,1)S(1)} all-to-all(bf16[8,288,128]{2,1,0:T(8,128)(2,1)S(1)} %get-tuple-element.19), channel_id=1, replica_groups={{0,2,4,6,8,10,12,14},{16,18,20,22,24,26,28,30},{32,34,36,38,40,42,44,46..., dimensions={0} | all-to-all | bytes 1179648 | tf_op jit(solution)/shard_map/all_to_all | solution.py:26
  18.1 0.1 forward.1.sums.own
  18.2 6.1 %collective-permute-start = (bf16[288,128]{1,0:T(8,128)(2,1)S(1)}, bf16[288,128]{1,0:T(8,128)(2,1)S(1)}, u32[]{:S(2)}, u32[]{:S(2)}) collective-permute-start(bf16[288,128]{1,0:T(8,128)(2,1)S(1)} %forward.1.sums.own), channel_id=1, source_target_pairs={{0,32},{2,34},{4,36},{6,38},{8,40},{10,42},{12,44},{14,46},{16,48}... | collective-permute-start | bytes 221192 | tf_op jit(solution)/shard_map/ppermute | solution.py:34
  24.3 1.2 %collective-permute-start.1 = (bf16[288,128]{1,0:T(8,128)(2,1)S(1)}, bf16[288,128]{1,0:T(8,128)(2,1)S(1)}, u32[]{:S(2)}, u32[]{:S(2)}) collective-permute-start(bf16[288,128]{1,0:T(8,128)(2,1)S(1)} %forward.1.sums.own), channel_id=1, source_target_pairs={{0,16},{2,18},{4,20},{6,22},{8,24},{10,26},{12,28},{14,30},{16,32}... | collective-permute-start | bytes 221192 | tf_op jit(solution)/shard_map/ppermute | solution.py:34
  25.5 2.4 %collective-permute-start.2 = (bf16[288,128]{1,0:T(8,128)(2,1)S(1)}, bf16[288,128]{1,0:T(8,128)(2,1)S(1)}, u32[]{:S(2)}, u32[]{:S(2)}) collective-permute-start(bf16[288,128]{1,0:T(8,128)(2,1)S(1)} %forward.1.sums.own), channel_id=1, source_target_pairs={{0,48},{2,50},{4,52},{6,54},{8,56},{10,58},{12,60},{14,62},{16,0},... | collective-permute-start | bytes 221192 | tf_op jit(solution)/shard_map/ppermute | solution.py:34
  29.2 1.9 %fetch.1 = (bf16[12,512,128]{2,1,0:T(8,128)(2,1)S(1)}, bf16[12,512,128]{2,1,0:T(8,128)(2,1)S(1)}) custom-call(bf16[288,128]{1,0:T(8,128)(2,1)S(1)} %forward.1.sums.own, bf16[12,512,128]{2,1,0:T(8,128)(2,1)} %bitcast.19, bf16[12,512,128]{2,1,0:T(8,128)(2,1)} %bitcast.20), custom_call_target="tpu_custom_call" | custom-call | tf_op jit(solution)/shard_map/fetch/pallas_call | solution.py:472
  31.1 0.0 collective-permute-done.first_part
  31.1 0.0 collective-permute-done.1.second_part
  31.1 0.3 collective-permute-done.2.third_part
  31.4 1.3 %attend.1 = (bf16[8,288,128]{2,1,0:T(8,128)(2,1)S(1)}, bf16[192,128]{1,0:T(8,128)(2,1)S(1)}, s32[2]{0:T(128)S(4)}) custom-call(s32[1]{0:T(128)S(6)} %copy.16.prefix_len, s32[1]{0:T(128)S(6)} %copy.17.accepted, f32[12]{0:T(128)S(4)} %get-tuple-element.18.bias, bf16[288,128]{1,0:T(8,128)(2,1)S(1)} %forward.1.sums.own, ...), custom_call_target="tpu_custom_call" | custom-call | tf_op jit(solution)/shard_map/attend/pallas_call | solution.py:482
  32.7 11.3 %all_to_all.11.arrived = bf16[8,288,128]{2,1,0:T(8,128)(2,1)S(1)} all-to-all(bf16[8,288,128]{2,1,0:T(8,128)(2,1)S(1)} %get-tuple-element.24), channel_id=1, replica_groups={{0,2,4,6,8,10,12,14},{16,18,20,22,24,26,28,30},{32,34,36,38,40,42,44,46..., dimensions={0} | all-to-all | bytes 1179648 | tf_op jit(solution)/shard_map/all_to_all | solution.py:26
  44.0 0.5 merge.1
  44.5 6.3 %collective-permute-start.3 = (bf16[208,128]{1,0:T(8,128)(2,1)S(1)}, bf16[208,128]{1,0:T(8,128)(2,1)S(1)}, u32[]{:S(2)}, u32[]{:S(2)}) collective-permute-start(bf16[208,128]{1,0:T(8,128)(2,1)S(1)} %get-tuple-element.30.own), channel_id=1, source_target_pairs={{0,32},{2,34},{4,36},{6,38},{8,40},{10,42},{12,44},{14,46},{16,48}... | collective-permute-start | bytes 159752 | tf_op jit(solution)/shard_map/ppermute | solution.py:34
  50.8 0.0 collective-permute-start.4
  50.8 3.6 %collective-permute-start.5 = (bf16[208,128]{1,0:T(8,128)(2,1)S(1)}, bf16[208,128]{1,0:T(8,128)(2,1)S(1)}, u32[]{:S(2)}, u32[]{:S(2)}) collective-permute-start(bf16[208,128]{1,0:T(8,128)(2,1)S(1)} %get-tuple-element.30.own), channel_id=1, source_target_pairs={{0,48},{2,50},{4,52},{6,54},{8,56},{10,58},{12,60},{14,62},{16,0},... | collective-permute-start | bytes 159752 | tf_op jit(solution)/shard_map/ppermute | solution.py:34
  54.4 2.5 %tree.1 = (f32[192,128]{1,0:T(8,128)S(1)}, f32[192,128]{1,0:T(8,128)S(1)}, f32[192,128]{1,0:T(8,128)S(1)}, bf16[12,512,128]{2,1,0:T(8,128)(2,1)}, bf16[12,512,128]{2,1,0:T(8,128)(2,1)}) custom-call(s32[2]{0:T(128)S(4)} %get-tuple-element.22.limits, f32[12]{0:T(128)S(4)} %get-tuple-element.18.bias, s32[16]{0:T(128)S(4)} %get-tuple-element.23.parent, ...), custom_call_target="tpu_custom_call" | custom-call | tf_op jit(solution)/shard_map/tree/pallas_call | solution.py:510
  56.9 0.0 collective-permute-done.3.first_part
  56.9 0.5 collective-permute-done.4.second_part
  57.4 0.0 collective-permute-done.5.third_part
  57.4 0.4 finish.1
  57.8 2.5 %collective-permute-start.6 = (bf16[16,64]{1,0:T(8,128)(2,1)S(1)}, bf16[16,64]{1,0:T(8,128)(2,1)S(1)}, u32[]{:S(2)}, u32[]{:S(2)}) collective-permute-start(bf16[16,64]{1,0:T(8,128)(2,1)S(1)} %finish.1), channel_id=1, source_target_pairs={{0,1},{1,0},{2,3},{3,2},{4,5},{5,4},{6,7},{7,6},{8,9},{9,8},{10,11... | collective-permute-start | bytes 6152 | tf_op jit(solution)/shard_map/ppermute | solution.py:544
  60.3 0.8 %collective-permute-done.6 = bf16[16,64]{1,0:T(8,128)(2,1)S(1)} collective-permute-done((bf16[16,64]{1,0:T(8,128)(2,1)S(1)}, bf16[16,64]{1,0:T(8,128)(2,1)S(1)}, u32[]{:S(2)}, u32[]{:S(2)}) %collective-permute-start.6) | collective-permute-done | bytes 2080 | tf_op jit(solution)/shard_map/ppermute | solution.py:544
  61.1 0.6 fusion
  (2 shorter events, 0.0 us)
Async XLA Ops:
  18.2 12.9 %collective-permute-start = (bf16[288,128]{1,0:T(8,128)(2,1)S(1)}, bf16[288,128]{1,0:T(8,128)(2,1)S(1)}, u32[]{:S(2)}, u32[]{:S(2)}) collective-permute-start(bf16[288,128]{1,0:T(8,128)(2,1)S(1)} %forward.1.sums.own), channel_id=1, source_target_pairs={{0,32},{2,34},{4,36},{6,38},{8,40},{10,42},{12,44},{14,46},{16,48}... | collective-permute-start | bytes 221192 | tf_op jit(solution)/shard_map/ppermute | solution.py:34
  24.3 6.8 %collective-permute-start.1 = (bf16[288,128]{1,0:T(8,128)(2,1)S(1)}, bf16[288,128]{1,0:T(8,128)(2,1)S(1)}, u32[]{:S(2)}, u32[]{:S(2)}) collective-permute-start(bf16[288,128]{1,0:T(8,128)(2,1)S(1)} %forward.1.sums.own), channel_id=1, source_target_pairs={{0,16},{2,18},{4,20},{6,22},{8,24},{10,26},{12,28},{14,30},{16,32}... | collective-permute-start | bytes 221192 | tf_op jit(solution)/shard_map/ppermute | solution.py:34
  25.5 5.9 %collective-permute-start.2 = (bf16[288,128]{1,0:T(8,128)(2,1)S(1)}, bf16[288,128]{1,0:T(8,128)(2,1)S(1)}, u32[]{:S(2)}, u32[]{:S(2)}) collective-permute-start(bf16[288,128]{1,0:T(8,128)(2,1)S(1)} %forward.1.sums.own), channel_id=1, source_target_pairs={{0,48},{2,50},{4,52},{6,54},{8,56},{10,58},{12,60},{14,62},{16,0},... | collective-permute-start | bytes 221192 | tf_op jit(solution)/shard_map/ppermute | solution.py:34
  44.5 12.4 %collective-permute-start.3 = (bf16[208,128]{1,0:T(8,128)(2,1)S(1)}, bf16[208,128]{1,0:T(8,128)(2,1)S(1)}, u32[]{:S(2)}, u32[]{:S(2)}) collective-permute-start(bf16[208,128]{1,0:T(8,128)(2,1)S(1)} %get-tuple-element.30.own), channel_id=1, source_target_pairs={{0,32},{2,34},{4,36},{6,38},{8,40},{10,42},{12,44},{14,46},{16,48}... | collective-permute-start | bytes 159752 | tf_op jit(solution)/shard_map/ppermute | solution.py:34
  50.8 6.6 %collective-permute-start.4 = (bf16[208,128]{1,0:T(8,128)(2,1)S(1)}, bf16[208,128]{1,0:T(8,128)(2,1)S(1)}, u32[]{:S(2)}, u32[]{:S(2)}) collective-permute-start(bf16[208,128]{1,0:T(8,128)(2,1)S(1)} %get-tuple-element.30.own), channel_id=1, source_target_pairs={{0,16},{2,18},{4,20},{6,22},{8,24},{10,26},{12,28},{14,30},{16,32}... | collective-permute-start | bytes 159752 | tf_op jit(solution)/shard_map/ppermute | solution.py:34
  50.8 6.6 %collective-permute-start.5 = (bf16[208,128]{1,0:T(8,128)(2,1)S(1)}, bf16[208,128]{1,0:T(8,128)(2,1)S(1)}, u32[]{:S(2)}, u32[]{:S(2)}) collective-permute-start(bf16[208,128]{1,0:T(8,128)(2,1)S(1)} %get-tuple-element.30.own), channel_id=1, source_target_pairs={{0,48},{2,50},{4,52},{6,54},{8,56},{10,58},{12,60},{14,62},{16,0},... | collective-permute-start | bytes 159752 | tf_op jit(solution)/shard_map/ppermute | solution.py:34
  54.4 3.0 %copy-start = (bf16[1536,64]{0,1:T(8,128)(2,1)S(1)}, bf16[1536,64]{0,1:T(8,128)(2,1)}, u32[]{:S(2)}) copy-start(bf16[1536,64]{0,1:T(8,128)(2,1)} %param.19) | copy-start | bytes 589828
  57.8 3.3 %collective-permute-start.6 = (bf16[16,64]{1,0:T(8,128)(2,1)S(1)}, bf16[16,64]{1,0:T(8,128)(2,1)S(1)}, u32[]{:S(2)}, u32[]{:S(2)}) collective-permute-start(bf16[16,64]{1,0:T(8,128)(2,1)S(1)} %finish.1), channel_id=1, source_target_pairs={{0,1},{1,0},{2,3},{3,2},{4,5},{5,4},{6,7},{7,6},{8,9},{9,8},{10,11... | collective-permute-start | bytes 6152 | tf_op jit(solution)/shard_map/ppermute | solution.py:544

commit v7 on v6

--- a/solution.py
+++ b/solution.py
@@ -11,7 +11,8 @@
 INNER = 8
 PROPS = 16
 WINDOW = 32
-STEPS = (2, 1, 3)
+FIRST = (2, 3, 1)
+LAST = (2, 1, 3)
 F32 = jnp.float32
 BF16 = jnp.bfloat16
 VMEM = pl.BlockSpec(memory_space=pltpu.VMEM)
@@ -26,10 +27,10 @@
     return held(lax.all_to_all(pieces, "kv", 0, 0, axis_index_groups=groups, tiled=True))
 
 
-def shifted(value):
+def shifted(value, steps):
     count = lax.axis_size("kv")
     parts = [value]
-    for step in STEPS:
+    for step in steps:
         pairs = [(spot, (spot + step * INNER) % count) for spot in range(count)]
         parts.append(lax.ppermute(value, "kv", pairs))
     return [held(part) for part in parts]
@@ -272,8 +273,8 @@
     factors = factors[::-1]
     for head in range(heads):
         there = slice(head * PROPS, (head + 1) * PROPS)
-        total = jnp.zeros((PROPS, HEAD), F32)
-        for source in range(count):
+        total = arrived[count - 1, there, :].astype(F32)
+        for source in range(count - 1):
             total = total + factors[source][:, head : head + 1] * arrived[
                 source, there, :
             ].astype(F32)
@@ -341,7 +342,7 @@
         takes.append(take)
         keeps.append(jnp.where(family, keep, 0.0))
     later, tail = after_and_all(jnp.concatenate(keeps, axis=0), after_table(PROPS))
-    tail_out[...] = tail
+    tail_out[...] = jnp.exp(tail)
     for head in range(heads):
         there = slice(head * PROPS, (head + 1) * PROPS)
         weight = jnp.where(family, jnp.exp(takes[head] + later[there, :PROPS]), 0.0).astype(BF16)
@@ -362,21 +363,20 @@
     rows = own.shape[0] - PROPS
     heads = rows // PROPS
     place = lax.axis_index("kv") // INNER
-    spots = [lax.rem(place + outer - step, outer) for step in (0, *STEPS)]
+    spots = [lax.rem(place + outer - step, outer) for step in (0, *LAST)]
     rests = [rest_sums(part[rows:, :]) for part in parts]
     beyonds = []
     for spot in spots:
         beyond = jnp.zeros((PROPS, HEAD), F32)
         for other, rest in zip(spots, rests):
             beyond = beyond + jnp.where(other > spot, rest, 0.0)
-        beyonds.append(beyond)
+        beyonds.append(jnp.exp(beyond))
     for head in range(heads):
         there = slice(head * PROPS, (head + 1) * PROPS)
-        total = tree[there, :]
-        for part, beyond in zip(parts, beyonds):
-            total = total + jnp.exp(beyond[:, head : head + 1] + tail[there, :]) * part[
-                there, :
-            ].astype(F32)
+        total = jnp.zeros((PROPS, HEAD), F32)
+        for part, scale in zip(parts, beyonds):
+            total = total + scale[:, head : head + 1] * part[there, :].astype(F32)
+        total = tree[there, :] + total * tail[there, :]
         mixin[:, head * HEAD : (head + 1) * HEAD] = (total * gate[there, :]).astype(BF16)
     out[...] = dot_t(mixin[...], w_out[...]).astype(BF16)
 
@@ -494,7 +494,7 @@
         prefix_len,
         accepted,
         bias,
-        *shifted(pieces),
+        *shifted(pieces, FIRST),
         keys,
         values,
     )
@@ -506,7 +506,7 @@
         name="merge",
         compiler_params=PARAMS,
     )(exchange(pieces))
-    parts = shifted(pieces)
+    parts = shifted(pieces, LAST)
     tree, tail, gate, keys_next, values_next = pl.pallas_call(
         tree_kernel,
         out_shape=(

time: 62 us -> 61.8 us (level)
  starting transfers between devices: 22 us -> 18.1 us
  waiting for transfers between devices: 1.66 us -> 5.49 us
    ppermute x6, starting transfers between devices: 19.6 us -> 15.5 us  [shifted(): parts.append(lax.ppermute(value, 'kv', pairs))]
    ppermute x6, waiting for transfers between devices: 0.84 us -> 4.66 us  [shifted(): parts.append(lax.ppermute(value, 'kv', pairs))]
where the time goes in v7:
time: 61.8 us; the launch traced here: 61.6 us
  blocking collectives  26.9 us (44%)
  starting transfers between devices  18.1 us (29%)
  Pallas kernels  8.42 us (14%)
  waiting for transfers between devices  5.49 us (9%)
  between operations  1.99 us (3%)
    all_to_all x2, blocking collectives, exchange(): lax.all_to_all(pieces, 'kv', 0, 0, axis_index_groups=groups, tiled=True)  26.9 us
    ppermute x6, starting transfers between devices, shifted(): parts.append(lax.ppermute(value, 'kv', pairs))  15.5 us
    ppermute x6, waiting for transfers between devices, shifted(): parts.append(lax.ppermute(value, 'kv', pairs))  4.66 us
    ppermute x1, starting transfers between devices, local(): other = lax.ppermute(part_out, 'tp', [(0, 1), (1, 0)])  2.61 us
    pallas_call x1, Pallas kernels, local(): pl.pallas_call(tree_kernel, out_shape=(*[near((rows, HEAD), F32)] * 3, sh...  2.59 us
    pallas_call x1, Pallas kernels, local(): pl.pallas_call(fetch_kernel, out_shape=(near(keys.shape), near(values.sha...  1.9 us
    pallas_call x1, Pallas kernels, local(): pl.pallas_call(project_kernel, out_shape=(near((INNER, sent, HEAD)), smal...  1.66 us
    pallas_call x1, Pallas kernels, local(): pl.pallas_call(attend_kernel, out_shape=(near((INNER, sent, HEAD)), near(...  1.28 us
  transfers between devices with their start and end apart: 7, of which 3 were waited for; matrix products, arithmetic and copies ran while one was open for 0% of the time, Pallas kernels for 7%

profile of v7, /device:TPU:1, one launch (start us, length us, event | category | flops | bytes accessed | tf_op | source)
XLA Modules:
  0.0 61.6 jit_solution(10696602694157786586)
XLA Ops:
  0.6 1.7 %project.1 = (bf16[8,288,128]{2,1,0:T(8,128)(2,1)S(1)}, f32[12]{0:T(128)S(4)}, s32[16]{0:T(128)S(4)}) custom-call(f32[12]{0:T(128)} %bias_far.1, s32[16]{0:T(128)} %bitcast.22, bf16[16,64]{1,0:T(8,128)(2,1)} %bitcast.21, f32[1,64]{1,0:T(1,128)} %bitcast.23, bf16[64,1536]{1,0:T(8,128)(2,1)} %query_far.1, bf16[64,1536]{1,0:T(8,128)(2,1)} %key_far.1, ...), custom_call_target="tpu_custom_call" | custom-call | tf_op jit(solution)/shard_map/project/pallas_call | solution.py:431
  2.3 15.8 %all_to_all.10.arrived = bf16[8,288,128]{2,1,0:T(8,128)(2,1)S(1)} all-to-all(bf16[8,288,128]{2,1,0:T(8,128)(2,1)S(1)} %get-tuple-element.19), channel_id=1, replica_groups={{0,2,4,6,8,10,12,14},{16,18,20,22,24,26,28,30},{32,34,36,38,40,42,44,46..., dimensions={0} | all-to-all | bytes 1179648 | tf_op jit(solution)/shard_map/all_to_all | solution.py:27
  18.1 0.1 forward.1.sums.own
  18.2 6.1 %collective-permute-start = (bf16[288,128]{1,0:T(8,128)(2,1)S(1)}, bf16[288,128]{1,0:T(8,128)(2,1)S(1)}, u32[]{:S(2)}, u32[]{:S(2)}) collective-permute-start(bf16[288,128]{1,0:T(8,128)(2,1)S(1)} %forward.1.sums.own), channel_id=1, source_target_pairs={{0,32},{2,34},{4,36},{6,38},{8,40},{10,42},{12,44},{14,46},{16,48}... | collective-permute-start | bytes 221192 | tf_op jit(solution)/shard_map/ppermute | solution.py:35
  24.3 0.3 collective-permute-start.1
  24.6 2.1 %collective-permute-start.2 = (bf16[288,128]{1,0:T(8,128)(2,1)S(1)}, bf16[288,128]{1,0:T(8,128)(2,1)S(1)}, u32[]{:S(2)}, u32[]{:S(2)}) collective-permute-start(bf16[288,128]{1,0:T(8,128)(2,1)S(1)} %forward.1.sums.own), channel_id=1, source_target_pairs={{0,16},{2,18},{4,20},{6,22},{8,24},{10,26},{12,28},{14,30},{16,32}... | collective-permute-start | bytes 221192 | tf_op jit(solution)/shard_map/ppermute | solution.py:35
  28.0 1.9 %fetch.1 = (bf16[12,512,128]{2,1,0:T(8,128)(2,1)S(1)}, bf16[12,512,128]{2,1,0:T(8,128)(2,1)S(1)}) custom-call(bf16[288,128]{1,0:T(8,128)(2,1)S(1)} %forward.1.sums.own, bf16[12,512,128]{2,1,0:T(8,128)(2,1)} %bitcast.19, bf16[12,512,128]{2,1,0:T(8,128)(2,1)} %bitcast.20), custom_call_target="tpu_custom_call" | custom-call | tf_op jit(solution)/shard_map/fetch/pallas_call | solution.py:472
  29.9 0.0 collective-permute-done.first_part
  29.9 2.2 %collective-permute-done.1.second_part = bf16[288,128]{1,0:T(8,128)(2,1)S(1)} collective-permute-done((bf16[288,128]{1,0:T(8,128)(2,1)S(1)}, bf16[288,128]{1,0:T(8,128)(2,1)S(1)}, u32[]{:S(2)}, u32[]{:S(2)}) %collective-permute-start.1) | collective-permute-done | bytes 73760 | tf_op jit(solution)/shard_map/ppermute | solution.py:35
  32.1 0.0 collective-permute-done.2.third_part
  32.1 1.3 %attend.1 = (bf16[8,288,128]{2,1,0:T(8,128)(2,1)S(1)}, bf16[192,128]{1,0:T(8,128)(2,1)S(1)}, s32[2]{0:T(128)S(4)}) custom-call(s32[1]{0:T(128)S(6)} %copy.16.prefix_len, s32[1]{0:T(128)S(6)} %copy.17.accepted, f32[12]{0:T(128)S(4)} %get-tuple-element.18.bias, bf16[288,128]{1,0:T(8,128)(2,1)S(1)} %forward.1.sums.own, ...), custom_call_target="tpu_custom_call" | custom-call | tf_op jit(solution)/shard_map/attend/pallas_call | solution.py:482
  33.4 11.2 %all_to_all.11.arrived = bf16[8,288,128]{2,1,0:T(8,128)(2,1)S(1)} all-to-all(bf16[8,288,128]{2,1,0:T(8,128)(2,1)S(1)} %get-tuple-element.24), channel_id=1, replica_groups={{0,2,4,6,8,10,12,14},{16,18,20,22,24,26,28,30},{32,34,36,38,40,42,44,46..., dimensions={0} | all-to-all | bytes 1179648 | tf_op jit(solution)/shard_map/all_to_all | solution.py:27
  44.5 0.5 merge.1
  45.0 3.3 %collective-permute-start.3 = (bf16[208,128]{1,0:T(8,128)(2,1)S(1)}, bf16[208,128]{1,0:T(8,128)(2,1)S(1)}, u32[]{:S(2)}, u32[]{:S(2)}) collective-permute-start(bf16[208,128]{1,0:T(8,128)(2,1)S(1)} %get-tuple-element.30.own), channel_id=1, source_target_pairs={{0,32},{2,34},{4,36},{6,38},{8,40},{10,42},{12,44},{14,46},{16,48}... | collective-permute-start | bytes 159752 | tf_op jit(solution)/shard_map/ppermute | solution.py:35
  48.3 3.0 %collective-permute-start.4 = (bf16[208,128]{1,0:T(8,128)(2,1)S(1)}, bf16[208,128]{1,0:T(8,128)(2,1)S(1)}, u32[]{:S(2)}, u32[]{:S(2)}) collective-permute-start(bf16[208,128]{1,0:T(8,128)(2,1)S(1)} %get-tuple-element.30.own), channel_id=1, source_target_pairs={{0,16},{2,18},{4,20},{6,22},{8,24},{10,26},{12,28},{14,30},{16,32}... | collective-permute-start | bytes 159752 | tf_op jit(solution)/shard_map/ppermute | solution.py:35
  51.2 0.8 %collective-permute-start.5 = (bf16[208,128]{1,0:T(8,128)(2,1)S(1)}, bf16[208,128]{1,0:T(8,128)(2,1)S(1)}, u32[]{:S(2)}, u32[]{:S(2)}) collective-permute-start(bf16[208,128]{1,0:T(8,128)(2,1)S(1)} %get-tuple-element.30.own), channel_id=1, source_target_pairs={{0,48},{2,50},{4,52},{6,54},{8,56},{10,58},{12,60},{14,62},{16,0},... | collective-permute-start | bytes 159752 | tf_op jit(solution)/shard_map/ppermute | solution.py:35
  52.0 2.6 %tree.1 = (f32[192,128]{1,0:T(8,128)S(1)}, f32[192,128]{1,0:T(8,128)S(1)}, f32[192,128]{1,0:T(8,128)S(1)}, bf16[12,512,128]{2,1,0:T(8,128)(2,1)}, bf16[12,512,128]{2,1,0:T(8,128)(2,1)}) custom-call(s32[2]{0:T(128)S(4)} %get-tuple-element.22.limits, f32[12]{0:T(128)S(4)} %get-tuple-element.18.bias, s32[16]{0:T(128)S(4)} %get-tuple-element.23.parent, ...), custom_call_target="tpu_custom_call" | custom-call | tf_op jit(solution)/shard_map/tree/pallas_call | solution.py:510
  54.6 0.0 collective-permute-done.3.first_part
  54.7 0.0 collective-permute-done.4.second_part
  54.7 2.4 %collective-permute-done.5.third_part = bf16[208,128]{1,0:T(8,128)(2,1)S(1)} collective-permute-done((bf16[208,128]{1,0:T(8,128)(2,1)S(1)}, bf16[208,128]{1,0:T(8,128)(2,1)S(1)}, u32[]{:S(2)}, u32[]{:S(2)}) %collective-permute-start.5) | collective-permute-done | bytes 53280 | tf_op jit(solution)/shard_map/ppermute | solution.py:35
  57.1 0.4 finish.1
  57.5 2.6 %collective-permute-start.6 = (bf16[16,64]{1,0:T(8,128)(2,1)S(1)}, bf16[16,64]{1,0:T(8,128)(2,1)S(1)}, u32[]{:S(2)}, u32[]{:S(2)}) collective-permute-start(bf16[16,64]{1,0:T(8,128)(2,1)S(1)} %finish.1), channel_id=1, source_target_pairs={{0,1},{1,0},{2,3},{3,2},{4,5},{5,4},{6,7},{7,6},{8,9},{9,8},{10,11... | collective-permute-start | bytes 6152 | tf_op jit(solution)/shard_map/ppermute | solution.py:544
  60.2 0.8 %collective-permute-done.6 = bf16[16,64]{1,0:T(8,128)(2,1)S(1)} collective-permute-done((bf16[16,64]{1,0:T(8,128)(2,1)S(1)}, bf16[16,64]{1,0:T(8,128)(2,1)S(1)}, u32[]{:S(2)}, u32[]{:S(2)}) %collective-permute-start.6) | collective-permute-done | bytes 2080 | tf_op jit(solution)/shard_map/ppermute | solution.py:544
  61.0 0.6 fusion
  (2 shorter events, 0.0 us)
Async XLA Ops:
  18.2 11.7 %collective-permute-start = (bf16[288,128]{1,0:T(8,128)(2,1)S(1)}, bf16[288,128]{1,0:T(8,128)(2,1)S(1)}, u32[]{:S(2)}, u32[]{:S(2)}) collective-permute-start(bf16[288,128]{1,0:T(8,128)(2,1)S(1)} %forward.1.sums.own), channel_id=1, source_target_pairs={{0,32},{2,34},{4,36},{6,38},{8,40},{10,42},{12,44},{14,46},{16,48}... | collective-permute-start | bytes 221192 | tf_op jit(solution)/shard_map/ppermute | solution.py:35
  24.3 7.8 %collective-permute-start.1 = (bf16[288,128]{1,0:T(8,128)(2,1)S(1)}, bf16[288,128]{1,0:T(8,128)(2,1)S(1)}, u32[]{:S(2)}, u32[]{:S(2)}) collective-permute-start(bf16[288,128]{1,0:T(8,128)(2,1)S(1)} %forward.1.sums.own), channel_id=1, source_target_pairs={{0,48},{2,50},{4,52},{6,54},{8,56},{10,58},{12,60},{14,62},{16,0},... | collective-permute-start | bytes 221192 | tf_op jit(solution)/shard_map/ppermute | solution.py:35
  24.6 7.5 %collective-permute-start.2 = (bf16[288,128]{1,0:T(8,128)(2,1)S(1)}, bf16[288,128]{1,0:T(8,128)(2,1)S(1)}, u32[]{:S(2)}, u32[]{:S(2)}) collective-permute-start(bf16[288,128]{1,0:T(8,128)(2,1)S(1)} %forward.1.sums.own), channel_id=1, source_target_pairs={{0,16},{2,18},{4,20},{6,22},{8,24},{10,26},{12,28},{14,30},{16,32}... | collective-permute-start | bytes 221192 | tf_op jit(solution)/shard_map/ppermute | solution.py:35
  45.0 9.7 %collective-permute-start.3 = (bf16[208,128]{1,0:T(8,128)(2,1)S(1)}, bf16[208,128]{1,0:T(8,128)(2,1)S(1)}, u32[]{:S(2)}, u32[]{:S(2)}) collective-permute-start(bf16[208,128]{1,0:T(8,128)(2,1)S(1)} %get-tuple-element.30.own), channel_id=1, source_target_pairs={{0,32},{2,34},{4,36},{6,38},{8,40},{10,42},{12,44},{14,46},{16,48}... | collective-permute-start | bytes 159752 | tf_op jit(solution)/shard_map/ppermute | solution.py:35
  48.3 6.4 %collective-permute-start.4 = (bf16[208,128]{1,0:T(8,128)(2,1)S(1)}, bf16[208,128]{1,0:T(8,128)(2,1)S(1)}, u32[]{:S(2)}, u32[]{:S(2)}) collective-permute-start(bf16[208,128]{1,0:T(8,128)(2,1)S(1)} %get-tuple-element.30.own), channel_id=1, source_target_pairs={{0,16},{2,18},{4,20},{6,22},{8,24},{10,26},{12,28},{14,30},{16,32}... | collective-permute-start | bytes 159752 | tf_op jit(solution)/shard_map/ppermute | solution.py:35
  51.2 5.9 %collective-permute-start.5 = (bf16[208,128]{1,0:T(8,128)(2,1)S(1)}, bf16[208,128]{1,0:T(8,128)(2,1)S(1)}, u32[]{:S(2)}, u32[]{:S(2)}) collective-permute-start(bf16[208,128]{1,0:T(8,128)(2,1)S(1)} %get-tuple-element.30.own), channel_id=1, source_target_pairs={{0,48},{2,50},{4,52},{6,54},{8,56},{10,58},{12,60},{14,62},{16,0},... | collective-permute-start | bytes 159752 | tf_op jit(solution)/shard_map/ppermute | solution.py:35
  52.0 5.1 %copy-start = (bf16[1536,64]{0,1:T(8,128)(2,1)S(1)}, bf16[1536,64]{0,1:T(8,128)(2,1)}, u32[]{:S(2)}) copy-start(bf16[1536,64]{0,1:T(8,128)(2,1)} %param.19) | copy-start | bytes 589828
  57.5 3.4 %collective-permute-start.6 = (bf16[16,64]{1,0:T(8,128)(2,1)S(1)}, bf16[16,64]{1,0:T(8,128)(2,1)S(1)}, u32[]{:S(2)}, u32[]{:S(2)}) collective-permute-start(bf16[16,64]{1,0:T(8,128)(2,1)S(1)} %finish.1), channel_id=1, source_target_pairs={{0,1},{1,0},{2,3},{3,2},{4,5},{5,4},{6,7},{7,6},{8,9},{9,8},{10,11... | collective-permute-start | bytes 6152 | tf_op jit(solution)/shard_map/ppermute | solution.py:544

commit v8 on v7

--- a/solution.py
+++ b/solution.py
@@ -91,10 +91,8 @@
 
 def after_and_all(values, table):
     high = values.astype(BF16)
-    rest = values - high.astype(F32)
-    middle = rest.astype(BF16)
-    low = (rest - middle.astype(F32)).astype(BF16)
-    sums = dot(high, table) + dot(middle, table) + dot(low, table)
+    rest = (values - high.astype(F32)).astype(BF16)
+    sums = dot(high, table) + dot(rest, table)
     return sums[:, :HEAD], sums[:, HEAD:]
 
 

time: 61.8 us -> 61.7 us (level)
  no operation moved by 1% of the time
where the time goes in v8:
time: 61.7 us; the launch traced here: 61.5 us
  blocking collectives  26.9 us (44%)
  starting transfers between devices  18.1 us (29%)
  Pallas kernels  8.33 us (14%)
  waiting for transfers between devices  5.49 us (9%)
  between operations  1.99 us (3%)
    all_to_all x2, blocking collectives, exchange(): lax.all_to_all(pieces, 'kv', 0, 0, axis_index_groups=groups, tiled=True)  26.9 us
    ppermute x6, starting transfers between devices, shifted(): parts.append(lax.ppermute(value, 'kv', pairs))  15.5 us
    ppermute x6, waiting for transfers between devices, shifted(): parts.append(lax.ppermute(value, 'kv', pairs))  4.67 us
    ppermute x1, starting transfers between devices, local(): other = lax.ppermute(part_out, 'tp', [(0, 1), (1, 0)])  2.61 us
    pallas_call x1, Pallas kernels, local(): pl.pallas_call(tree_kernel, out_shape=(*[near((rows, HEAD), F32)] * 3, sh...  2.59 us
    pallas_call x1, Pallas kernels, local(): pl.pallas_call(fetch_kernel, out_shape=(near(keys.shape), near(values.sha...  1.9 us
    pallas_call x1, Pallas kernels, local(): pl.pallas_call(project_kernel, out_shape=(near((INNER, sent, HEAD)), smal...  1.66 us
  transfers between devices with their start and end apart: 7, of which 3 were waited for; matrix products, arithmetic and copies ran while one was open for 0% of the time, Pallas kernels for 7%

profile of v8, /device:TPU:1, one launch (start us, length us, event | category | flops | bytes accessed | tf_op | source)
XLA Modules:
  0.0 61.5 jit_solution(14097537283308132271)
XLA Ops:
  0.6 1.7 %project.1 = (bf16[8,288,128]{2,1,0:T(8,128)(2,1)S(1)}, f32[12]{0:T(128)S(4)}, s32[16]{0:T(128)S(4)}) custom-call(f32[12]{0:T(128)} %bias_far.1, s32[16]{0:T(128)} %bitcast.22, bf16[16,64]{1,0:T(8,128)(2,1)} %bitcast.21, f32[1,64]{1,0:T(1,128)} %bitcast.23, bf16[64,1536]{1,0:T(8,128)(2,1)} %query_far.1, bf16[64,1536]{1,0:T(8,128)(2,1)} %key_far.1, ...), custom_call_target="tpu_custom_call" | custom-call | tf_op jit(solution)/shard_map/project/pallas_call | solution.py:429
  2.3 15.8 %all_to_all.10.arrived = bf16[8,288,128]{2,1,0:T(8,128)(2,1)S(1)} all-to-all(bf16[8,288,128]{2,1,0:T(8,128)(2,1)S(1)} %get-tuple-element.19), channel_id=1, replica_groups={{0,2,4,6,8,10,12,14},{16,18,20,22,24,26,28,30},{32,34,36,38,40,42,44,46..., dimensions={0} | all-to-all | bytes 1179648 | tf_op jit(solution)/shard_map/all_to_all | solution.py:27
  18.1 0.1 forward.1.sums.own
  18.2 6.1 %collective-permute-start = (bf16[288,128]{1,0:T(8,128)(2,1)S(1)}, bf16[288,128]{1,0:T(8,128)(2,1)S(1)}, u32[]{:S(2)}, u32[]{:S(2)}) collective-permute-start(bf16[288,128]{1,0:T(8,128)(2,1)S(1)} %forward.1.sums.own), channel_id=1, source_target_pairs={{0,32},{2,34},{4,36},{6,38},{8,40},{10,42},{12,44},{14,46},{16,48}... | collective-permute-start | bytes 221192 | tf_op jit(solution)/shard_map/ppermute | solution.py:35
  24.3 0.3 collective-permute-start.1
  24.6 2.1 %collective-permute-start.2 = (bf16[288,128]{1,0:T(8,128)(2,1)S(1)}, bf16[288,128]{1,0:T(8,128)(2,1)S(1)}, u32[]{:S(2)}, u32[]{:S(2)}) collective-permute-start(bf16[288,128]{1,0:T(8,128)(2,1)S(1)} %forward.1.sums.own), channel_id=1, source_target_pairs={{0,16},{2,18},{4,20},{6,22},{8,24},{10,26},{12,28},{14,30},{16,32}... | collective-permute-start | bytes 221192 | tf_op jit(solution)/shard_map/ppermute | solution.py:35
  28.0 1.9 %fetch.1 = (bf16[12,512,128]{2,1,0:T(8,128)(2,1)S(1)}, bf16[12,512,128]{2,1,0:T(8,128)(2,1)S(1)}) custom-call(bf16[288,128]{1,0:T(8,128)(2,1)S(1)} %forward.1.sums.own, bf16[12,512,128]{2,1,0:T(8,128)(2,1)} %bitcast.19, bf16[12,512,128]{2,1,0:T(8,128)(2,1)} %bitcast.20), custom_call_target="tpu_custom_call" | custom-call | tf_op jit(solution)/shard_map/fetch/pallas_call | solution.py:470
  29.9 0.0 collective-permute-done.first_part
  29.9 2.2 %collective-permute-done.1.second_part = bf16[288,128]{1,0:T(8,128)(2,1)S(1)} collective-permute-done((bf16[288,128]{1,0:T(8,128)(2,1)S(1)}, bf16[288,128]{1,0:T(8,128)(2,1)S(1)}, u32[]{:S(2)}, u32[]{:S(2)}) %collective-permute-start.1) | collective-permute-done | bytes 73760 | tf_op jit(solution)/shard_map/ppermute | solution.py:35
  32.1 0.0 collective-permute-done.2.third_part
  32.1 1.2 %attend.1 = (bf16[8,288,128]{2,1,0:T(8,128)(2,1)S(1)}, bf16[192,128]{1,0:T(8,128)(2,1)S(1)}, s32[2]{0:T(128)S(4)}) custom-call(s32[1]{0:T(128)S(6)} %copy.16.prefix_len, s32[1]{0:T(128)S(6)} %copy.17.accepted, f32[12]{0:T(128)S(4)} %get-tuple-element.18.bias, bf16[288,128]{1,0:T(8,128)(2,1)S(1)} %forward.1.sums.own, ...), custom_call_target="tpu_custom_call" | custom-call | tf_op jit(solution)/shard_map/attend/pallas_call | solution.py:480
  33.3 11.2 %all_to_all.11.arrived = bf16[8,288,128]{2,1,0:T(8,128)(2,1)S(1)} all-to-all(bf16[8,288,128]{2,1,0:T(8,128)(2,1)S(1)} %get-tuple-element.24), channel_id=1, replica_groups={{0,2,4,6,8,10,12,14},{16,18,20,22,24,26,28,30},{32,34,36,38,40,42,44,46..., dimensions={0} | all-to-all | bytes 1179648 | tf_op jit(solution)/shard_map/all_to_all | solution.py:27
  44.4 0.5 merge.1
  44.9 3.3 %collective-permute-start.3 = (bf16[208,128]{1,0:T(8,128)(2,1)S(1)}, bf16[208,128]{1,0:T(8,128)(2,1)S(1)}, u32[]{:S(2)}, u32[]{:S(2)}) collective-permute-start(bf16[208,128]{1,0:T(8,128)(2,1)S(1)} %get-tuple-element.30.own), channel_id=1, source_target_pairs={{0,32},{2,34},{4,36},{6,38},{8,40},{10,42},{12,44},{14,46},{16,48}... | collective-permute-start | bytes 159752 | tf_op jit(solution)/shard_map/ppermute | solution.py:35
  48.2 3.0 %collective-permute-start.4 = (bf16[208,128]{1,0:T(8,128)(2,1)S(1)}, bf16[208,128]{1,0:T(8,128)(2,1)S(1)}, u32[]{:S(2)}, u32[]{:S(2)}) collective-permute-start(bf16[208,128]{1,0:T(8,128)(2,1)S(1)} %get-tuple-element.30.own), channel_id=1, source_target_pairs={{0,16},{2,18},{4,20},{6,22},{8,24},{10,26},{12,28},{14,30},{16,32}... | collective-permute-start | bytes 159752 | tf_op jit(solution)/shard_map/ppermute | solution.py:35
  51.1 0.8 %collective-permute-start.5 = (bf16[208,128]{1,0:T(8,128)(2,1)S(1)}, bf16[208,128]{1,0:T(8,128)(2,1)S(1)}, u32[]{:S(2)}, u32[]{:S(2)}) collective-permute-start(bf16[208,128]{1,0:T(8,128)(2,1)S(1)} %get-tuple-element.30.own), channel_id=1, source_target_pairs={{0,48},{2,50},{4,52},{6,54},{8,56},{10,58},{12,60},{14,62},{16,0},... | collective-permute-start | bytes 159752 | tf_op jit(solution)/shard_map/ppermute | solution.py:35
  51.9 2.6 %tree.1 = (f32[192,128]{1,0:T(8,128)S(1)}, f32[192,128]{1,0:T(8,128)S(1)}, f32[192,128]{1,0:T(8,128)S(1)}, bf16[12,512,128]{2,1,0:T(8,128)(2,1)}, bf16[12,512,128]{2,1,0:T(8,128)(2,1)}) custom-call(s32[2]{0:T(128)S(4)} %get-tuple-element.22.limits, f32[12]{0:T(128)S(4)} %get-tuple-element.18.bias, s32[16]{0:T(128)S(4)} %get-tuple-element.23.parent, ...), custom_call_target="tpu_custom_call" | custom-call | tf_op jit(solution)/shard_map/tree/pallas_call | solution.py:508
  54.5 0.0 collective-permute-done.3.first_part
  54.5 0.0 collective-permute-done.4.second_part
  54.6 2.4 %collective-permute-done.5.third_part = bf16[208,128]{1,0:T(8,128)(2,1)S(1)} collective-permute-done((bf16[208,128]{1,0:T(8,128)(2,1)S(1)}, bf16[208,128]{1,0:T(8,128)(2,1)S(1)}, u32[]{:S(2)}, u32[]{:S(2)}) %collective-permute-start.5) | collective-permute-done | bytes 53280 | tf_op jit(solution)/shard_map/ppermute | solution.py:35
  57.0 0.4 finish.1
  57.4 2.6 %collective-permute-start.6 = (bf16[16,64]{1,0:T(8,128)(2,1)S(1)}, bf16[16,64]{1,0:T(8,128)(2,1)S(1)}, u32[]{:S(2)}, u32[]{:S(2)}) collective-permute-start(bf16[16,64]{1,0:T(8,128)(2,1)S(1)} %finish.1), channel_id=1, source_target_pairs={{0,1},{1,0},{2,3},{3,2},{4,5},{5,4},{6,7},{7,6},{8,9},{9,8},{10,11... | collective-permute-start | bytes 6152 | tf_op jit(solution)/shard_map/ppermute | solution.py:542
  60.1 0.8 %collective-permute-done.6 = bf16[16,64]{1,0:T(8,128)(2,1)S(1)} collective-permute-done((bf16[16,64]{1,0:T(8,128)(2,1)S(1)}, bf16[16,64]{1,0:T(8,128)(2,1)S(1)}, u32[]{:S(2)}, u32[]{:S(2)}) %collective-permute-start.6) | collective-permute-done | bytes 2080 | tf_op jit(solution)/shard_map/ppermute | solution.py:542
  60.9 0.6 fusion
  (2 shorter events, 0.0 us)
Async XLA Ops:
  18.2 11.7 %collective-permute-start = (bf16[288,128]{1,0:T(8,128)(2,1)S(1)}, bf16[288,128]{1,0:T(8,128)(2,1)S(1)}, u32[]{:S(2)}, u32[]{:S(2)}) collective-permute-start(bf16[288,128]{1,0:T(8,128)(2,1)S(1)} %forward.1.sums.own), channel_id=1, source_target_pairs={{0,32},{2,34},{4,36},{6,38},{8,40},{10,42},{12,44},{14,46},{16,48}... | collective-permute-start | bytes 221192 | tf_op jit(solution)/shard_map/ppermute | solution.py:35
  24.3 7.8 %collective-permute-start.1 = (bf16[288,128]{1,0:T(8,128)(2,1)S(1)}, bf16[288,128]{1,0:T(8,128)(2,1)S(1)}, u32[]{:S(2)}, u32[]{:S(2)}) collective-permute-start(bf16[288,128]{1,0:T(8,128)(2,1)S(1)} %forward.1.sums.own), channel_id=1, source_target_pairs={{0,48},{2,50},{4,52},{6,54},{8,56},{10,58},{12,60},{14,62},{16,0},... | collective-permute-start | bytes 221192 | tf_op jit(solution)/shard_map/ppermute | solution.py:35
  24.6 7.5 %collective-permute-start.2 = (bf16[288,128]{1,0:T(8,128)(2,1)S(1)}, bf16[288,128]{1,0:T(8,128)(2,1)S(1)}, u32[]{:S(2)}, u32[]{:S(2)}) collective-permute-start(bf16[288,128]{1,0:T(8,128)(2,1)S(1)} %forward.1.sums.own), channel_id=1, source_target_pairs={{0,16},{2,18},{4,20},{6,22},{8,24},{10,26},{12,28},{14,30},{16,32}... | collective-permute-start | bytes 221192 | tf_op jit(solution)/shard_map/ppermute | solution.py:35
  44.9 9.7 %collective-permute-start.3 = (bf16[208,128]{1,0:T(8,128)(2,1)S(1)}, bf16[208,128]{1,0:T(8,128)(2,1)S(1)}, u32[]{:S(2)}, u32[]{:S(2)}) collective-permute-start(bf16[208,128]{1,0:T(8,128)(2,1)S(1)} %get-tuple-element.30.own), channel_id=1, source_target_pairs={{0,32},{2,34},{4,36},{6,38},{8,40},{10,42},{12,44},{14,46},{16,48}... | collective-permute-start | bytes 159752 | tf_op jit(solution)/shard_map/ppermute | solution.py:35
  48.2 6.4 %collective-permute-start.4 = (bf16[208,128]{1,0:T(8,128)(2,1)S(1)}, bf16[208,128]{1,0:T(8,128)(2,1)S(1)}, u32[]{:S(2)}, u32[]{:S(2)}) collective-permute-start(bf16[208,128]{1,0:T(8,128)(2,1)S(1)} %get-tuple-element.30.own), channel_id=1, source_target_pairs={{0,16},{2,18},{4,20},{6,22},{8,24},{10,26},{12,28},{14,30},{16,32}... | collective-permute-start | bytes 159752 | tf_op jit(solution)/shard_map/ppermute | solution.py:35
  51.1 5.9 %collective-permute-start.5 = (bf16[208,128]{1,0:T(8,128)(2,1)S(1)}, bf16[208,128]{1,0:T(8,128)(2,1)S(1)}, u32[]{:S(2)}, u32[]{:S(2)}) collective-permute-start(bf16[208,128]{1,0:T(8,128)(2,1)S(1)} %get-tuple-element.30.own), channel_id=1, source_target_pairs={{0,48},{2,50},{4,52},{6,54},{8,56},{10,58},{12,60},{14,62},{16,0},... | collective-permute-start | bytes 159752 | tf_op jit(solution)/shard_map/ppermute | solution.py:35
  51.9 5.1 %copy-start = (bf16[1536,64]{0,1:T(8,128)(2,1)S(1)}, bf16[1536,64]{0,1:T(8,128)(2,1)}, u32[]{:S(2)}) copy-start(bf16[1536,64]{0,1:T(8,128)(2,1)} %param.19) | copy-start | bytes 589828
  57.4 3.4 %collective-permute-start.6 = (bf16[16,64]{1,0:T(8,128)(2,1)S(1)}, bf16[16,64]{1,0:T(8,128)(2,1)S(1)}, u32[]{:S(2)}, u32[]{:S(2)}) collective-permute-start(bf16[16,64]{1,0:T(8,128)(2,1)S(1)} %finish.1), channel_id=1, source_target_pairs={{0,1},{1,0},{2,3},{3,2},{4,5},{5,4},{6,7},{7,6},{8,9},{9,8},{10,11... | collective-permute-start | bytes 6152 | tf_op jit(solution)/shard_map/ppermute | solution.py:542
